TPU v7x, 512 devices: a whole 4x8x8 slice. The times are simulated.
512 devices in a mesh: ep: 32 (over z, x), tp: 16 (over y, core).
Axes of the slice: x: 4, y: 8, z: 8, core: 2. Of those that a mesh axis runs over, the one named last changes fastest.
Arguments:
- tokens: bfloat16 [8192, 4096], P('ep', 'tp'), may hold values from -72 to 72
- pre_gain: float32 [4096], P('tp'), may hold values from 0.1 to 1.9
- expert_ids: int32 [8192, 3], P('ep'), may hold values from 0 to 63, all different within a row; in each aligned block of 256 rows (0 to 255, 256 to 511, ...) at most 16 rows name the same one
- route_weight: float32 [8192, 3], P('ep'), may hold values from 0.2 to 2
- expert_gate: bfloat16 [64, 1024, 4096], P('ep', 'tp'), may hold values from -0.09375 to 0.09375
- expert_up: bfloat16 [64, 1024, 4096], P('ep', 'tp'), may hold values from -0.09375 to 0.09375
- expert_down: bfloat16 [64, 1024, 4096], P('ep', None, 'tp'), may hold values from -0.9375 to 0.9375
- shared_gate: bfloat16 [1024, 4096], P('tp'), may hold values from -0.09375 to 0.09375
- shared_up: bfloat16 [1024, 4096], P('tp'), may hold values from -0.09375 to 0.09375
- shared_down: bfloat16 [1024, 4096], P(None, 'tp'), may hold values from -0.9375 to 0.9375
- out_gain: float32 [4096], P('tp'), may hold values from 0.1 to 1.9
Outputs:
- mixed: bfloat16 [8192, 4096], P('ep', 'tp')
Inputs may be any that keep to these rules, and one draw needn't show every extreme that they name: `expert_ids`: A row names 3 different experts. Among the rows of one index of ep no expert is named more than 16 times, and in every draw some expert is named exactly 16 times there.
All inputs are finite; a program needn't handle non-finite values.
Results may differ from a plain program's by a relative error of at most 0.0068.
Values may be sent and summed in bfloat16 or wider, within the bound.
No kernel may reach another device: no remote copies, remote signals or barrier semaphores. Data moves between devices by JAX's collectives and lax.ppermute only.
A program may use at most 64 MiB of HBM per device.

v0:
```python
import functools

import jax
import jax.numpy as jnp
from jax import lax
from jax.experimental import pallas as pl
from jax.experimental.pallas import tpu as pltpu
from jax.sharding import PartitionSpec as P


EPSILON = 1e-06
BF = jnp.bfloat16
F32 = jnp.float32


VMEM = pl.BlockSpec(memory_space=pltpu.VMEM)
SMEM = pl.BlockSpec(memory_space=pltpu.SMEM)


def after(x, *first):
    return lax.optimization_barrier((x,) + first)[0]


def times(x, w):
    return lax.dot_general(x, w, (((1,), (1,)), ((), ())), preferred_element_type=F32)


def product(pieces, places, spans, n_y, width, y, w_refs, half, total):
    for piece, (k, offset) in zip(pieces, places):
        if k != half:
            continue
        at = pl.multiple_of(lax.rem(y + offset + n_y, n_y) * width, width)
        for i, (low, high, which) in enumerate(spans[half]):
            term = times(piece[low:high, :], w_refs[which][:, pl.ds(at, width)])
            total[i] = term if total[i] is None else total[i] + term
    return total


def early_kernel(places, spans, n_y, width, y_ref, w_ref, sw_ref, *refs):
    out_ref = refs[-1]
    n_sub = out_ref.shape[0] // 2
    for half in range(2):
        total = [None] * len(spans[half])
        total = product(refs[:-1], places, spans, n_y, width, y_ref[0], (w_ref, sw_ref), half, total)
        for (low, high, _), value in zip(spans[half], total):
            out_ref[half * n_sub + low : half * n_sub + high, :] = value


def late_kernel(places, spans, n_y, width, y_ref, w_ref, sw_ref, total_ref, scale_ref, *refs):
    out_ref = refs[-1]
    n_sub = out_ref.shape[0] // 2
    for half in range(2):
        at = [slice(half * n_sub + low, half * n_sub + high) for low, high, _ in spans[half]]
        total = [total_ref[rows, :] for rows in at]
        total = product(refs[:-1], places, spans, n_y, width, y_ref[0], (w_ref, sw_ref), half, total)
        for rows, value in zip(at, total):
            out_ref[rows, :] = activated(value * scale_ref[rows, :])


def activated(total):
    n = total.shape[1] // 2
    gate, up = total[:, :n], total[:, n:]
    return (gate / (1.0 + jnp.exp(-gate)) * up).astype(BF)


def call(kernel, out, flops, args, smem=0):
    size = sum(a.size * a.dtype.itemsize for a in args)
    return pl.pallas_call(
        kernel,
        out_shape=out,
        in_specs=[SMEM] * smem + [VMEM] * (len(args) - smem),
        out_specs=VMEM,
        cost_estimate=pl.CostEstimate(flops=flops, bytes_accessed=size, transcendentals=0),
    )(*args)


def body(
    tokens,
    pre_gain,
    expert_ids,
    route_weight,
    expert_gate,
    expert_up,
    expert_down,
    shared_gate,
    shared_up,
    shared_down,
    out_gain,
):
    tok, top = expert_ids.shape
    n_ep = lax.axis_size("ep")
    n_tp = lax.axis_size("tp")
    n_y = n_tp // 2
    experts = expert_gate.shape[0] * n_ep
    cap = 4 * tok * top // (3 * experts)
    feat = tokens.shape[1]
    feat_all = feat * n_tp
    width = 2 * feat
    hid = expert_gate.shape[1]
    n_hid = expert_down.shape[1]
    half = tok // 2
    slots = n_ep * cap
    tp = lax.axis_index("tp")
    core = lax.rem(tp, 2)
    y = lax.div(tp, 2)
    first = core == 0
    other_core = 1 - core

    swap = [(i, i ^ 1) for i in range(n_tp)]
    y_groups = [[c + 2 * k for k in range(n_y)] for c in range(2)]

    def y_shift(d):
        return [(i, ((i // 2 + d) % n_y) * 2 + i % 2) for i in range(n_tp)]

    def own_first(mine, other, axis):
        return jnp.where(
            first,
            jnp.concatenate([mine, other], axis=axis),
            jnp.concatenate([other, mine], axis=axis),
        )

    def to_all_y(v):
        sent = jnp.broadcast_to(v[None], (n_y,) + v.shape)
        return lax.all_to_all(sent, "tp", 0, 0, axis_index_groups=y_groups, tiled=True)

    whole = own_first(tokens, lax.ppermute(tokens, "tp", swap), 1)
    ids = expert_ids.T
    named = 2 * jnp.arange(n_ep, dtype=jnp.int32)[:, None] + core
    hit = [(ids[k][None, :] == named) for k in range(top)]
    member = hit[0] | hit[1] | hit[2]
    earlier = (
        jnp.arange(tok, dtype=jnp.int32)[:, None] < jnp.arange(tok, dtype=jnp.int32)[None, :]
    ).astype(BF)
    rank = jnp.dot(member.astype(BF), earlier, preferred_element_type=F32)
    rank = jnp.where(member, rank, -1.0)
    slot_no = jnp.arange(cap, dtype=jnp.int32).astype(F32)
    pick = rank[:, None, :] == slot_no[None, :, None]
    one_hot = pick.astype(BF).reshape(slots, tok)
    outgoing = jnp.dot(one_hot, whole, preferred_element_type=F32).astype(BF)
    arrived = lax.all_to_all(outgoing.reshape(n_ep, cap, width), "ep", 0, 0, tiled=True)
    arrived = arrived.reshape(slots, width)

    gain = own_first(pre_gain, lax.ppermute(after(pre_gain, outgoing), "tp", swap), 0)
    own_rows = lax.dynamic_slice_in_dim(whole, core * half, half, 0)

    e_gate, e_up, s_gate, s_up, _ = lax.optimization_barrier((expert_gate, expert_up, shared_gate, shared_up, outgoing))
    sent_in = jnp.concatenate(
        [
            lax.dynamic_index_in_dim(e_gate, other_core, 0, keepdims=False),
            lax.dynamic_index_in_dim(e_up, other_core, 0, keepdims=False),
            s_gate,
            s_up,
        ],
        axis=0,
    )
    got_in = lax.ppermute(sent_in, "tp", swap)
    in_w = jnp.concatenate(
        [
            own_first(lax.dynamic_index_in_dim(e_gate, core, 0, keepdims=False), got_in[:hid], 0),
            own_first(
                lax.dynamic_index_in_dim(e_up, core, 0, keepdims=False), got_in[hid : 2 * hid], 0
            ),
        ],
        axis=0,
    )
    sin_w = jnp.concatenate(
        [own_first(s_gate, got_in[2 * hid : 3 * hid], 0), own_first(s_up, got_in[3 * hid :], 0)],
        axis=0,
    )
    e_down, s_down, _ = lax.optimization_barrier((expert_down, shared_down, outgoing))
    sent_out = jnp.concatenate(
        [lax.dynamic_index_in_dim(e_down, other_core, 0, keepdims=False), s_down], axis=0
    )
    got_out = lax.ppermute(sent_out, "tp", swap)
    down_w = own_first(
        lax.dynamic_index_in_dim(e_down, core, 0, keepdims=False), got_out[:n_hid], 1
    ).reshape(n_y, 2 * hid, width)
    sdown_w = own_first(s_down, got_out[n_hid:], 1).reshape(n_y, 2 * hid, width)

    rows = slots + half
    n_sub = rows // 2
    raw = jnp.concatenate([arrived, own_rows], axis=0).astype(F32)
    chunk = (raw * gain).astype(BF)
    square = jnp.sum(raw * raw, axis=1)
    spans = (((0, n_sub, 0),), ((0, slots - n_sub, 0), (slots - n_sub, n_sub, 1)))
    fwd = [chunk[:n_sub], chunk[n_sub:]]
    bwd = list(fwd)
    early, early_at = list(fwd), [(0, 0), (1, 0)]
    late, late_at = [], []
    for step in range(1, n_y // 2 + 1):
        last = step == n_y // 2
        pieces, at = (late, late_at) if last else (early, early_at)
        for k in range(2):
            if not last or k == 0:
                fwd[k] = lax.ppermute(fwd[k], "tp", y_shift(1))
                pieces.append(fwd[k])
                at.append((k, -step))
            if not last or k == 1:
                bwd[k] = lax.ppermute(bwd[k], "tp", y_shift(-1))
                pieces.append(bwd[k])
                at.append((k, step))
        if step == 1:
            square_sum = jnp.sum(to_all_y(after(square, fwd[0])), axis=0)
            scale = lax.rsqrt(square_sum / feat_all + EPSILON)[:, None]

    where = y[None].astype(jnp.int32)
    flops = 2 * rows * feat_all * 4 * hid
    total = call(
        functools.partial(early_kernel, early_at, spans, n_y, width),
        jax.ShapeDtypeStruct((rows, 4 * hid), F32),
        flops,
        (where, in_w, sin_w, *early),
        smem=1,
    )
    hidden = call(
        functools.partial(late_kernel, late_at, spans, n_y, width),
        jax.ShapeDtypeStruct((rows, 2 * hid), BF),
        flops // n_y,
        (where, in_w, sin_w, total, scale, *late),
        smem=1,
    )

    hidden_all = to_all_y(hidden)
    contract = (((0, 2), (0, 1)), ((), ()))
    expert_out = lax.dot_general(hidden_all[:, :slots], down_w, contract, preferred_element_type=F32).astype(BF)
    returned = lax.all_to_all(expert_out.reshape(n_ep, cap, width), "ep", 0, 0, tiled=True)
    returned = returned.reshape(slots, width)

    shared_out = lax.dot_general(hidden_all[:, slots:], sdown_w, contract, preferred_element_type=F32)
    weight = sum(jnp.where(hit[k], route_weight.T[k][None, :], 0.0) for k in range(top))
    mix = jnp.where(pick, weight[:, None, :], 0.0).reshape(slots, tok)
    high = lax.reduce_precision(mix, 8, 7)
    middle = lax.reduce_precision(mix - high, 8, 7)
    low = mix - high - middle
    part = sum(
        lax.dot_general(m.astype(BF), returned, (((0,), (0,)), ((), ())), preferred_element_type=F32)
        for m in (high, middle, low)
    )
    zero = jnp.zeros_like(shared_out)
    part = part + jnp.where(
        first,
        jnp.concatenate([shared_out, zero], axis=0),
        jnp.concatenate([zero, shared_out], axis=0),
    )
    away = jnp.where(first, part[:, feat:], part[:, :feat])
    home = jnp.where(first, part[:, :feat], part[:, feat:])
    summed = home + lax.ppermute(away, "tp", swap)
    own_square = jnp.sum(summed * summed, axis=1)
    sent = jnp.broadcast_to(own_square[None, :], (n_tp, tok))
    out_square = jnp.sum(lax.all_to_all(sent, "tp", 0, 0, tiled=True), axis=0)
    return (summed * lax.rsqrt(out_square[:, None] / feat_all + EPSILON) * out_gain).astype(BF)


def solution(mesh):
    return jax.shard_map(
        body,
        mesh=mesh,
        in_specs=(
            P("ep", "tp"),
            P("tp"),
            P("ep", None),
            P("ep", None),
            P("ep", "tp", None),
            P("ep", "tp", None),
            P("ep", None, "tp"),
            P("tp", None),
            P("tp", None),
            P(None, "tp"),
            P("tp"),
        ),
        out_specs=P("ep", "tp"),
        check_vma=False,
    )
```

profile of v0, /device:TPU:1, one launch (start us, length us, event | category | flops | bytes accessed | tf_op | source)
XLA Modules:
  0.0 190.2 jit_solution(12357325269507463793)
XLA Ops:
  0.0 8.9 %collective-permute-start = (bf16[256,256]{1,0:T(8,128)(2,1)}, bf16[256,256]{1,0:T(8,128)(2,1)S(1)}, u32[]{:S(2)}, u32[]{:S(2)}) collective-permute-start(bf16[256,256]{1,0:T(8,128)(2,1)} %param.11), channel_id=1, source_target_pairs={{0,1},{1,0},{2,3},{3,2},{4,5},{5,4},{6,7},{7,6},{8,9},{9,8},{10,11... | collective-permute-start | bytes 393224 | tf_op jit(solution)/shard_map/ppermute | solution.py:126
  13.8 7.5 %all-to-all-start = ((bf16[32,16,512]{2,1,0:T(8,128)(2,1)}), bf16[32,16,512]{2,1,0:T(8,128)(2,1)S(1)}, u32[]{:S(2)}, u32[]{:S(2)}) async-start(bf16[32,16,512]{2,1,0:T(8,128)(2,1)} %bitcast.14), calls=%async_computation | async-start | bytes 1048576 | tf_op jit(solution)/shard_map/all_to_all | solution.py:140
  22.9 2.2 %collective-permute-start.1 = (bf16[256,4096]{1,0:T(8,128)(2,1)}, bf16[256,4096]{1,0:T(8,128)(2,1)S(1)}, u32[]{:S(2)}, u32[]{:S(2)}) collective-permute-start(bf16[256,4096]{1,0:T(8,128)(2,1)} %pad_maximum_fusion), channel_id=1, source_target_pairs={{0,1},{1,0},{2,3},{3,2},{4,5},{5,4},{6,7},{7,6},{8,9},{9,8},{10,11... | collective-permute-start | bytes 6291464 | tf_op jit(solution)/shard_map/ppermute | solution.py:156
  25.1 2.1 %collective-permute-start.2 = (f32[256]{0:T(256)S(1)}, f32[256]{0:T(256)S(1)}, u32[]{:S(2)}, u32[]{:S(2)}) collective-permute-start(f32[256]{0:T(256)S(1)} %copy-done.17), channel_id=1, source_target_pairs={{0,1},{1,0},{2,3},{3,2},{4,5},{5,4},{6,7},{7,6},{8,9},{9,8},{10,11... | collective-permute-start | bytes 3080 | tf_op jit(solution)/shard_map/ppermute | solution.py:143
  29.2 9.0 %all-to-all-done = bf16[32,16,512]{2,1,0:T(8,128)(2,1)S(1)} async-done(((bf16[32,16,512]{2,1,0:T(8,128)(2,1)}), bf16[32,16,512]{2,1,0:T(8,128)(2,1)S(1)}, u32[]{:S(2)}, u32[]{:S(2)}) %all-to-all-start) | async-done | bytes 524320 | tf_op jit(solution)/shard_map/all_to_all | solution.py:140
  38.4 3.2 %collective-permute-start.3 = (bf16[320,512]{1,0:T(8,128)(2,1)S(1)}, bf16[320,512]{1,0:T(8,128)(2,1)S(1)}, u32[]{:S(2)}, u32[]{:S(2)}) collective-permute-start(bf16[320,512]{1,0:T(8,128)(2,1)S(1)} %get-tuple-element.38.refs_0_), channel_id=1, source_target_pairs={{0,2},{1,3},{2,4},{3,5},{4,6},{5,7},{6,8},{7,9},{8,10},{9,11},{10,... | collective-permute-start | bytes 983048 | tf_op jit(solution)/shard_map/ppermute | solution.py:195
  41.7 3.8 %collective-permute-start.6 = (bf16[320,512]{1,0:T(8,128)(2,1)S(1)}, bf16[320,512]{1,0:T(8,128)(2,1)S(1)}, u32[]{:S(2)}, u32[]{:S(2)}) collective-permute-start(bf16[320,512]{1,0:T(8,128)(2,1)S(1)} %get-tuple-element.37.refs_1_), channel_id=1, source_target_pairs={{0,14},{1,15},{2,0},{3,1},{4,2},{5,3},{6,4},{7,5},{8,6},{9,7},{10,... | collective-permute-start | bytes 983048 | tf_op jit(solution)/shard_map/ppermute | solution.py:199
  45.5 3.4 %collective-permute-start.4 = (bf16[320,512]{1,0:T(8,128)(2,1)S(1)}, bf16[320,512]{1,0:T(8,128)(2,1)}, u32[]{:S(2)}, u32[]{:S(2)}) collective-permute-start(bf16[320,512]{1,0:T(8,128)(2,1)S(1)} %get-tuple-element.38.refs_0_), channel_id=1, source_target_pairs={{0,14},{1,15},{2,0},{3,1},{4,2},{5,3},{6,4},{7,5},{8,6},{9,7},{10,... | collective-permute-start | bytes 983048 | tf_op jit(solution)/shard_map/ppermute | solution.py:199
  48.9 1.9 %collective-permute-start.5 = (bf16[320,512]{1,0:T(8,128)(2,1)S(1)}, bf16[320,512]{1,0:T(8,128)(2,1)}, u32[]{:S(2)}, u32[]{:S(2)}) collective-permute-start(bf16[320,512]{1,0:T(8,128)(2,1)S(1)} %get-tuple-element.37.refs_1_), channel_id=1, source_target_pairs={{0,2},{1,3},{2,4},{3,5},{4,6},{5,7},{6,8},{7,9},{8,10},{9,11},{10,... | collective-permute-start | bytes 983048 | tf_op jit(solution)/shard_map/ppermute | solution.py:195
  50.8 1.9 %collective-permute-start.7 = (bf16[320,512]{1,0:T(8,128)(2,1)S(1)}, bf16[320,512]{1,0:T(8,128)(2,1)}, u32[]{:S(2)}, u32[]{:S(2)}) collective-permute-start(bf16[320,512]{1,0:T(8,128)(2,1)S(1)} %collective-permute-done.3.refs_2_), channel_id=1, source_target_pairs={{0,2},{1,3},{2,4},{3,5},{4,6},{5,7},{6,8},{7,9},{8,10},{9,11},{10,... | collective-permute-start | bytes 983048 | tf_op jit(solution)/shard_map/ppermute | solution.py:195
  52.8 4.6 %collective-permute-start.10 = (bf16[320,512]{1,0:T(8,128)(2,1)S(1)}, bf16[320,512]{1,0:T(8,128)(2,1)}, u32[]{:S(2)}, u32[]{:S(2)}) collective-permute-start(bf16[320,512]{1,0:T(8,128)(2,1)S(1)} %collective-permute-done.6.refs_5_), channel_id=1, source_target_pairs={{0,14},{1,15},{2,0},{3,1},{4,2},{5,3},{6,4},{7,5},{8,6},{9,7},{10,... | collective-permute-start | bytes 983048 | tf_op jit(solution)/shard_map/ppermute | solution.py:199
  57.6 5.3 %collective-permute-start.8 = (bf16[320,512]{1,0:T(8,128)(2,1)}, bf16[320,512]{1,0:T(8,128)(2,1)}, u32[]{:S(2)}, u32[]{:S(2)}) collective-permute-start(bf16[320,512]{1,0:T(8,128)(2,1)} %collective-permute-done.4.refs_3_), channel_id=1, source_target_pairs={{0,14},{1,15},{2,0},{3,1},{4,2},{5,3},{6,4},{7,5},{8,6},{9,7},{10,... | collective-permute-start | bytes 983048 | tf_op jit(solution)/shard_map/ppermute | solution.py:199
  63.0 1.9 %collective-permute-start.9 = (bf16[320,512]{1,0:T(8,128)(2,1)}, bf16[320,512]{1,0:T(8,128)(2,1)}, u32[]{:S(2)}, u32[]{:S(2)}) collective-permute-start(bf16[320,512]{1,0:T(8,128)(2,1)} %collective-permute-done.5.refs_4_), channel_id=1, source_target_pairs={{0,2},{1,3},{2,4},{3,5},{4,6},{5,7},{6,8},{7,9},{8,10},{9,11},{10,... | collective-permute-start | bytes 983048 | tf_op jit(solution)/shard_map/ppermute | solution.py:195
  65.5 1.9 %collective-permute-start.11 = (bf16[320,512]{1,0:T(8,128)(2,1)}, bf16[320,512]{1,0:T(8,128)(2,1)}, u32[]{:S(2)}, u32[]{:S(2)}) collective-permute-start(bf16[320,512]{1,0:T(8,128)(2,1)} %collective-permute-done.7.refs_6_), channel_id=1, source_target_pairs={{0,2},{1,3},{2,4},{3,5},{4,6},{5,7},{6,8},{7,9},{8,10},{9,11},{10,... | collective-permute-start | bytes 983048 | tf_op jit(solution)/shard_map/ppermute | solution.py:195
  67.4 4.6 %collective-permute-start.14 = (bf16[320,512]{1,0:T(8,128)(2,1)}, bf16[320,512]{1,0:T(8,128)(2,1)}, u32[]{:S(2)}, u32[]{:S(2)}) collective-permute-start(bf16[320,512]{1,0:T(8,128)(2,1)} %collective-permute-done.10.refs_9_), channel_id=1, source_target_pairs={{0,14},{1,15},{2,0},{3,1},{4,2},{5,3},{6,4},{7,5},{8,6},{9,7},{10,... | collective-permute-start | bytes 983048 | tf_op jit(solution)/shard_map/ppermute | solution.py:199
  72.6 5.4 %all-to-all-start.1 = ((f32[8,1,640]{2,1,0:T(1,128)}), f32[8,1,640]{2,1,0:T(1,128)S(1)}, u32[]{:S(2)}, u32[]{:S(2)}) async-start(f32[8,1,640]{2,1,0:T(1,128)} %broadcast_in_dim.89), calls=%async_computation.1 | async-start | bytes 40960 | tf_op jit(solution)/shard_map/all_to_all | solution.py:124
  78.1 6.9 %all-to-all-done.1 = f32[8,1,640]{2,1,0:T(1,128)S(1)} async-done(((f32[8,1,640]{2,1,0:T(1,128)}), f32[8,1,640]{2,1,0:T(1,128)S(1)}, u32[]{:S(2)}, u32[]{:S(2)}) %all-to-all-start.1) | async-done | bytes 20512 | tf_op jit(solution)/shard_map/all_to_all | solution.py:124
  85.9 2.2 %collective-permute-start.12 = (bf16[320,512]{1,0:T(8,128)(2,1)}, bf16[320,512]{1,0:T(8,128)(2,1)}, u32[]{:S(2)}, u32[]{:S(2)}) collective-permute-start(bf16[320,512]{1,0:T(8,128)(2,1)} %collective-permute-done.8.refs_7_), channel_id=1, source_target_pairs={{0,14},{1,15},{2,0},{3,1},{4,2},{5,3},{6,4},{7,5},{8,6},{9,7},{10,... | collective-permute-start | bytes 983048 | tf_op jit(solution)/shard_map/ppermute | solution.py:199
  88.1 3.2 %collective-permute-start.13 = (bf16[320,512]{1,0:T(8,128)(2,1)}, bf16[320,512]{1,0:T(8,128)(2,1)}, u32[]{:S(2)}, u32[]{:S(2)}) collective-permute-start(bf16[320,512]{1,0:T(8,128)(2,1)} %collective-permute-done.9.refs_8_), channel_id=1, source_target_pairs={{0,2},{1,3},{2,4},{3,5},{4,6},{5,7},{6,8},{7,9},{8,10},{9,11},{10,... | collective-permute-start | bytes 983048 | tf_op jit(solution)/shard_map/ppermute | solution.py:195
  91.3 2.3 %collective-permute-start.15 = (bf16[320,512]{1,0:T(8,128)(2,1)}, bf16[320,512]{1,0:T(8,128)(2,1)}, u32[]{:S(2)}, u32[]{:S(2)}) collective-permute-start(bf16[320,512]{1,0:T(8,128)(2,1)} %collective-permute-done.11.refs_10_), channel_id=1, source_target_pairs={{0,2},{1,3},{2,4},{3,5},{4,6},{5,7},{6,8},{7,9},{8,10},{9,11},{10,... | collective-permute-start | bytes 983048 | tf_op jit(solution)/shard_map/ppermute | solution.py:195
  93.6 4.2 %collective-permute-start.16 = (bf16[320,512]{1,0:T(8,128)(2,1)}, bf16[320,512]{1,0:T(8,128)(2,1)}, u32[]{:S(2)}, u32[]{:S(2)}) collective-permute-start(bf16[320,512]{1,0:T(8,128)(2,1)} %collective-permute-done.14.refs_13_), channel_id=1, source_target_pairs={{0,14},{1,15},{2,0},{3,1},{4,2},{5,3},{6,4},{7,5},{8,6},{9,7},{10,... | collective-permute-start | bytes 983048 | tf_op jit(solution)/shard_map/ppermute | solution.py:199
  102.2 6.1 %shard_map.109.total_ref = f32[640,256]{1,0:T(8,128)} custom-call(s32[1]{0:T(128)} %bitcast.8.y_ref, bf16[256,4096]{1,0:T(8,128)(2,1)} %pad_maximum_fusion.1.w_ref, bf16[256,4096]{1,0:T(8,128)(2,1)} %pad_maximum_fusion.2.sw_ref, bf16[320,512]{1,0:T(8,128)(2,1)} %copy-done.6, bf16[320,512]{1,0:T(8,128)(2,1)} %copy-done.5, bf16[320,512]{1,0:T(8,128)(2,1)} %copy-done.11, ...), custom_call_target="tpu_custom_call" | custom-call | flops 1342177280 | bytes 8781828 | tf_op jit(solution)/shard_map/pallas_call | solution.py:68
  108.3 3.7 %shard_map.110 = bf16[640,128]{1,0:T(8,128)(2,1)} custom-call(s32[1]{0:T(128)} %bitcast.8.y_ref, bf16[256,4096]{1,0:T(8,128)(2,1)} %pad_maximum_fusion.1.w_ref, bf16[256,4096]{1,0:T(8,128)(2,1)} %pad_maximum_fusion.2.sw_ref, f32[640,256]{1,0:T(8,128)} %shard_map.109.total_ref, f32[640,1]{1,0:T(8,128)} %rsqrt.24.scale_ref, ...), custom_call_target="tpu_custom_call" | custom-call | flops 167772160 | bytes 5507588 | tf_op jit(solution)/shard_map/pallas_call | solution.py:68
  112.1 2.3 %broadcast_in_dim.90 = bf16[8,640,128]{2,1,0:T(8,128)(2,1)} broadcast(bf16[640,128]{1,0:T(8,128)(2,1)} %shard_map.110), dimensions={1,2} | broadcast | bytes 1474560 | tf_op jit(solution)/shard_map/broadcast_in_dim | solution.py:123
  114.4 3.7 %all-to-all-start.2 = ((bf16[8,640,128]{2,1,0:T(8,128)(2,1)}), bf16[8,640,128]{2,1,0:T(8,128)(2,1)S(1)}, u32[]{:S(2)}, u32[]{:S(2)}) async-start(bf16[8,640,128]{2,1,0:T(8,128)(2,1)} %broadcast_in_dim.90), calls=%async_computation.2 | async-start | bytes 2621440 | tf_op jit(solution)/shard_map/all_to_all | solution.py:124
  118.2 10.4 %collective-permute-start.17 = (bf16[2048,256]{1,0:T(8,128)(2,1)S(1)}, bf16[2048,256]{1,0:T(8,128)(2,1)S(1)}, u32[]{:S(2)}, u32[]{:S(2)}) collective-permute-start(bf16[2048,256]{1,0:T(8,128)(2,1)S(1)} %pad_maximum_fusion.3), channel_id=1, source_target_pairs={{0,1},{1,0},{2,3},{3,2},{4,5},{5,4},{6,7},{7,6},{8,9},{9,8},{10,11... | collective-permute-start | bytes 3145736 | tf_op jit(solution)/shard_map/ppermute | solution.py:174
  128.7 2.3 %collective-permute-done.17 = bf16[2048,256]{1,0:T(8,128)(2,1)S(1)} collective-permute-done((bf16[2048,256]{1,0:T(8,128)(2,1)S(1)}, bf16[2048,256]{1,0:T(8,128)(2,1)S(1)}, u32[]{:S(2)}, u32[]{:S(2)}) %collective-permute-start.17) | collective-permute-done | bytes 1048608 | tf_op jit(solution)/shard_map/ppermute | solution.py:174
  131.0 15.8 %all-to-all-done.2 = bf16[8,640,128]{2,1,0:T(8,128)(2,1)S(1)} async-done(((bf16[8,640,128]{2,1,0:T(8,128)(2,1)}), bf16[8,640,128]{2,1,0:T(8,128)(2,1)S(1)}, u32[]{:S(2)}, u32[]{:S(2)}) %all-to-all-start.2) | async-done | bytes 1310752 | tf_op jit(solution)/shard_map/all_to_all | solution.py:124
  148.4 6.9 %all-to-all-start.3 = ((bf16[32,16,512]{2,1,0:T(8,128)(2,1)}), bf16[32,16,512]{2,1,0:T(8,128)(2,1)S(1)}, u32[]{:S(2)}, u32[]{:S(2)}) async-start(bf16[32,16,512]{2,1,0:T(8,128)(2,1)} %bitcast.20), calls=%async_computation.3 | async-start | bytes 1048576 | tf_op jit(solution)/shard_map/all_to_all | solution.py:226
  155.8 12.3 %all-to-all-done.3 = bf16[32,16,512]{2,1,0:T(8,128)(2,1)S(1)} async-done(((bf16[32,16,512]{2,1,0:T(8,128)(2,1)}), bf16[32,16,512]{2,1,0:T(8,128)(2,1)S(1)}, u32[]{:S(2)}, u32[]{:S(2)}) %all-to-all-start.3) | async-done | bytes 524320 | tf_op jit(solution)/shard_map/all_to_all | solution.py:226
  169.4 8.6 %collective-permute-start.18 = (f32[256,256]{1,0:T(8,128)S(1)}, f32[256,256]{1,0:T(8,128)S(1)}, u32[]{:S(2)}, u32[]{:S(2)}) collective-permute-start(f32[256,256]{1,0:T(8,128)S(1)} %slice_select_fusion), channel_id=1, source_target_pairs={{0,1},{1,0},{2,3},{3,2},{4,5},{5,4},{6,7},{7,6},{8,9},{9,8},{10,11... | collective-permute-start | bytes 786440 | tf_op jit(solution)/shard_map/ppermute | solution.py:247
  179.3 10.1 %all_to_all.27 = f32[16,1,256]{2,1,0:T(1,128)S(1)} all-to-all(f32[16,1,256]{2,1,0:T(1,128)S(1)} %broadcast_in_dim.91), channel_id=1, replica_groups=mesh['ep'=32,'tp'=16] {'tp'}, dimensions={0} | all-to-all | bytes 32768 | tf_op jit(solution)/shard_map/all_to_all | solution.py:250
  (103 shorter events, 20.9 us)
Async XLA Ops:
  0.0 12.8 %copy-start.7 = (bf16[2,64,4096]{2,1,0:T(8,128)(2,1)S(1)}, bf16[2,64,4096]{2,1,0:T(8,128)(2,1)}, u32[]{:S(2)}) copy-start(bf16[2,64,4096]{2,1,0:T(8,128)(2,1)} %param.15) | copy-start | bytes 3145732
  0.0 10.7 %collective-permute-start = (bf16[256,256]{1,0:T(8,128)(2,1)}, bf16[256,256]{1,0:T(8,128)(2,1)S(1)}, u32[]{:S(2)}, u32[]{:S(2)}) collective-permute-start(bf16[256,256]{1,0:T(8,128)(2,1)} %param.11), channel_id=1, source_target_pairs={{0,1},{1,0},{2,3},{3,2},{4,5},{5,4},{6,7},{7,6},{8,9},{9,8},{10,11... | collective-permute-start | bytes 393224 | tf_op jit(solution)/shard_map/ppermute | solution.py:126
  13.8 24.3 %all-to-all-start = ((bf16[32,16,512]{2,1,0:T(8,128)(2,1)}), bf16[32,16,512]{2,1,0:T(8,128)(2,1)S(1)}, u32[]{:S(2)}, u32[]{:S(2)}) async-start(bf16[32,16,512]{2,1,0:T(8,128)(2,1)} %bitcast.14), calls=%async_computation | async-start | bytes 1048576 | tf_op jit(solution)/shard_map/all_to_all | solution.py:140
  22.9 74.9 %collective-permute-start.1 = (bf16[256,4096]{1,0:T(8,128)(2,1)}, bf16[256,4096]{1,0:T(8,128)(2,1)S(1)}, u32[]{:S(2)}, u32[]{:S(2)}) collective-permute-start(bf16[256,4096]{1,0:T(8,128)(2,1)} %pad_maximum_fusion), channel_id=1, source_target_pairs={{0,1},{1,0},{2,3},{3,2},{4,5},{5,4},{6,7},{7,6},{8,9},{9,8},{10,11... | collective-permute-start | bytes 6291464 | tf_op jit(solution)/shard_map/ppermute | solution.py:156
  25.1 4.0 %collective-permute-start.2 = (f32[256]{0:T(256)S(1)}, f32[256]{0:T(256)S(1)}, u32[]{:S(2)}, u32[]{:S(2)}) collective-permute-start(f32[256]{0:T(256)S(1)} %copy-done.17), channel_id=1, source_target_pairs={{0,1},{1,0},{2,3},{3,2},{4,5},{5,4},{6,7},{7,6},{8,9},{9,8},{10,11... | collective-permute-start | bytes 3080 | tf_op jit(solution)/shard_map/ppermute | solution.py:143
  38.4 59.6 %copy-start.5 = (bf16[320,512]{1,0:T(8,128)(2,1)}, bf16[320,512]{1,0:T(8,128)(2,1)S(1)}, u32[]{:S(2)}) copy-start(bf16[320,512]{1,0:T(8,128)(2,1)S(1)} %get-tuple-element.37.refs_1_) | copy-start | bytes 983044
  38.4 59.6 %copy-start.6 = (bf16[320,512]{1,0:T(8,128)(2,1)}, bf16[320,512]{1,0:T(8,128)(2,1)S(1)}, u32[]{:S(2)}) copy-start(bf16[320,512]{1,0:T(8,128)(2,1)S(1)} %get-tuple-element.38.refs_0_) | copy-start | bytes 983044
  38.4 12.3 %collective-permute-start.3 = (bf16[320,512]{1,0:T(8,128)(2,1)S(1)}, bf16[320,512]{1,0:T(8,128)(2,1)S(1)}, u32[]{:S(2)}, u32[]{:S(2)}) collective-permute-start(bf16[320,512]{1,0:T(8,128)(2,1)S(1)} %get-tuple-element.38.refs_0_), channel_id=1, source_target_pairs={{0,2},{1,3},{2,4},{3,5},{4,6},{5,7},{6,8},{7,9},{8,10},{9,11},{10,... | collective-permute-start | bytes 983048 | tf_op jit(solution)/shard_map/ppermute | solution.py:195
  41.7 11.1 %collective-permute-start.6 = (bf16[320,512]{1,0:T(8,128)(2,1)S(1)}, bf16[320,512]{1,0:T(8,128)(2,1)S(1)}, u32[]{:S(2)}, u32[]{:S(2)}) collective-permute-start(bf16[320,512]{1,0:T(8,128)(2,1)S(1)} %get-tuple-element.37.refs_1_), channel_id=1, source_target_pairs={{0,14},{1,15},{2,0},{3,1},{4,2},{5,3},{6,4},{7,5},{8,6},{9,7},{10,... | collective-permute-start | bytes 983048 | tf_op jit(solution)/shard_map/ppermute | solution.py:199
  45.5 12.2 %collective-permute-start.4 = (bf16[320,512]{1,0:T(8,128)(2,1)S(1)}, bf16[320,512]{1,0:T(8,128)(2,1)}, u32[]{:S(2)}, u32[]{:S(2)}) collective-permute-start(bf16[320,512]{1,0:T(8,128)(2,1)S(1)} %get-tuple-element.38.refs_0_), channel_id=1, source_target_pairs={{0,14},{1,15},{2,0},{3,1},{4,2},{5,3},{6,4},{7,5},{8,6},{9,7},{10,... | collective-permute-start | bytes 983048 | tf_op jit(solution)/shard_map/ppermute | solution.py:199
  48.9 14.1 %collective-permute-start.5 = (bf16[320,512]{1,0:T(8,128)(2,1)S(1)}, bf16[320,512]{1,0:T(8,128)(2,1)}, u32[]{:S(2)}, u32[]{:S(2)}) collective-permute-start(bf16[320,512]{1,0:T(8,128)(2,1)S(1)} %get-tuple-element.37.refs_1_), channel_id=1, source_target_pairs={{0,2},{1,3},{2,4},{3,5},{4,6},{5,7},{6,8},{7,9},{8,10},{9,11},{10,... | collective-permute-start | bytes 983048 | tf_op jit(solution)/shard_map/ppermute | solution.py:195
  50.8 12.2 %copy-start.11 = (bf16[320,512]{1,0:T(8,128)(2,1)}, bf16[320,512]{1,0:T(8,128)(2,1)S(1)}, u32[]{:S(2)}) copy-start(bf16[320,512]{1,0:T(8,128)(2,1)S(1)} %collective-permute-done.3.refs_2_) | copy-start | bytes 983044
  50.8 14.7 %collective-permute-start.7 = (bf16[320,512]{1,0:T(8,128)(2,1)S(1)}, bf16[320,512]{1,0:T(8,128)(2,1)}, u32[]{:S(2)}, u32[]{:S(2)}) collective-permute-start(bf16[320,512]{1,0:T(8,128)(2,1)S(1)} %collective-permute-done.3.refs_2_), channel_id=1, source_target_pairs={{0,2},{1,3},{2,4},{3,5},{4,6},{5,7},{6,8},{7,9},{8,10},{9,11},{10,... | collective-permute-start | bytes 983048 | tf_op jit(solution)/shard_map/ppermute | solution.py:195
  52.7 12.7 %copy-start.12 = (bf16[320,512]{1,0:T(8,128)(2,1)}, bf16[320,512]{1,0:T(8,128)(2,1)S(1)}, u32[]{:S(2)}) copy-start(bf16[320,512]{1,0:T(8,128)(2,1)S(1)} %collective-permute-done.6.refs_5_) | copy-start | bytes 983044
  52.8 14.7 %collective-permute-start.10 = (bf16[320,512]{1,0:T(8,128)(2,1)S(1)}, bf16[320,512]{1,0:T(8,128)(2,1)}, u32[]{:S(2)}, u32[]{:S(2)}) collective-permute-start(bf16[320,512]{1,0:T(8,128)(2,1)S(1)} %collective-permute-done.6.refs_5_), channel_id=1, source_target_pairs={{0,14},{1,15},{2,0},{3,1},{4,2},{5,3},{6,4},{7,5},{8,6},{9,7},{10,... | collective-permute-start | bytes 983048 | tf_op jit(solution)/shard_map/ppermute | solution.py:199
  57.6 28.2 %collective-permute-start.8 = (bf16[320,512]{1,0:T(8,128)(2,1)}, bf16[320,512]{1,0:T(8,128)(2,1)}, u32[]{:S(2)}, u32[]{:S(2)}) collective-permute-start(bf16[320,512]{1,0:T(8,128)(2,1)} %collective-permute-done.4.refs_3_), channel_id=1, source_target_pairs={{0,14},{1,15},{2,0},{3,1},{4,2},{5,3},{6,4},{7,5},{8,6},{9,7},{10,... | collective-permute-start | bytes 983048 | tf_op jit(solution)/shard_map/ppermute | solution.py:199
  63.0 25.1 %collective-permute-start.9 = (bf16[320,512]{1,0:T(8,128)(2,1)}, bf16[320,512]{1,0:T(8,128)(2,1)}, u32[]{:S(2)}, u32[]{:S(2)}) collective-permute-start(bf16[320,512]{1,0:T(8,128)(2,1)} %collective-permute-done.5.refs_4_), channel_id=1, source_target_pairs={{0,2},{1,3},{2,4},{3,5},{4,6},{5,7},{6,8},{7,9},{8,10},{9,11},{10,... | collective-permute-start | bytes 983048 | tf_op jit(solution)/shard_map/ppermute | solution.py:195
  65.5 25.8 %collective-permute-start.11 = (bf16[320,512]{1,0:T(8,128)(2,1)}, bf16[320,512]{1,0:T(8,128)(2,1)}, u32[]{:S(2)}, u32[]{:S(2)}) collective-permute-start(bf16[320,512]{1,0:T(8,128)(2,1)} %collective-permute-done.7.refs_6_), channel_id=1, source_target_pairs={{0,2},{1,3},{2,4},{3,5},{4,6},{5,7},{6,8},{7,9},{8,10},{9,11},{10,... | collective-permute-start | bytes 983048 | tf_op jit(solution)/shard_map/ppermute | solution.py:195
  67.4 26.2 %collective-permute-start.14 = (bf16[320,512]{1,0:T(8,128)(2,1)}, bf16[320,512]{1,0:T(8,128)(2,1)}, u32[]{:S(2)}, u32[]{:S(2)}) collective-permute-start(bf16[320,512]{1,0:T(8,128)(2,1)} %collective-permute-done.10.refs_9_), channel_id=1, source_target_pairs={{0,14},{1,15},{2,0},{3,1},{4,2},{5,3},{6,4},{7,5},{8,6},{9,7},{10,... | collective-permute-start | bytes 983048 | tf_op jit(solution)/shard_map/ppermute | solution.py:199
  72.6 12.3 %all-to-all-start.1 = ((f32[8,1,640]{2,1,0:T(1,128)}), f32[8,1,640]{2,1,0:T(1,128)S(1)}, u32[]{:S(2)}, u32[]{:S(2)}) async-start(f32[8,1,640]{2,1,0:T(1,128)} %broadcast_in_dim.89), calls=%async_computation.1 | async-start | bytes 40960 | tf_op jit(solution)/shard_map/all_to_all | solution.py:124
  85.8 12.2 %copy-start.4 = (bf16[64,4096]{1,0:T(8,128)(2,1)S(1)}, bf16[64,4096]{1,0:T(8,128)(2,1)}, u32[]{:S(2)}) copy-start(bf16[64,4096]{1,0:T(8,128)(2,1)} %param.18) | copy-start | bytes 1572868
  85.9 16.3 %collective-permute-start.12 = (bf16[320,512]{1,0:T(8,128)(2,1)}, bf16[320,512]{1,0:T(8,128)(2,1)}, u32[]{:S(2)}, u32[]{:S(2)}) collective-permute-start(bf16[320,512]{1,0:T(8,128)(2,1)} %collective-permute-done.8.refs_7_), channel_id=1, source_target_pairs={{0,14},{1,15},{2,0},{3,1},{4,2},{5,3},{6,4},{7,5},{8,6},{9,7},{10,... | collective-permute-start | bytes 983048 | tf_op jit(solution)/shard_map/ppermute | solution.py:199
  88.1 14.1 %collective-permute-start.13 = (bf16[320,512]{1,0:T(8,128)(2,1)}, bf16[320,512]{1,0:T(8,128)(2,1)}, u32[]{:S(2)}, u32[]{:S(2)}) collective-permute-start(bf16[320,512]{1,0:T(8,128)(2,1)} %collective-permute-done.9.refs_8_), channel_id=1, source_target_pairs={{0,2},{1,3},{2,4},{3,5},{4,6},{5,7},{6,8},{7,9},{8,10},{9,11},{10,... | collective-permute-start | bytes 983048 | tf_op jit(solution)/shard_map/ppermute | solution.py:195
  91.3 17.0 %collective-permute-start.15 = (bf16[320,512]{1,0:T(8,128)(2,1)}, bf16[320,512]{1,0:T(8,128)(2,1)}, u32[]{:S(2)}, u32[]{:S(2)}) collective-permute-start(bf16[320,512]{1,0:T(8,128)(2,1)} %collective-permute-done.11.refs_10_), channel_id=1, source_target_pairs={{0,2},{1,3},{2,4},{3,5},{4,6},{5,7},{6,8},{7,9},{8,10},{9,11},{10,... | collective-permute-start | bytes 983048 | tf_op jit(solution)/shard_map/ppermute | solution.py:195
  93.6 14.7 %collective-permute-start.16 = (bf16[320,512]{1,0:T(8,128)(2,1)}, bf16[320,512]{1,0:T(8,128)(2,1)}, u32[]{:S(2)}, u32[]{:S(2)}) collective-permute-start(bf16[320,512]{1,0:T(8,128)(2,1)} %collective-permute-done.14.refs_13_), channel_id=1, source_target_pairs={{0,14},{1,15},{2,0},{3,1},{4,2},{5,3},{6,4},{7,5},{8,6},{9,7},{10,... | collective-permute-start | bytes 983048 | tf_op jit(solution)/shard_map/ppermute | solution.py:199
  114.4 32.5 %all-to-all-start.2 = ((bf16[8,640,128]{2,1,0:T(8,128)(2,1)}), bf16[8,640,128]{2,1,0:T(8,128)(2,1)S(1)}, u32[]{:S(2)}, u32[]{:S(2)}) async-start(bf16[8,640,128]{2,1,0:T(8,128)(2,1)} %broadcast_in_dim.90), calls=%async_computation.2 | async-start | bytes 2621440 | tf_op jit(solution)/shard_map/all_to_all | solution.py:124
  118.2 12.7 %collective-permute-start.17 = (bf16[2048,256]{1,0:T(8,128)(2,1)S(1)}, bf16[2048,256]{1,0:T(8,128)(2,1)S(1)}, u32[]{:S(2)}, u32[]{:S(2)}) collective-permute-start(bf16[2048,256]{1,0:T(8,128)(2,1)S(1)} %pad_maximum_fusion.3), channel_id=1, source_target_pairs={{0,1},{1,0},{2,3},{3,2},{4,5},{5,4},{6,7},{7,6},{8,9},{9,8},{10,11... | collective-permute-start | bytes 3145736 | tf_op jit(solution)/shard_map/ppermute | solution.py:174
  148.4 19.7 %all-to-all-start.3 = ((bf16[32,16,512]{2,1,0:T(8,128)(2,1)}), bf16[32,16,512]{2,1,0:T(8,128)(2,1)S(1)}, u32[]{:S(2)}, u32[]{:S(2)}) async-start(bf16[32,16,512]{2,1,0:T(8,128)(2,1)} %bitcast.20), calls=%async_computation.3 | async-start | bytes 1048576 | tf_op jit(solution)/shard_map/all_to_all | solution.py:226
  155.4 12.7 %copy-start.14 = (f32[32,256]{1,0:T(8,128)S(1)}, f32[32,256]{1,0:T(8,128)}, u32[]{:S(2)}) copy-start(f32[32,256]{1,0:T(8,128)} %copy-done.13) | copy-start | bytes 98308
  155.4 12.6 %copy-start.21 = (f32[16]{0:T(128)S(1)}, f32[16]{0:T(128)}, u32[]{:S(2)}) copy-start(f32[16]{0:T(128)} %copy-done.20) | copy-start | bytes 196
  168.9 20.6 %copy-start.16 = (f32[256]{0:T(256)S(1)}, f32[256]{0:T(256)}, u32[]{:S(2)}) copy-start(f32[256]{0:T(256)} %param.21) | copy-start | bytes 3076
  169.4 9.7 %collective-permute-start.18 = (f32[256,256]{1,0:T(8,128)S(1)}, f32[256,256]{1,0:T(8,128)S(1)}, u32[]{:S(2)}, u32[]{:S(2)}) collective-permute-start(f32[256,256]{1,0:T(8,128)S(1)} %slice_select_fusion), channel_id=1, source_target_pairs={{0,1},{1,0},{2,3},{3,2},{4,5},{5,4},{6,7},{7,6},{8,9},{9,8},{10,11... | collective-permute-start | bytes 786440 | tf_op jit(solution)/shard_map/ppermute | solution.py:247
  (13 other events, 66.6 us)
where the time goes:
time: 191 us; the launch traced here: 190 us
  starting transfers between devices  100 us (52%)
  waiting for transfers between devices  50.1 us (26%)
  blocking collectives  10.1 us (5%)
  Pallas kernels  9.87 us (5%)
  other arithmetic  8.24 us (4%)
  local copies, waits for them, and re-layouts  6.58 us (3%)
  matrix products  4.44 us (2%)
    ppermute x7, starting transfers between devices, body(): bwd[k] = lax.ppermute(bwd[k], 'tp', y_shift(-1))  28 us
    all_to_all x2, waiting for transfers between devices, to_all_y(): lax.all_to_all(sent, 'tp', 0, 0, axis_index_groups=y_groups, tiled=True)  22.7 us
    ppermute x7, starting transfers between devices, body(): fwd[k] = lax.ppermute(fwd[k], 'tp', y_shift(1))  16.4 us
    all_to_all x1, waiting for transfers between devices, body(): lax.all_to_all(expert_out.reshape(n_ep, cap, width), 'ep', 0, 0, tiled=True)  12.3 us
    ppermute x1, starting transfers between devices, body(): got_out = lax.ppermute(sent_out, 'tp', swap)  10.4 us
    all_to_all x1, blocking collectives, body(): out_square = jnp.sum(lax.all_to_all(sent, 'tp', 0, 0, tiled=True), axis=0)  10.1 us
    pallas_call x2, Pallas kernels, call(): pl.pallas_call(kernel, out_shape=out, in_specs=[SMEM] * smem + [VMEM] * (...  9.87 us
    all_to_all x2, starting transfers between devices, to_all_y(): lax.all_to_all(sent, 'tp', 0, 0, axis_index_groups=y_groups, tiled=True)  9.15 us
  transfers between devices with their start and end apart: 23, of which 9 were waited for; matrix products, arithmetic and copies ran while one was open for 5% of the time, Pallas kernels for 3%

commit v1 on v0

--- a/solution.py
+++ b/solution.py
@@ -15,6 +15,7 @@
 
 VMEM = pl.BlockSpec(memory_space=pltpu.VMEM)
 SMEM = pl.BlockSpec(memory_space=pltpu.SMEM)
+HBM = pl.BlockSpec(memory_space=pltpu.HBM)
 
 
 def after(x, *first):
@@ -25,53 +26,98 @@
     return lax.dot_general(x, w, (((1,), (1,)), ((), ())), preferred_element_type=F32)
 
 
-def product(pieces, places, spans, n_y, width, y, w_refs, half, total):
-    for piece, (k, offset) in zip(pieces, places):
-        if k != half:
-            continue
-        at = pl.multiple_of(lax.rem(y + offset + n_y, n_y) * width, width)
-        for i, (low, high, which) in enumerate(spans[half]):
-            term = times(piece[low:high, :], w_refs[which][:, pl.ds(at, width)])
-            total[i] = term if total[i] is None else total[i] + term
-    return total
-
-
-def early_kernel(places, spans, n_y, width, y_ref, w_ref, sw_ref, *refs):
-    out_ref = refs[-1]
-    n_sub = out_ref.shape[0] // 2
+def early_kernel(places, spans, n_y, width, at_ref, gate, up, s_gate, s_up, got, *refs):
+    n = len(places)
+    pieces = refs[:n]
+    total_ref, w_last, sw_last = refs[n : n + 3]
+    w, sw, held, w_sem, sem = refs[n + 3 :]
+    core, y = at_ref[0], at_ref[1]
+    hid = s_gate.shape[0]
+    n_sub = total_ref.shape[0] // 2
+    own = pl.multiple_of(core * hid, hid)
+    other = pl.multiple_of((1 - core) * hid, hid)
+    moves = []
+    for i, (mine, into, base) in enumerate(
+        ((gate.at[core], w, 0), (up.at[core], w, 2 * hid), (s_gate, sw, 0), (s_up, sw, 2 * hid))
+    ):
+        moves.append(pltpu.make_async_copy(mine, into.at[pl.ds(base + own, hid)], w_sem.at[2 * i]))
+        theirs = got.at[pl.ds(i * hid, hid)]
+        moves.append(pltpu.make_async_copy(theirs, into.at[pl.ds(base + other, hid)], w_sem.at[2 * i + 1]))
+    loads = [pltpu.make_async_copy(p, held.at[i], sem.at[i]) for i, p in enumerate(pieces)]
+    for copy in moves + loads:
+        copy.start()
+    for copy in moves:
+        copy.wait()
     for half in range(2):
         total = [None] * len(spans[half])
-        total = product(refs[:-1], places, spans, n_y, width, y_ref[0], (w_ref, sw_ref), half, total)
+        for i, (k, offset) in enumerate(places):
+            if k != half:
+                continue
+            loads[i].wait()
+            at = pl.multiple_of(lax.rem(y + offset + n_y, n_y) * width, width)
+            for j, (low, high, which) in enumerate(spans[half]):
+                term = times(held[i, low:high, :], (w, sw)[which][:, pl.ds(at, width)])
+                total[j] = term if total[j] is None else total[j] + term
         for (low, high, _), value in zip(spans[half], total):
-            out_ref[half * n_sub + low : half * n_sub + high, :] = value
-
-
-def late_kernel(places, spans, n_y, width, y_ref, w_ref, sw_ref, total_ref, scale_ref, *refs):
+            total_ref[half * n_sub + low : half * n_sub + high, :] = value
+    at = pl.multiple_of(lax.rem(y + n_y // 2, n_y) * width, width)
+    w_last[...] = w[:, pl.ds(at, width)]
+    sw_last[...] = sw[:, pl.ds(at, width)]
+
+
+def late_kernel(spans, w_ref, sw_ref, total_ref, scale_ref, *refs):
     out_ref = refs[-1]
-    n_sub = out_ref.shape[0] // 2
+    n_sub = total_ref.shape[0] // 2
     for half in range(2):
-        at = [slice(half * n_sub + low, half * n_sub + high) for low, high, _ in spans[half]]
-        total = [total_ref[rows, :] for rows in at]
-        total = product(refs[:-1], places, spans, n_y, width, y_ref[0], (w_ref, sw_ref), half, total)
-        for rows, value in zip(at, total):
-            out_ref[rows, :] = activated(value * scale_ref[rows, :])
+        for low, high, which in spans[half]:
+            rows = slice(half * n_sub + low, half * n_sub + high)
+            total = total_ref[rows, :] + times(refs[half][low:high, :], (w_ref, sw_ref)[which][...])
+            hidden = activated(total * scale_ref[rows, :])
+            for j in range(out_ref.shape[0]):
+                out_ref[j, rows, :] = hidden
+
+
+def pack_kernel(at_ref, *refs):
+    n = len(refs) - 3
+    arrays, out_ref, held, sem = refs[:n], refs[n], refs[n + 1], refs[n + 2]
+    rows = out_ref.shape[0] // n
+    ins = []
+    for i, a in enumerate(arrays):
+        part = a.at[1 - at_ref[0]] if len(a.shape) == 3 else a
+        ins.append(pltpu.make_async_copy(part, held.at[pl.ds(i * rows, rows)], sem.at[i]))
+    outs = [
+        pltpu.make_async_copy(
+            held.at[pl.ds(i * rows, rows)], out_ref.at[pl.ds(i * rows, rows)], sem.at[n + i]
+        )
+        for i in range(n)
+    ]
+    for copy in ins:
+        copy.start()
+    for i in range(n):
+        ins[i].wait()
+        outs[i].start()
+    for copy in outs:
+        copy.wait()
+
+
+def pack(at, arrays):
+    rows, cols = arrays[0].shape[-2:]
+    shape = (rows * len(arrays), cols)
+    return pl.pallas_call(
+        pack_kernel,
+        out_shape=jax.ShapeDtypeStruct(shape, BF),
+        in_specs=[SMEM] + [HBM] * len(arrays),
+        out_specs=HBM,
+        scratch_shapes=[pltpu.VMEM(shape, BF), pltpu.SemaphoreType.DMA((2 * len(arrays),))],
+        cost_estimate=pl.CostEstimate(flops=4 * 10**8, bytes_accessed=2**22, transcendentals=0),
+        compiler_params=pltpu.CompilerParams(vmem_limit_bytes=4 * 2**20),
+    )(at, *arrays)
 
 
 def activated(total):
     n = total.shape[1] // 2
     gate, up = total[:, :n], total[:, n:]
     return (gate / (1.0 + jnp.exp(-gate)) * up).astype(BF)
-
-
-def call(kernel, out, flops, args, smem=0):
-    size = sum(a.size * a.dtype.itemsize for a in args)
-    return pl.pallas_call(
-        kernel,
-        out_shape=out,
-        in_specs=[SMEM] * smem + [VMEM] * (len(args) - smem),
-        out_specs=VMEM,
-        cost_estimate=pl.CostEstimate(flops=flops, bytes_accessed=size, transcendentals=0),
-    )(*args)
 
 
 def body(
@@ -104,8 +150,8 @@
     core = lax.rem(tp, 2)
     y = lax.div(tp, 2)
     first = core == 0
-    other_core = 1 - core
-
+
+    place = jnp.stack([core, y]).astype(jnp.int32)
     swap = [(i, i ^ 1) for i in range(n_tp)]
     y_groups = [[c + 2 * k for k in range(n_y)] for c in range(2)]
 
@@ -143,35 +189,11 @@
     gain = own_first(pre_gain, lax.ppermute(after(pre_gain, outgoing), "tp", swap), 0)
     own_rows = lax.dynamic_slice_in_dim(whole, core * half, half, 0)
 
-    e_gate, e_up, s_gate, s_up, _ = lax.optimization_barrier((expert_gate, expert_up, shared_gate, shared_up, outgoing))
-    sent_in = jnp.concatenate(
-        [
-            lax.dynamic_index_in_dim(e_gate, other_core, 0, keepdims=False),
-            lax.dynamic_index_in_dim(e_up, other_core, 0, keepdims=False),
-            s_gate,
-            s_up,
-        ],
-        axis=0,
-    )
+    sent_in = pack(after(place, outgoing), [expert_gate, expert_up, shared_gate, shared_up])
     got_in = lax.ppermute(sent_in, "tp", swap)
-    in_w = jnp.concatenate(
-        [
-            own_first(lax.dynamic_index_in_dim(e_gate, core, 0, keepdims=False), got_in[:hid], 0),
-            own_first(
-                lax.dynamic_index_in_dim(e_up, core, 0, keepdims=False), got_in[hid : 2 * hid], 0
-            ),
-        ],
-        axis=0,
-    )
-    sin_w = jnp.concatenate(
-        [own_first(s_gate, got_in[2 * hid : 3 * hid], 0), own_first(s_up, got_in[3 * hid :], 0)],
-        axis=0,
-    )
-    e_down, s_down, _ = lax.optimization_barrier((expert_down, shared_down, outgoing))
-    sent_out = jnp.concatenate(
-        [lax.dynamic_index_in_dim(e_down, other_core, 0, keepdims=False), s_down], axis=0
-    )
+    sent_out = pack(after(place, outgoing), [expert_down, shared_down])
     got_out = lax.ppermute(sent_out, "tp", swap)
+    e_down, s_down = expert_down, shared_down
     down_w = own_first(
         lax.dynamic_index_in_dim(e_down, core, 0, keepdims=False), got_out[:n_hid], 1
     ).reshape(n_y, 2 * hid, width)
@@ -200,27 +222,42 @@
                 pieces.append(bwd[k])
                 at.append((k, step))
         if step == 1:
-            square_sum = jnp.sum(to_all_y(after(square, fwd[0])), axis=0)
+            squares = to_all_y(after(square, fwd[0]))
+        if step == 3:
+            square_sum = jnp.sum(after(squares, fwd[0], bwd[0]), axis=0)
             scale = lax.rsqrt(square_sum / feat_all + EPSILON)[:, None]
 
-    where = y[None].astype(jnp.int32)
     flops = 2 * rows * feat_all * 4 * hid
-    total = call(
+    n_early = len(early)
+    total, w_last, sw_last = pl.pallas_call(
         functools.partial(early_kernel, early_at, spans, n_y, width),
-        jax.ShapeDtypeStruct((rows, 4 * hid), F32),
-        flops,
-        (where, in_w, sin_w, *early),
-        smem=1,
-    )
-    hidden = call(
-        functools.partial(late_kernel, late_at, spans, n_y, width),
-        jax.ShapeDtypeStruct((rows, 2 * hid), BF),
-        flops // n_y,
-        (where, in_w, sin_w, total, scale, *late),
-        smem=1,
-    )
-
-    hidden_all = to_all_y(hidden)
+        out_shape=(
+            jax.ShapeDtypeStruct((rows, 4 * hid), F32),
+            jax.ShapeDtypeStruct((4 * hid, width), BF),
+            jax.ShapeDtypeStruct((4 * hid, width), BF),
+        ),
+        in_specs=[SMEM] + [HBM] * (5 + n_early),
+        out_specs=(VMEM, VMEM, VMEM),
+        scratch_shapes=[
+            pltpu.VMEM((4 * hid, feat_all), BF),
+            pltpu.VMEM((4 * hid, feat_all), BF),
+            pltpu.VMEM((n_early, n_sub, width), BF),
+            pltpu.SemaphoreType.DMA((8,)),
+            pltpu.SemaphoreType.DMA((n_early,)),
+        ],
+        cost_estimate=pl.CostEstimate(flops=flops, bytes_accessed=2**23, transcendentals=0),
+        compiler_params=pltpu.CompilerParams(vmem_limit_bytes=20 * 2**20),
+    )(place, expert_gate, expert_up, shared_gate, shared_up, got_in, *early)
+    hidden = pl.pallas_call(
+        functools.partial(late_kernel, spans),
+        out_shape=jax.ShapeDtypeStruct((n_y, rows, 2 * hid), BF),
+        in_specs=[VMEM] * 6,
+        out_specs=VMEM,
+        cost_estimate=pl.CostEstimate(flops=flops // 8, bytes_accessed=2**21, transcendentals=0),
+        compiler_params=pltpu.CompilerParams(vmem_limit_bytes=12 * 2**20),
+    )(w_last, sw_last, total, scale, *late)
+
+    hidden_all = lax.all_to_all(hidden, "tp", 0, 0, axis_index_groups=y_groups, tiled=True)
     contract = (((0, 2), (0, 1)), ((), ()))
     expert_out = lax.dot_general(hidden_all[:, :slots], down_w, contract, preferred_element_type=F32).astype(BF)
     returned = lax.all_to_all(expert_out.reshape(n_ep, cap, width), "ep", 0, 0, tiled=True)

time: 191 us -> 197 us (1.031)
  local copies, waits for them, and re-layouts: 6.58 us -> 19.7 us
  blocking collectives: 10.1 us -> 23.1 us
  waiting for transfers between devices: 50.1 us -> 38.9 us
  starting transfers between devices: 100 us -> 91.8 us
  other arithmetic: 8.24 us -> 4.4 us
  matrix products: 4.44 us -> 6.64 us
    unnamed x44 -> x67, local copies, waits for them, and re-layouts: 0.56 us -> 17.3 us
    all_to_all x0 -> x1, blocking collectives: none -> 13 us  [to_all_y(): lax.all_to_all(sent, 'tp', 0, 0, axis_index_groups=y_groups, tiled=True)]
    all_to_all x2 -> x1, waiting for transfers between devices: 22.7 us -> 15.9 us  [body(): lax.all_to_all(hidden, 'tp', 0, 0, axis_index_groups=y_groups, tiled=True)]
    all_to_all x2 -> x1, starting transfers between devices: 9.15 us -> 4.41 us  [body(): lax.all_to_all(hidden, 'tp', 0, 0, axis_index_groups=y_groups, tiled=True)]
    concatenate x4 -> x0, other arithmetic: 4.65 us -> none  [the longest x1 1.56 us: body(): jnp.concatenate([own_first(lax.dynamic_index_in_dim(e_gate, core, 0, keep...]
    broadcast_in_dim x2 -> x1, local copies, waits for them, and re-layouts: 2.89 us -> 0.01 us  [to_all_y(): sent = jnp.broadcast_to(v[None], (n_y,) + v.shape)]
    all_to_all x1, waiting for transfers between devices: 8.96 us -> 6.13 us  [body(): lax.all_to_all(outgoing.reshape(n_ep, cap, width), 'ep', 0, 0, tiled=True)]
    pallas_call x2 -> x4, Pallas kernels: 9.87 us -> 10.7 us  [the longest x1 6.33 us: body(): pl.pallas_call(functools.partial(early_kernel, early_at, spans, n_y, widt...]
  transfers between devices with their start and end apart: 23 -> 22, of which waited for: 9 -> 6; matrix products, arithmetic and copies ran while one was open for 5% -> 3% of each run, Pallas kernels for 3% -> 5%
where the time goes in v1:
time: 197 us; the launch traced here: 196 us
  starting transfers between devices  91.8 us (47%)
  waiting for transfers between devices  38.9 us (20%)
  blocking collectives  23.1 us (12%)
  local copies, waits for them, and re-layouts  19.7 us (10%)
  Pallas kernels  10.7 us (5%)
  matrix products  6.64 us (3%)
  other arithmetic  4.4 us (2%)
    ppermute x7, starting transfers between devices, body(): bwd[k] = lax.ppermute(bwd[k], 'tp', y_shift(-1))  26.7 us
    unnamed x67, local copies, waits for them, and re-layouts  17.3 us
    all_to_all x1, waiting for transfers between devices, body(): lax.all_to_all(hidden, 'tp', 0, 0, axis_index_groups=y_groups, tiled=True)  15.9 us
    ppermute x7, starting transfers between devices, body(): fwd[k] = lax.ppermute(fwd[k], 'tp', y_shift(1))  15.6 us
    all_to_all x1, blocking collectives, to_all_y(): lax.all_to_all(sent, 'tp', 0, 0, axis_index_groups=y_groups, tiled=True)  13 us
    all_to_all x1, waiting for transfers between devices, body(): lax.all_to_all(expert_out.reshape(n_ep, cap, width), 'ep', 0, 0, tiled=True)  11.3 us
    all_to_all x1, blocking collectives, body(): out_square = jnp.sum(lax.all_to_all(sent, 'tp', 0, 0, tiled=True), axis=0)  10.1 us
    ppermute x1, starting transfers between devices, body(): got_out = lax.ppermute(sent_out, 'tp', swap)  9.38 us
  transfers between devices with their start and end apart: 22, of which 6 were waited for; matrix products, arithmetic and copies ran while one was open for 3% of the time, Pallas kernels for 5%

profile of v1, /device:TPU:1, one launch (start us, length us, event | category | flops | bytes accessed | tf_op | source)
XLA Modules:
  0.0 195.9 jit_solution(14195852076037491831)
XLA Ops:
  0.0 9.0 %collective-permute-start = (bf16[256,256]{1,0:T(8,128)(2,1)}, bf16[256,256]{1,0:T(8,128)(2,1)S(1)}, u32[]{:S(2)}, u32[]{:S(2)}) collective-permute-start(bf16[256,256]{1,0:T(8,128)(2,1)} %param.11), channel_id=1, source_target_pairs={{0,1},{1,0},{2,3},{3,2},{4,5},{5,4},{6,7},{7,6},{8,9},{9,8},{10,11... | collective-permute-start | bytes 393224 | tf_op jit(solution)/shard_map/ppermute | solution.py:172
  13.4 7.7 %all-to-all-start = ((bf16[32,16,512]{2,1,0:T(8,128)(2,1)}), bf16[32,16,512]{2,1,0:T(8,128)(2,1)}, u32[]{:S(2)}, u32[]{:S(2)}) async-start(bf16[32,16,512]{2,1,0:T(8,128)(2,1)} %bitcast.11), calls=%async_computation | async-start | bytes 1048576 | tf_op jit(solution)/shard_map/all_to_all | solution.py:186
  22.3 2.1 %shard_map.109 = bf16[256,4096]{1,0:T(8,128)(2,1)} custom-call(s32[2]{0:T(128)S(1)} %pad_add_fusion.at_ref, bf16[2,64,4096]{2,1,0:T(8,128)(2,1)S(1)} %copy-done, bf16[2,64,4096]{2,1,0:T(8,128)(2,1)S(1)} %copy-done.1, bf16[64,4096]{1,0:T(8,128)(2,1)S(1)} %copy-done.3, bf16[64,4096]{1,0:T(8,128)(2,1)S(1)} %copy-done.4), custom_call_target="tpu_custom_call" | custom-call | flops 400000000 | bytes 4194304 | tf_op jit(solution)/shard_map/pallas_call | solution.py:106
  24.4 2.3 %collective-permute-start.1 = (bf16[256,4096]{1,0:T(8,128)(2,1)}, bf16[256,4096]{1,0:T(8,128)(2,1)}, u32[]{:S(2)}, u32[]{:S(2)}) collective-permute-start(bf16[256,4096]{1,0:T(8,128)(2,1)} %shard_map.109), channel_id=1, source_target_pairs={{0,1},{1,0},{2,3},{3,2},{4,5},{5,4},{6,7},{7,6},{8,9},{9,8},{10,11... | collective-permute-start | bytes 6291464 | tf_op jit(solution)/shard_map/ppermute | solution.py:193
  26.7 2.1 %collective-permute-start.2 = (f32[256]{0:T(256)}, f32[256]{0:T(256)S(1)}, u32[]{:S(2)}, u32[]{:S(2)}) collective-permute-start(f32[256]{0:T(256)} %param.12), channel_id=1, source_target_pairs={{0,1},{1,0},{2,3},{3,2},{4,5},{5,4},{6,7},{7,6},{8,9},{9,8},{10,11... | collective-permute-start | bytes 3080 | tf_op jit(solution)/shard_map/ppermute | solution.py:189
  28.9 2.0 %collective-permute-done.2 = f32[256]{0:T(256)S(1)} collective-permute-done((f32[256]{0:T(256)}, f32[256]{0:T(256)S(1)}, u32[]{:S(2)}, u32[]{:S(2)}) %collective-permute-start.2) | collective-permute-done | bytes 1056 | tf_op jit(solution)/shard_map/ppermute | solution.py:189
  31.7 6.1 %all-to-all-done = bf16[32,16,512]{2,1,0:T(8,128)(2,1)} async-done(((bf16[32,16,512]{2,1,0:T(8,128)(2,1)}), bf16[32,16,512]{2,1,0:T(8,128)(2,1)}, u32[]{:S(2)}, u32[]{:S(2)}) %all-to-all-start) | async-done | bytes 524320 | tf_op jit(solution)/shard_map/all_to_all | solution.py:186
  39.2 3.2 %collective-permute-start.3 = (bf16[320,512]{1,0:T(8,128)(2,1)S(1)}, bf16[320,512]{1,0:T(8,128)(2,1)S(1)}, u32[]{:S(2)}, u32[]{:S(2)}) collective-permute-start(bf16[320,512]{1,0:T(8,128)(2,1)S(1)} %get-tuple-element.26.refs_0_), channel_id=1, source_target_pairs={{0,2},{1,3},{2,4},{3,5},{4,6},{5,7},{6,8},{7,9},{8,10},{9,11},{10,... | collective-permute-start | bytes 983048 | tf_op jit(solution)/shard_map/ppermute | solution.py:217
  42.4 3.8 %collective-permute-start.4 = (bf16[320,512]{1,0:T(8,128)(2,1)S(1)}, bf16[320,512]{1,0:T(8,128)(2,1)S(1)}, u32[]{:S(2)}, u32[]{:S(2)}) collective-permute-start(bf16[320,512]{1,0:T(8,128)(2,1)S(1)} %get-tuple-element.26.refs_0_), channel_id=1, source_target_pairs={{0,14},{1,15},{2,0},{3,1},{4,2},{5,3},{6,4},{7,5},{8,6},{9,7},{10,... | collective-permute-start | bytes 983048 | tf_op jit(solution)/shard_map/ppermute | solution.py:221
  46.9 3.4 %collective-permute-start.6 = (bf16[320,512]{1,0:T(8,128)(2,1)S(1)}, bf16[320,512]{1,0:T(8,128)(2,1)S(1)}, u32[]{:S(2)}, u32[]{:S(2)}) collective-permute-start(bf16[320,512]{1,0:T(8,128)(2,1)S(1)} %get-tuple-element.25.refs_1_), channel_id=1, source_target_pairs={{0,14},{1,15},{2,0},{3,1},{4,2},{5,3},{6,4},{7,5},{8,6},{9,7},{10,... | collective-permute-start | bytes 983048 | tf_op jit(solution)/shard_map/ppermute | solution.py:221
  50.3 1.9 collective-permute-start.5
  52.2 1.9 collective-permute-start.7
  54.9 4.6 %collective-permute-start.8 = (bf16[320,512]{1,0:T(8,128)(2,1)S(1)}, bf16[320,512]{1,0:T(8,128)(2,1)S(1)}, u32[]{:S(2)}, u32[]{:S(2)}) collective-permute-start(bf16[320,512]{1,0:T(8,128)(2,1)S(1)} %collective-permute-done.4.refs_3_), channel_id=1, source_target_pairs={{0,14},{1,15},{2,0},{3,1},{4,2},{5,3},{6,4},{7,5},{8,6},{9,7},{10,... | collective-permute-start | bytes 983048 | tf_op jit(solution)/shard_map/ppermute | solution.py:221
  60.2 3.4 %collective-permute-start.10 = (bf16[320,512]{1,0:T(8,128)(2,1)S(1)}, bf16[320,512]{1,0:T(8,128)(2,1)}, u32[]{:S(2)}, u32[]{:S(2)}) collective-permute-start(bf16[320,512]{1,0:T(8,128)(2,1)S(1)} %collective-permute-done.6.refs_5_), channel_id=1, source_target_pairs={{0,14},{1,15},{2,0},{3,1},{4,2},{5,3},{6,4},{7,5},{8,6},{9,7},{10,... | collective-permute-start | bytes 983048 | tf_op jit(solution)/shard_map/ppermute | solution.py:221
  64.3 1.9 collective-permute-start.9
  66.9 2.4 %collective-permute-start.11 = (bf16[320,512]{1,0:T(8,128)(2,1)S(1)}, bf16[320,512]{1,0:T(8,128)(2,1)S(1)}, u32[]{:S(2)}, u32[]{:S(2)}) collective-permute-start(bf16[320,512]{1,0:T(8,128)(2,1)S(1)} %collective-permute-done.7.refs_6_), channel_id=1, source_target_pairs={{0,2},{1,3},{2,4},{3,5},{4,6},{5,7},{6,8},{7,9},{8,10},{9,11},{10,... | collective-permute-start | bytes 983048 | tf_op jit(solution)/shard_map/ppermute | solution.py:217
  70.1 4.1 %collective-permute-start.12 = (bf16[320,512]{1,0:T(8,128)(2,1)S(1)}, bf16[320,512]{1,0:T(8,128)(2,1)S(1)}, u32[]{:S(2)}, u32[]{:S(2)}) collective-permute-start(bf16[320,512]{1,0:T(8,128)(2,1)S(1)} %collective-permute-done.8.refs_7_), channel_id=1, source_target_pairs={{0,14},{1,15},{2,0},{3,1},{4,2},{5,3},{6,4},{7,5},{8,6},{9,7},{10,... | collective-permute-start | bytes 983048 | tf_op jit(solution)/shard_map/ppermute | solution.py:221
  74.9 3.4 %collective-permute-start.14 = (bf16[320,512]{1,0:T(8,128)(2,1)}, bf16[320,512]{1,0:T(8,128)(2,1)}, u32[]{:S(2)}, u32[]{:S(2)}) collective-permute-start(bf16[320,512]{1,0:T(8,128)(2,1)} %collective-permute-done.10.refs_9_), channel_id=1, source_target_pairs={{0,14},{1,15},{2,0},{3,1},{4,2},{5,3},{6,4},{7,5},{8,6},{9,7},{10,... | collective-permute-start | bytes 983048 | tf_op jit(solution)/shard_map/ppermute | solution.py:221
  78.3 1.9 collective-permute-start.13
  80.2 13.0 %all_to_all.30 = f32[8,1,640]{2,1,0:T(1,128)S(1)} all-to-all(f32[8,1,640]{2,1,0:T(1,128)S(1)} %broadcast_in_dim.79), channel_id=1, replica_groups={{0,2,4,6,8,10,12,14},{1,3,5,7,9,11,13,15},{16,18,20,22,24,26,28,30},{17..., dimensions={0} | all-to-all | bytes 40960 | tf_op jit(solution)/shard_map/all_to_all | solution.py:170
  94.7 2.3 %collective-permute-start.15 = (bf16[320,512]{1,0:T(8,128)(2,1)}, bf16[320,512]{1,0:T(8,128)(2,1)S(1)}, u32[]{:S(2)}, u32[]{:S(2)}) collective-permute-start(bf16[320,512]{1,0:T(8,128)(2,1)} %copy-done.21), channel_id=1, source_target_pairs={{0,2},{1,3},{2,4},{3,5},{4,6},{5,7},{6,8},{7,9},{8,10},{9,11},{10,... | collective-permute-start | bytes 983048 | tf_op jit(solution)/shard_map/ppermute | solution.py:217
  97.0 4.2 %collective-permute-start.16 = (bf16[320,512]{1,0:T(8,128)(2,1)}, bf16[320,512]{1,0:T(8,128)(2,1)S(1)}, u32[]{:S(2)}, u32[]{:S(2)}) collective-permute-start(bf16[320,512]{1,0:T(8,128)(2,1)} %collective-permute-done.14.refs_13_), channel_id=1, source_target_pairs={{0,14},{1,15},{2,0},{3,1},{4,2},{5,3},{6,4},{7,5},{8,6},{9,7},{10,... | collective-permute-start | bytes 983048 | tf_op jit(solution)/shard_map/ppermute | solution.py:221
  110.2 6.3 %shard_map.110 = (f32[640,256]{1,0:T(8,128)S(1)}, bf16[256,512]{1,0:T(8,128)(2,1)S(1)}, bf16[256,512]{1,0:T(8,128)(2,1)S(1)}) custom-call(s32[2]{0:T(128)S(1)} %pad_add_fusion.at_ref, bf16[2,64,4096]{2,1,0:T(8,128)(2,1)S(1)} %copy-done, bf16[2,64,4096]{2,1,0:T(8,128)(2,1)S(1)} %copy-done.1, bf16[64,4096]{1,0:T(8,128)(2,1)S(1)} %copy-done.3, ...), custom_call_target="tpu_custom_call" | custom-call | flops 1342177280 | bytes 8388608 | tf_op jit(solution)/shard_map/pallas_call | solution.py:232
  118.0 4.4 %all-to-all-start.2 = ((bf16[8,640,128]{2,1,0:T(8,128)(2,1)}), bf16[8,640,128]{2,1,0:T(8,128)(2,1)}, u32[]{:S(2)}, u32[]{:S(2)}) async-start(bf16[8,640,128]{2,1,0:T(8,128)(2,1)} %shard_map.111), calls=%async_computation.2 | async-start | bytes 2621440 | tf_op jit(solution)/shard_map/all_to_all | solution.py:260
  123.2 9.4 %collective-permute-start.17 = (bf16[2048,256]{1,0:T(8,128)(2,1)S(1)}, bf16[2048,256]{1,0:T(8,128)(2,1)}, u32[]{:S(2)}, u32[]{:S(2)}) collective-permute-start(bf16[2048,256]{1,0:T(8,128)(2,1)S(1)} %shard_map.112), channel_id=1, source_target_pairs={{0,1},{1,0},{2,3},{3,2},{4,5},{5,4},{6,7},{7,6},{8,9},{9,8},{10,11... | collective-permute-start | bytes 3145736 | tf_op jit(solution)/shard_map/ppermute | solution.py:195
  132.7 2.3 %collective-permute-done.17 = bf16[2048,256]{1,0:T(8,128)(2,1)} collective-permute-done((bf16[2048,256]{1,0:T(8,128)(2,1)S(1)}, bf16[2048,256]{1,0:T(8,128)(2,1)}, u32[]{:S(2)}, u32[]{:S(2)}) %collective-permute-start.17) | collective-permute-done | bytes 1048608 | tf_op jit(solution)/shard_map/ppermute | solution.py:195
  136.3 15.9 %all-to-all-done.2 = bf16[8,640,128]{2,1,0:T(8,128)(2,1)} async-done(((bf16[8,640,128]{2,1,0:T(8,128)(2,1)}), bf16[8,640,128]{2,1,0:T(8,128)(2,1)}, u32[]{:S(2)}, u32[]{:S(2)}) %all-to-all-start.2) | async-done | bytes 1310752 | tf_op jit(solution)/shard_map/all_to_all | solution.py:260
  152.1 2.8 %fusion.2 = bf16[512,512]{1,0:T(8,128)(2,1)} fusion(bf16[8,640,128]{2,1,0:T(8,128)(2,1)} %all-to-all-done.2, bf16[8,128,256]{2,1,0:T(8,128)(2,1)S(1)} %bitcast.48, bf16[8,128,256]{2,1,0:T(8,128)(2,1)S(1)} %bitcast.46, pred[]{:T(512)S(6)} %eq.84), kind=kOutput, calls=%fused_computation.5 | convolution fusion | flops 541851648 | bytes 2621441 | tf_op jit(solution)/shard_map/dot_general | solution.py:262
  154.9 6.1 %all-to-all-start.3 = ((bf16[32,16,512]{2,1,0:T(8,128)(2,1)}), bf16[32,16,512]{2,1,0:T(8,128)(2,1)S(1)}, u32[]{:S(2)}, u32[]{:S(2)}) async-start(bf16[32,16,512]{2,1,0:T(8,128)(2,1)} %bitcast.16), calls=%async_computation.3 | async-start | bytes 1048576 | tf_op jit(solution)/shard_map/all_to_all | solution.py:263
  162.4 11.3 %all-to-all-done.3 = bf16[32,16,512]{2,1,0:T(8,128)(2,1)S(1)} async-done(((bf16[32,16,512]{2,1,0:T(8,128)(2,1)}), bf16[32,16,512]{2,1,0:T(8,128)(2,1)S(1)}, u32[]{:S(2)}, u32[]{:S(2)}) %all-to-all-start.3) | async-done | bytes 524320 | tf_op jit(solution)/shard_map/all_to_all | solution.py:263
  175.1 8.6 %collective-permute-start.18 = (f32[256,256]{1,0:T(8,128)S(1)}, f32[256,256]{1,0:T(8,128)S(1)}, u32[]{:S(2)}, u32[]{:S(2)}) collective-permute-start(f32[256,256]{1,0:T(8,128)S(1)} %slice_select_fusion), channel_id=1, source_target_pairs={{0,1},{1,0},{2,3},{3,2},{4,5},{5,4},{6,7},{7,6},{8,9},{9,8},{10,11... | collective-permute-start | bytes 786440 | tf_op jit(solution)/shard_map/ppermute | solution.py:284
  184.9 10.1 %all_to_all.31 = f32[16,1,256]{2,1,0:T(1,128)S(1)} all-to-all(f32[16,1,256]{2,1,0:T(1,128)S(1)} %broadcast_in_dim.80), channel_id=1, replica_groups=mesh['ep'=32,'tp'=16] {'tp'}, dimensions={0} | all-to-all | bytes 32768 | tf_op jit(solution)/shard_map/all_to_all | solution.py:287
  (118 shorter events, 31.5 us)
Async XLA Ops:
  0.0 21.2 %copy-start = (bf16[2,64,4096]{2,1,0:T(8,128)(2,1)S(1)}, bf16[2,64,4096]{2,1,0:T(8,128)(2,1)}, u32[]{:S(2)}) copy-start(bf16[2,64,4096]{2,1,0:T(8,128)(2,1)} %gate.1) | copy-start | bytes 3145732
  0.0 21.2 %copy-start.1 = (bf16[2,64,4096]{2,1,0:T(8,128)(2,1)S(1)}, bf16[2,64,4096]{2,1,0:T(8,128)(2,1)}, u32[]{:S(2)}) copy-start(bf16[2,64,4096]{2,1,0:T(8,128)(2,1)} %up.1) | copy-start | bytes 3145732
  0.0 21.2 %copy-start.3 = (bf16[64,4096]{1,0:T(8,128)(2,1)S(1)}, bf16[64,4096]{1,0:T(8,128)(2,1)}, u32[]{:S(2)}) copy-start(bf16[64,4096]{1,0:T(8,128)(2,1)} %s_gate.1) | copy-start | bytes 1572868
  0.0 11.2 %collective-permute-start = (bf16[256,256]{1,0:T(8,128)(2,1)}, bf16[256,256]{1,0:T(8,128)(2,1)S(1)}, u32[]{:S(2)}, u32[]{:S(2)}) collective-permute-start(bf16[256,256]{1,0:T(8,128)(2,1)} %param.11), channel_id=1, source_target_pairs={{0,1},{1,0},{2,3},{3,2},{4,5},{5,4},{6,7},{7,6},{8,9},{9,8},{10,11... | collective-permute-start | bytes 393224 | tf_op jit(solution)/shard_map/ppermute | solution.py:172
  9.1 12.1 %copy-start.29 = (s32[32]{0:T(128)}, s32[32]{0:T(128)S(1)}, u32[]{:S(2)}) copy-start(s32[32]{0:T(128)S(1)} %multiply_add_fusion) | copy-start | bytes 388
  13.4 24.4 %all-to-all-start = ((bf16[32,16,512]{2,1,0:T(8,128)(2,1)}), bf16[32,16,512]{2,1,0:T(8,128)(2,1)}, u32[]{:S(2)}, u32[]{:S(2)}) async-start(bf16[32,16,512]{2,1,0:T(8,128)(2,1)} %bitcast.11), calls=%async_computation | async-start | bytes 1048576 | tf_op jit(solution)/shard_map/all_to_all | solution.py:186
  24.4 77.0 %copy-start.5 = (bf16[64,4096]{1,0:T(8,128)(2,1)S(1)}, bf16[64,4096]{1,0:T(8,128)(2,1)}, u32[]{:S(2)}) copy-start(bf16[64,4096]{1,0:T(8,128)(2,1)} %s_up.1) | copy-start | bytes 1572868
  24.4 77.0 %collective-permute-start.1 = (bf16[256,4096]{1,0:T(8,128)(2,1)}, bf16[256,4096]{1,0:T(8,128)(2,1)}, u32[]{:S(2)}, u32[]{:S(2)}) collective-permute-start(bf16[256,4096]{1,0:T(8,128)(2,1)} %shard_map.109), channel_id=1, source_target_pairs={{0,1},{1,0},{2,3},{3,2},{4,5},{5,4},{6,7},{7,6},{8,9},{9,8},{10,11... | collective-permute-start | bytes 6291464 | tf_op jit(solution)/shard_map/ppermute | solution.py:193
  26.7 4.2 %collective-permute-start.2 = (f32[256]{0:T(256)}, f32[256]{0:T(256)S(1)}, u32[]{:S(2)}, u32[]{:S(2)}) collective-permute-start(f32[256]{0:T(256)} %param.12), channel_id=1, source_target_pairs={{0,1},{1,0},{2,3},{3,2},{4,5},{5,4},{6,7},{7,6},{8,9},{9,8},{10,11... | collective-permute-start | bytes 3080 | tf_op jit(solution)/shard_map/ppermute | solution.py:189
  39.2 13.1 %collective-permute-start.3 = (bf16[320,512]{1,0:T(8,128)(2,1)S(1)}, bf16[320,512]{1,0:T(8,128)(2,1)S(1)}, u32[]{:S(2)}, u32[]{:S(2)}) collective-permute-start(bf16[320,512]{1,0:T(8,128)(2,1)S(1)} %get-tuple-element.26.refs_0_), channel_id=1, source_target_pairs={{0,2},{1,3},{2,4},{3,5},{4,6},{5,7},{6,8},{7,9},{8,10},{9,11},{10,... | collective-permute-start | bytes 983048 | tf_op jit(solution)/shard_map/ppermute | solution.py:217
  42.4 12.5 %collective-permute-start.4 = (bf16[320,512]{1,0:T(8,128)(2,1)S(1)}, bf16[320,512]{1,0:T(8,128)(2,1)S(1)}, u32[]{:S(2)}, u32[]{:S(2)}) collective-permute-start(bf16[320,512]{1,0:T(8,128)(2,1)S(1)} %get-tuple-element.26.refs_0_), channel_id=1, source_target_pairs={{0,14},{1,15},{2,0},{3,1},{4,2},{5,3},{6,4},{7,5},{8,6},{9,7},{10,... | collective-permute-start | bytes 983048 | tf_op jit(solution)/shard_map/ppermute | solution.py:221
  46.9 13.3 %collective-permute-start.6 = (bf16[320,512]{1,0:T(8,128)(2,1)S(1)}, bf16[320,512]{1,0:T(8,128)(2,1)S(1)}, u32[]{:S(2)}, u32[]{:S(2)}) collective-permute-start(bf16[320,512]{1,0:T(8,128)(2,1)S(1)} %get-tuple-element.25.refs_1_), channel_id=1, source_target_pairs={{0,14},{1,15},{2,0},{3,1},{4,2},{5,3},{6,4},{7,5},{8,6},{9,7},{10,... | collective-permute-start | bytes 983048 | tf_op jit(solution)/shard_map/ppermute | solution.py:221
  50.3 14.0 %collective-permute-start.5 = (bf16[320,512]{1,0:T(8,128)(2,1)S(1)}, bf16[320,512]{1,0:T(8,128)(2,1)S(1)}, u32[]{:S(2)}, u32[]{:S(2)}) collective-permute-start(bf16[320,512]{1,0:T(8,128)(2,1)S(1)} %get-tuple-element.25.refs_1_), channel_id=1, source_target_pairs={{0,2},{1,3},{2,4},{3,5},{4,6},{5,7},{6,8},{7,9},{8,10},{9,11},{10,... | collective-permute-start | bytes 983048 | tf_op jit(solution)/shard_map/ppermute | solution.py:217
  52.2 14.7 %collective-permute-start.7 = (bf16[320,512]{1,0:T(8,128)(2,1)S(1)}, bf16[320,512]{1,0:T(8,128)(2,1)S(1)}, u32[]{:S(2)}, u32[]{:S(2)}) collective-permute-start(bf16[320,512]{1,0:T(8,128)(2,1)S(1)} %collective-permute-done.3.refs_2_), channel_id=1, source_target_pairs={{0,2},{1,3},{2,4},{3,5},{4,6},{5,7},{6,8},{7,9},{8,10},{9,11},{10,... | collective-permute-start | bytes 983048 | tf_op jit(solution)/shard_map/ppermute | solution.py:217
  54.9 15.2 %collective-permute-start.8 = (bf16[320,512]{1,0:T(8,128)(2,1)S(1)}, bf16[320,512]{1,0:T(8,128)(2,1)S(1)}, u32[]{:S(2)}, u32[]{:S(2)}) collective-permute-start(bf16[320,512]{1,0:T(8,128)(2,1)S(1)} %collective-permute-done.4.refs_3_), channel_id=1, source_target_pairs={{0,14},{1,15},{2,0},{3,1},{4,2},{5,3},{6,4},{7,5},{8,6},{9,7},{10,... | collective-permute-start | bytes 983048 | tf_op jit(solution)/shard_map/ppermute | solution.py:221
  60.2 14.7 %collective-permute-start.10 = (bf16[320,512]{1,0:T(8,128)(2,1)S(1)}, bf16[320,512]{1,0:T(8,128)(2,1)}, u32[]{:S(2)}, u32[]{:S(2)}) collective-permute-start(bf16[320,512]{1,0:T(8,128)(2,1)S(1)} %collective-permute-done.6.refs_5_), channel_id=1, source_target_pairs={{0,14},{1,15},{2,0},{3,1},{4,2},{5,3},{6,4},{7,5},{8,6},{9,7},{10,... | collective-permute-start | bytes 983048 | tf_op jit(solution)/shard_map/ppermute | solution.py:221
  64.3 14.0 %collective-permute-start.9 = (bf16[320,512]{1,0:T(8,128)(2,1)S(1)}, bf16[320,512]{1,0:T(8,128)(2,1)}, u32[]{:S(2)}, u32[]{:S(2)}) collective-permute-start(bf16[320,512]{1,0:T(8,128)(2,1)S(1)} %collective-permute-done.5.refs_4_), channel_id=1, source_target_pairs={{0,2},{1,3},{2,4},{3,5},{4,6},{5,7},{6,8},{7,9},{8,10},{9,11},{10,... | collective-permute-start | bytes 983048 | tf_op jit(solution)/shard_map/ppermute | solution.py:217
  66.9 26.3 %collective-permute-start.11 = (bf16[320,512]{1,0:T(8,128)(2,1)S(1)}, bf16[320,512]{1,0:T(8,128)(2,1)S(1)}, u32[]{:S(2)}, u32[]{:S(2)}) collective-permute-start(bf16[320,512]{1,0:T(8,128)(2,1)S(1)} %collective-permute-done.7.refs_6_), channel_id=1, source_target_pairs={{0,2},{1,3},{2,4},{3,5},{4,6},{5,7},{6,8},{7,9},{8,10},{9,11},{10,... | collective-permute-start | bytes 983048 | tf_op jit(solution)/shard_map/ppermute | solution.py:217
  70.1 23.1 %collective-permute-start.12 = (bf16[320,512]{1,0:T(8,128)(2,1)S(1)}, bf16[320,512]{1,0:T(8,128)(2,1)S(1)}, u32[]{:S(2)}, u32[]{:S(2)}) collective-permute-start(bf16[320,512]{1,0:T(8,128)(2,1)S(1)} %collective-permute-done.8.refs_7_), channel_id=1, source_target_pairs={{0,14},{1,15},{2,0},{3,1},{4,2},{5,3},{6,4},{7,5},{8,6},{9,7},{10,... | collective-permute-start | bytes 983048 | tf_op jit(solution)/shard_map/ppermute | solution.py:221
  74.9 22.1 %collective-permute-start.14 = (bf16[320,512]{1,0:T(8,128)(2,1)}, bf16[320,512]{1,0:T(8,128)(2,1)}, u32[]{:S(2)}, u32[]{:S(2)}) collective-permute-start(bf16[320,512]{1,0:T(8,128)(2,1)} %collective-permute-done.10.refs_9_), channel_id=1, source_target_pairs={{0,14},{1,15},{2,0},{3,1},{4,2},{5,3},{6,4},{7,5},{8,6},{9,7},{10,... | collective-permute-start | bytes 983048 | tf_op jit(solution)/shard_map/ppermute | solution.py:221
  78.3 23.1 %collective-permute-start.13 = (bf16[320,512]{1,0:T(8,128)(2,1)}, bf16[320,512]{1,0:T(8,128)(2,1)}, u32[]{:S(2)}, u32[]{:S(2)}) collective-permute-start(bf16[320,512]{1,0:T(8,128)(2,1)} %collective-permute-done.9.refs_8_), channel_id=1, source_target_pairs={{0,2},{1,3},{2,4},{3,5},{4,6},{5,7},{6,8},{7,9},{8,10},{9,11},{10,... | collective-permute-start | bytes 983048 | tf_op jit(solution)/shard_map/ppermute | solution.py:217
  94.7 21.8 %collective-permute-start.15 = (bf16[320,512]{1,0:T(8,128)(2,1)}, bf16[320,512]{1,0:T(8,128)(2,1)S(1)}, u32[]{:S(2)}, u32[]{:S(2)}) collective-permute-start(bf16[320,512]{1,0:T(8,128)(2,1)} %copy-done.21), channel_id=1, source_target_pairs={{0,2},{1,3},{2,4},{3,5},{4,6},{5,7},{6,8},{7,9},{8,10},{9,11},{10,... | collective-permute-start | bytes 983048 | tf_op jit(solution)/shard_map/ppermute | solution.py:217
  97.0 19.5 %collective-permute-start.16 = (bf16[320,512]{1,0:T(8,128)(2,1)}, bf16[320,512]{1,0:T(8,128)(2,1)S(1)}, u32[]{:S(2)}, u32[]{:S(2)}) collective-permute-start(bf16[320,512]{1,0:T(8,128)(2,1)} %collective-permute-done.14.refs_13_), channel_id=1, source_target_pairs={{0,14},{1,15},{2,0},{3,1},{4,2},{5,3},{6,4},{7,5},{8,6},{9,7},{10,... | collective-permute-start | bytes 983048 | tf_op jit(solution)/shard_map/ppermute | solution.py:221
  118.0 34.1 %all-to-all-start.2 = ((bf16[8,640,128]{2,1,0:T(8,128)(2,1)}), bf16[8,640,128]{2,1,0:T(8,128)(2,1)}, u32[]{:S(2)}, u32[]{:S(2)}) async-start(bf16[8,640,128]{2,1,0:T(8,128)(2,1)} %shard_map.111), calls=%async_computation.2 | async-start | bytes 2621440 | tf_op jit(solution)/shard_map/all_to_all | solution.py:260
  123.2 11.8 %collective-permute-start.17 = (bf16[2048,256]{1,0:T(8,128)(2,1)S(1)}, bf16[2048,256]{1,0:T(8,128)(2,1)}, u32[]{:S(2)}, u32[]{:S(2)}) collective-permute-start(bf16[2048,256]{1,0:T(8,128)(2,1)S(1)} %shard_map.112), channel_id=1, source_target_pairs={{0,1},{1,0},{2,3},{3,2},{4,5},{5,4},{6,7},{7,6},{8,9},{9,8},{10,11... | collective-permute-start | bytes 3145736 | tf_op jit(solution)/shard_map/ppermute | solution.py:195
  152.1 8.8 %copy-start.27 = (f32[256,3]{0,1:T(4,128)S(1)}, f32[256,3]{0,1:T(4,128)}, u32[]{:S(2)}) copy-start(f32[256,3]{0,1:T(4,128)} %param.14) | copy-start | bytes 9220
  152.1 8.9 %copy-start.30 = (s32[32]{0:T(128)S(1)}, s32[32]{0:T(128)}, u32[]{:S(2)}) copy-start(s32[32]{0:T(128)} %copy-done.29) | copy-start | bytes 388
  154.9 18.9 %all-to-all-start.3 = ((bf16[32,16,512]{2,1,0:T(8,128)(2,1)}), bf16[32,16,512]{2,1,0:T(8,128)(2,1)S(1)}, u32[]{:S(2)}, u32[]{:S(2)}) async-start(bf16[32,16,512]{2,1,0:T(8,128)(2,1)} %bitcast.16), calls=%async_computation.3 | async-start | bytes 1048576 | tf_op jit(solution)/shard_map/all_to_all | solution.py:263
  161.1 12.7 %copy-start.26 = (f32[32,256]{1,0:T(8,128)S(1)}, f32[32,256]{1,0:T(8,128)}, u32[]{:S(2)}) copy-start(f32[32,256]{1,0:T(8,128)} %copy-done.25) | copy-start | bytes 98308
  161.1 12.6 %copy-start.32 = (f32[16]{0:T(128)S(1)}, f32[16]{0:T(128)}, u32[]{:S(2)}) copy-start(f32[16]{0:T(128)} %copy-done.31) | copy-start | bytes 196
  174.6 20.5 %copy-start.28 = (f32[256]{0:T(256)S(1)}, f32[256]{0:T(256)}, u32[]{:S(2)}) copy-start(f32[256]{0:T(256)} %param.21) | copy-start | bytes 3076
  175.1 9.7 %collective-permute-start.18 = (f32[256,256]{1,0:T(8,128)S(1)}, f32[256,256]{1,0:T(8,128)S(1)}, u32[]{:S(2)}, u32[]{:S(2)}) collective-permute-start(f32[256,256]{1,0:T(8,128)S(1)} %slice_select_fusion), channel_id=1, source_target_pairs={{0,1},{1,0},{2,3},{3,2},{4,5},{5,4},{6,7},{7,6},{8,9},{9,8},{10,11... | collective-permute-start | bytes 786440 | tf_op jit(solution)/shard_map/ppermute | solution.py:284
  (23 other events, 26.4 us)

commit v2 on v1

--- a/solution.py
+++ b/solution.py
@@ -18,24 +18,24 @@
 HBM = pl.BlockSpec(memory_space=pltpu.HBM)
 
 
-def after(x, *first):
-    return lax.optimization_barrier((x,) + first)[0]
-
-
 def times(x, w):
     return lax.dot_general(x, w, (((1,), (1,)), ((), ())), preferred_element_type=F32)
 
 
-def early_kernel(places, spans, n_y, width, at_ref, gate, up, s_gate, s_up, got, *refs):
-    n = len(places)
-    pieces = refs[:n]
-    total_ref, w_last, sw_last = refs[n : n + 3]
-    w, sw, held, w_sem, sem = refs[n + 3 :]
+def early_kernel(places, n_y, width, at_ref, gate, up, s_gate, s_up, got, *refs):
+    n, ns = len(places), n_y
+    pieces, shared = refs[:n], refs[n : n + ns]
+    total_ref, s_total_ref, w_last = refs[n + ns : n + ns + 3]
+    w, sw, held, s_held, w_sem, sem, s_sem = refs[n + ns + 3 :]
     core, y = at_ref[0], at_ref[1]
     hid = s_gate.shape[0]
     n_sub = total_ref.shape[0] // 2
     own = pl.multiple_of(core * hid, hid)
     other = pl.multiple_of((1 - core) * hid, hid)
+
+    def columns(offset):
+        return pl.ds(pl.multiple_of(lax.rem(y + offset + n_y, n_y) * width, width), width)
+
     moves = []
     for i, (mine, into, base) in enumerate(
         ((gate.at[core], w, 0), (up.at[core], w, 2 * hid), (s_gate, sw, 0), (s_up, sw, 2 * hid))
@@ -43,38 +43,50 @@
         moves.append(pltpu.make_async_copy(mine, into.at[pl.ds(base + own, hid)], w_sem.at[2 * i]))
         theirs = got.at[pl.ds(i * hid, hid)]
         moves.append(pltpu.make_async_copy(theirs, into.at[pl.ds(base + other, hid)], w_sem.at[2 * i + 1]))
-    loads = [pltpu.make_async_copy(p, held.at[i], sem.at[i]) for i, p in enumerate(pieces)]
-    for copy in moves + loads:
+    loads = [
+        pltpu.make_async_copy(p, held.at[pl.ds(k * n_sub, n_sub), columns(offset)], sem.at[i])
+        for i, (p, (k, offset)) in enumerate(zip(pieces, places))
+    ]
+    s_loads = [
+        pltpu.make_async_copy(p, s_held.at[:, columns(offset)], s_sem.at[i])
+        for i, (p, offset) in enumerate(zip(shared, shared_offsets(n_y)))
+    ]
+    for copy in moves[:4] + loads + moves[4:] + s_loads:
         copy.start()
-    for copy in moves:
+    held[:, columns(n_y // 2)] = jnp.zeros((2 * n_sub, width), BF)
+    for copy in moves[:4] + loads:
         copy.wait()
+    total_ref[...] = times(held[...], w[...])
+    w_last[...] = w[:, columns(n_y // 2)]
+    for copy in moves[4:] + s_loads:
+        copy.wait()
+    s_total_ref[...] = times(s_held[...], sw[...])
+
+
+def shared_offsets(n_y):
+    steps = range(1, n_y // 2 + 1)
+    return [0] + [o for s in steps for o in ((-s, s) if s < n_y // 2 else (-s,))]
+
+
+def late_kernel(w_ref, total_ref, s_total_ref, scale_ref, *refs):
+    out_ref = refs[-1]
+    n = total_ref.shape[0]
+    n_sub = n // 2
     for half in range(2):
-        total = [None] * len(spans[half])
-        for i, (k, offset) in enumerate(places):
-            if k != half:
-                continue
-            loads[i].wait()
-            at = pl.multiple_of(lax.rem(y + offset + n_y, n_y) * width, width)
-            for j, (low, high, which) in enumerate(spans[half]):
-                term = times(held[i, low:high, :], (w, sw)[which][:, pl.ds(at, width)])
-                total[j] = term if total[j] is None else total[j] + term
-        for (low, high, _), value in zip(spans[half], total):
-            total_ref[half * n_sub + low : half * n_sub + high, :] = value
-    at = pl.multiple_of(lax.rem(y + n_y // 2, n_y) * width, width)
-    w_last[...] = w[:, pl.ds(at, width)]
-    sw_last[...] = sw[:, pl.ds(at, width)]
-
-
-def late_kernel(spans, w_ref, sw_ref, total_ref, scale_ref, *refs):
-    out_ref = refs[-1]
-    n_sub = total_ref.shape[0] // 2
-    for half in range(2):
-        for low, high, which in spans[half]:
-            rows = slice(half * n_sub + low, half * n_sub + high)
-            total = total_ref[rows, :] + times(refs[half][low:high, :], (w_ref, sw_ref)[which][...])
-            hidden = activated(total * scale_ref[rows, :])
-            for j in range(out_ref.shape[0]):
-                out_ref[j, rows, :] = hidden
+        rows = slice(half * n_sub, (half + 1) * n_sub)
+        total = total_ref[rows, :] + times(refs[half][...], w_ref[...])
+        hidden = activated(total * scale_ref[rows, :])
+        for j in range(out_ref.shape[0]):
+            out_ref[j, rows, :] = hidden
+    hidden = activated(s_total_ref[...] * scale_ref[n:, :])
+    for j in range(out_ref.shape[0]):
+        out_ref[j, n:, :] = hidden
+
+
+def activated(total):
+    n = total.shape[1] // 2
+    gate, up = total[:, :n], total[:, n:]
+    return (gate / (1.0 + jnp.exp(-gate)) * up).astype(BF)
 
 
 def pack_kernel(at_ref, *refs):
@@ -112,12 +124,6 @@
         cost_estimate=pl.CostEstimate(flops=4 * 10**8, bytes_accessed=2**22, transcendentals=0),
         compiler_params=pltpu.CompilerParams(vmem_limit_bytes=4 * 2**20),
     )(at, *arrays)
-
-
-def activated(total):
-    n = total.shape[1] // 2
-    gate, up = total[:, :n], total[:, n:]
-    return (gate / (1.0 + jnp.exp(-gate)) * up).astype(BF)
 
 
 def body(
@@ -169,7 +175,13 @@
         sent = jnp.broadcast_to(v[None], (n_y,) + v.shape)
         return lax.all_to_all(sent, "tp", 0, 0, axis_index_groups=y_groups, tiled=True)
 
-    whole = own_first(tokens, lax.ppermute(tokens, "tp", swap), 1)
+    g_high = lax.reduce_precision(pre_gain, 8, 7)
+    g_middle = lax.reduce_precision(pre_gain - g_high, 8, 7)
+    g_rows = jnp.stack([g_high, g_middle, pre_gain - g_high - g_middle] + [jnp.zeros_like(g_high)] * 13)
+    partner = lax.ppermute(jnp.concatenate([tokens, g_rows.astype(BF)], axis=0), "tp", swap)
+    whole = own_first(tokens, partner[:tok], 1)
+    partner_gain = jnp.sum(partner[tok : tok + 3].astype(F32), axis=0)
+    gain = own_first(pre_gain, partner_gain, 0)
     ids = expert_ids.T
     named = 2 * jnp.arange(n_ep, dtype=jnp.int32)[:, None] + core
     hit = [(ids[k][None, :] == named) for k in range(top)]
@@ -186,12 +198,23 @@
     arrived = lax.all_to_all(outgoing.reshape(n_ep, cap, width), "ep", 0, 0, tiled=True)
     arrived = arrived.reshape(slots, width)
 
-    gain = own_first(pre_gain, lax.ppermute(after(pre_gain, outgoing), "tp", swap), 0)
     own_rows = lax.dynamic_slice_in_dim(whole, core * half, half, 0)
-
-    sent_in = pack(after(place, outgoing), [expert_gate, expert_up, shared_gate, shared_up])
-    got_in = lax.ppermute(sent_in, "tp", swap)
-    sent_out = pack(after(place, outgoing), [expert_down, shared_down])
+    shared = [(own_rows.astype(F32) * gain).astype(BF)]
+    s_fwd = s_bwd = shared[0]
+
+    def shared_step(step):
+        f, b = s_fwd, s_bwd
+        f = lax.ppermute(f, "tp", y_shift(1))
+        shared.append(f)
+        if step < n_y // 2:
+            b = lax.ppermute(b, "tp", y_shift(-1))
+            shared.append(b)
+        return f, b
+
+    s_fwd, s_bwd = shared_step(1)
+    s_fwd, s_bwd = shared_step(2)
+
+    sent_out = pack(place, [expert_down, shared_down])
     got_out = lax.ppermute(sent_out, "tp", swap)
     e_down, s_down = expert_down, shared_down
     down_w = own_first(
@@ -200,11 +223,12 @@
     sdown_w = own_first(s_down, got_out[n_hid:], 1).reshape(n_y, 2 * hid, width)
 
     rows = slots + half
-    n_sub = rows // 2
-    raw = jnp.concatenate([arrived, own_rows], axis=0).astype(F32)
+    n_sub = slots // 2
+    arrived, shared[1], shared[2] = lax.optimization_barrier((arrived, shared[1], shared[2]))
+    raw = arrived.astype(F32)
     chunk = (raw * gain).astype(BF)
-    square = jnp.sum(raw * raw, axis=1)
-    spans = (((0, n_sub, 0),), ((0, slots - n_sub, 0), (slots - n_sub, n_sub, 1)))
+    own_rows = own_rows.astype(F32)
+    square = jnp.concatenate([jnp.sum(raw * raw, axis=1), jnp.sum(own_rows * own_rows, axis=1)])
     fwd = [chunk[:n_sub], chunk[n_sub:]]
     bwd = list(fwd)
     early, early_at = list(fwd), [(0, 0), (1, 0)]
@@ -222,40 +246,49 @@
                 pieces.append(bwd[k])
                 at.append((k, step))
         if step == 1:
-            squares = to_all_y(after(square, fwd[0]))
+            squares = to_all_y(square)
+            sent_in = pack(
+                place, [expert_gate, expert_up, shared_gate, shared_up]
+            )
+            got_in = lax.ppermute(sent_in, "tp", swap)
+            s_fwd, s_bwd = shared_step(3)
+        if step == 2:
+            s_fwd, s_bwd = shared_step(4)
         if step == 3:
-            square_sum = jnp.sum(after(squares, fwd[0], bwd[0]), axis=0)
+            square_sum = jnp.sum(squares, axis=0)
             scale = lax.rsqrt(square_sum / feat_all + EPSILON)[:, None]
 
     flops = 2 * rows * feat_all * 4 * hid
     n_early = len(early)
-    total, w_last, sw_last = pl.pallas_call(
-        functools.partial(early_kernel, early_at, spans, n_y, width),
+    total, s_total, w_last = pl.pallas_call(
+        functools.partial(early_kernel, early_at, n_y, width),
         out_shape=(
-            jax.ShapeDtypeStruct((rows, 4 * hid), F32),
-            jax.ShapeDtypeStruct((4 * hid, width), BF),
+            jax.ShapeDtypeStruct((slots, 4 * hid), F32),
+            jax.ShapeDtypeStruct((half, 4 * hid), F32),
             jax.ShapeDtypeStruct((4 * hid, width), BF),
         ),
-        in_specs=[SMEM] + [HBM] * (5 + n_early),
+        in_specs=[SMEM] + [HBM] * (5 + n_early + n_y),
         out_specs=(VMEM, VMEM, VMEM),
         scratch_shapes=[
             pltpu.VMEM((4 * hid, feat_all), BF),
             pltpu.VMEM((4 * hid, feat_all), BF),
-            pltpu.VMEM((n_early, n_sub, width), BF),
+            pltpu.VMEM((slots, feat_all), BF),
+            pltpu.VMEM((half, feat_all), BF),
             pltpu.SemaphoreType.DMA((8,)),
             pltpu.SemaphoreType.DMA((n_early,)),
+            pltpu.SemaphoreType.DMA((n_y,)),
         ],
         cost_estimate=pl.CostEstimate(flops=flops, bytes_accessed=2**23, transcendentals=0),
-        compiler_params=pltpu.CompilerParams(vmem_limit_bytes=20 * 2**20),
-    )(place, expert_gate, expert_up, shared_gate, shared_up, got_in, *early)
+        compiler_params=pltpu.CompilerParams(vmem_limit_bytes=24 * 2**20),
+    )(place, expert_gate, expert_up, shared_gate, shared_up, got_in, *early, *shared)
     hidden = pl.pallas_call(
-        functools.partial(late_kernel, spans),
+        late_kernel,
         out_shape=jax.ShapeDtypeStruct((n_y, rows, 2 * hid), BF),
         in_specs=[VMEM] * 6,
         out_specs=VMEM,
         cost_estimate=pl.CostEstimate(flops=flops // 8, bytes_accessed=2**21, transcendentals=0),
         compiler_params=pltpu.CompilerParams(vmem_limit_bytes=12 * 2**20),
-    )(w_last, sw_last, total, scale, *late)
+    )(w_last, total, s_total, scale, *late)
 
     hidden_all = lax.all_to_all(hidden, "tp", 0, 0, axis_index_groups=y_groups, tiled=True)
     contract = (((0, 2), (0, 1)), ((), ()))

time: 197 us -> 213 us (1.081)
  starting transfers between devices: 91.8 us -> 117 us
  waiting for transfers between devices: 38.9 us -> 31.1 us
  local copies, waits for them, and re-layouts: 19.7 us -> 16.7 us
  other arithmetic: 4.4 us -> 6.62 us
    ppermute x2 -> x8, starting transfers between devices: 11.1 us -> 30.6 us  [the longest x3 12.9 us: shared_step(): b = lax.ppermute(b, 'tp', y_shift(-1))]
    all_to_all x1, waiting for transfers between devices: 6.13 us -> 0.01 us  [body(): lax.all_to_all(outgoing.reshape(n_ep, cap, width), 'ep', 0, 0, tiled=True)]
    all_to_all x1, starting transfers between devices: 6.08 us -> 10.2 us  [body(): lax.all_to_all(expert_out.reshape(n_ep, cap, width), 'ep', 0, 0, tiled=True)]
    unnamed x67 -> x70, local copies, waits for them, and re-layouts: 17.3 us -> 13.3 us
    all_to_all x1, waiting for transfers between devices: 15.9 us -> 13.6 us  [body(): lax.all_to_all(hidden, 'tp', 0, 0, axis_index_groups=y_groups, tiled=True)]
  transfers between devices with their start and end apart: 22 -> 28, of which waited for: 6 -> 6; matrix products, arithmetic and copies ran while one was open for 3% -> 4% of each run, Pallas kernels for 5% -> 4%
where the time goes in v2:
time: 213 us; the launch traced here: 212 us
  starting transfers between devices  117 us (55%)
  waiting for transfers between devices  31.1 us (15%)
  blocking collectives  22.6 us (11%)
  local copies, waits for them, and re-layouts  16.7 us (8%)
  Pallas kernels  10.2 us (5%)
  other arithmetic  6.62 us (3%)
  matrix products  6.61 us (3%)
    ppermute x7, starting transfers between devices, body(): bwd[k] = lax.ppermute(bwd[k], 'tp', y_shift(-1))  26.3 us
    ppermute x7, starting transfers between devices, body(): fwd[k] = lax.ppermute(fwd[k], 'tp', y_shift(1))  15.5 us
    all_to_all x1, waiting for transfers between devices, body(): lax.all_to_all(hidden, 'tp', 0, 0, axis_index_groups=y_groups, tiled=True)  13.6 us
    unnamed x70, local copies, waits for them, and re-layouts  13.3 us
    ppermute x3, starting transfers between devices, shared_step(): b = lax.ppermute(b, 'tp', y_shift(-1))  12.9 us
    all_to_all x1, blocking collectives, to_all_y(): lax.all_to_all(sent, 'tp', 0, 0, axis_index_groups=y_groups, tiled=True)  12.5 us
    all_to_all x1, waiting for transfers between devices, body(): lax.all_to_all(expert_out.reshape(n_ep, cap, width), 'ep', 0, 0, tiled=True)  11.2 us
    ppermute x1, starting transfers between devices, body(): got_out = lax.ppermute(sent_out, 'tp', swap)  10.7 us
  transfers between devices with their start and end apart: 28, of which 6 were waited for; matrix products, arithmetic and copies ran while one was open for 4% of the time, Pallas kernels for 4%

profile of v2, /device:TPU:1, one launch (start us, length us, event | category | flops | bytes accessed | tf_op | source)
XLA Modules:
  0.0 211.7 jit_solution(5769394994429764668)
XLA Ops:
  1.9 8.7 %collective-permute-start.1 = (bf16[272,256]{1,0:T(8,128)(2,1)S(1)}, bf16[272,256]{1,0:T(8,128)(2,1)S(1)}, u32[]{:S(2)}, u32[]{:S(2)}) collective-permute-start(bf16[272,256]{1,0:T(8,128)(2,1)S(1)} %concatenate.57), channel_id=1, source_target_pairs={{0,1},{1,0},{2,3},{3,2},{4,5},{5,4},{6,7},{7,6},{8,9},{9,8},{10,11... | collective-permute-start | bytes 417800 | tf_op jit(solution)/shard_map/ppermute | solution.py:181
  15.7 7.7 %all-to-all-start = ((bf16[32,16,512]{2,1,0:T(8,128)(2,1)}), bf16[32,16,512]{2,1,0:T(8,128)(2,1)}, u32[]{:S(2)}, u32[]{:S(2)}) async-start(bf16[32,16,512]{2,1,0:T(8,128)(2,1)} %bitcast.43), calls=%async_computation | async-start | bytes 1048576 | tf_op jit(solution)/shard_map/all_to_all | solution.py:198
  23.5 2.1 %shard_map.109 = bf16[256,4096]{1,0:T(8,128)(2,1)} custom-call(s32[2]{0:T(128)S(1)} %pad_add_fusion.at_ref, bf16[2,64,4096]{2,1,0:T(8,128)(2,1)S(1)} %copy-done, bf16[2,64,4096]{2,1,0:T(8,128)(2,1)S(1)} %copy-done.1, bf16[64,4096]{1,0:T(8,128)(2,1)S(1)} %copy-done.3, bf16[64,4096]{1,0:T(8,128)(2,1)S(1)} %copy-done.4), custom_call_target="tpu_custom_call" | custom-call | flops 400000000 | bytes 4194304 | tf_op jit(solution)/shard_map/pallas_call | solution.py:118
  25.7 2.2 %collective-permute-start = (bf16[256,4096]{1,0:T(8,128)(2,1)}, bf16[256,4096]{1,0:T(8,128)(2,1)}, u32[]{:S(2)}, u32[]{:S(2)}) collective-permute-start(bf16[256,4096]{1,0:T(8,128)(2,1)} %shard_map.109), channel_id=1, source_target_pairs={{0,1},{1,0},{2,3},{3,2},{4,5},{5,4},{6,7},{7,6},{8,9},{9,8},{10,11... | collective-permute-start | bytes 6291464 | tf_op jit(solution)/shard_map/ppermute | solution.py:253
  29.3 3.2 %collective-permute-start.2 = (bf16[128,512]{1,0:T(8,128)(2,1)S(1)}, bf16[128,512]{1,0:T(8,128)(2,1)S(1)}, u32[]{:S(2)}, u32[]{:S(2)}) collective-permute-start(bf16[128,512]{1,0:T(8,128)(2,1)S(1)} %get-tuple-element.26.refs_14_), channel_id=1, source_target_pairs={{0,2},{1,3},{2,4},{3,5},{4,6},{5,7},{6,8},{7,9},{8,10},{9,11},{10,... | collective-permute-start | bytes 393224 | tf_op jit(solution)/shard_map/ppermute | solution.py:207
  32.5 3.8 %collective-permute-start.3 = (bf16[128,512]{1,0:T(8,128)(2,1)S(1)}, bf16[128,512]{1,0:T(8,128)(2,1)S(1)}, u32[]{:S(2)}, u32[]{:S(2)}) collective-permute-start(bf16[128,512]{1,0:T(8,128)(2,1)S(1)} %get-tuple-element.26.refs_14_), channel_id=1, source_target_pairs={{0,14},{1,15},{2,0},{3,1},{4,2},{5,3},{6,4},{7,5},{8,6},{9,7},{10,... | collective-permute-start | bytes 393224 | tf_op jit(solution)/shard_map/ppermute | solution.py:210
  40.1 4.6 %collective-permute-start.17 = (bf16[128,512]{1,0:T(8,128)(2,1)S(1)}, bf16[128,512]{1,0:T(8,128)(2,1)}, u32[]{:S(2)}, u32[]{:S(2)}) collective-permute-start(bf16[128,512]{1,0:T(8,128)(2,1)S(1)} %collective-permute-done.3.refs_16_), channel_id=1, source_target_pairs={{0,14},{1,15},{2,0},{3,1},{4,2},{5,3},{6,4},{7,5},{8,6},{9,7},{10,... | collective-permute-start | bytes 393224 | tf_op jit(solution)/shard_map/ppermute | solution.py:210
  48.2 4.6 %collective-permute-start.19 = (bf16[128,512]{1,0:T(8,128)(2,1)}, bf16[128,512]{1,0:T(8,128)(2,1)}, u32[]{:S(2)}, u32[]{:S(2)}) collective-permute-start(bf16[128,512]{1,0:T(8,128)(2,1)} %collective-permute-done.17.refs_18_), channel_id=1, source_target_pairs={{0,14},{1,15},{2,0},{3,1},{4,2},{5,3},{6,4},{7,5},{8,6},{9,7},{10,... | collective-permute-start | bytes 393224 | tf_op jit(solution)/shard_map/ppermute | solution.py:210
  52.8 1.9 collective-permute-start.20
  56.0 1.9 collective-permute-start.4
  58.0 4.6 %collective-permute-start.7 = (bf16[256,512]{1,0:T(8,128)(2,1)S(1)}, bf16[256,512]{1,0:T(8,128)(2,1)S(1)}, u32[]{:S(2)}, u32[]{:S(2)}) collective-permute-start(bf16[256,512]{1,0:T(8,128)(2,1)S(1)} %get-tuple-element.23.refs_1_), channel_id=1, source_target_pairs={{0,14},{1,15},{2,0},{3,1},{4,2},{5,3},{6,4},{7,5},{8,6},{9,7},{10,... | collective-permute-start | bytes 786440 | tf_op jit(solution)/shard_map/ppermute | solution.py:245
  62.6 3.4 %collective-permute-start.5 = (bf16[256,512]{1,0:T(8,128)(2,1)S(1)}, bf16[256,512]{1,0:T(8,128)(2,1)S(1)}, u32[]{:S(2)}, u32[]{:S(2)}) collective-permute-start(bf16[256,512]{1,0:T(8,128)(2,1)S(1)} %get-tuple-element.24.refs_0_), channel_id=1, source_target_pairs={{0,14},{1,15},{2,0},{3,1},{4,2},{5,3},{6,4},{7,5},{8,6},{9,7},{10,... | collective-permute-start | bytes 786440 | tf_op jit(solution)/shard_map/ppermute | solution.py:245
  68.6 2.8 %collective-permute-start.8 = (bf16[256,512]{1,0:T(8,128)(2,1)S(1)}, bf16[256,512]{1,0:T(8,128)(2,1)}, u32[]{:S(2)}, u32[]{:S(2)}) collective-permute-start(bf16[256,512]{1,0:T(8,128)(2,1)S(1)} %collective-permute-done.4.refs_2_), channel_id=1, source_target_pairs={{0,2},{1,3},{2,4},{3,5},{4,6},{5,7},{6,8},{7,9},{8,10},{9,11},{10,... | collective-permute-start | bytes 786440 | tf_op jit(solution)/shard_map/ppermute | solution.py:241
  72.1 3.7 %collective-permute-start.11 = (bf16[256,512]{1,0:T(8,128)(2,1)S(1)}, bf16[256,512]{1,0:T(8,128)(2,1)}, u32[]{:S(2)}, u32[]{:S(2)}) collective-permute-start(bf16[256,512]{1,0:T(8,128)(2,1)S(1)} %collective-permute-done.7.refs_5_), channel_id=1, source_target_pairs={{0,14},{1,15},{2,0},{3,1},{4,2},{5,3},{6,4},{7,5},{8,6},{9,7},{10,... | collective-permute-start | bytes 786440 | tf_op jit(solution)/shard_map/ppermute | solution.py:245
  76.5 3.4 %collective-permute-start.9 = (bf16[256,512]{1,0:T(8,128)(2,1)S(1)}, bf16[256,512]{1,0:T(8,128)(2,1)}, u32[]{:S(2)}, u32[]{:S(2)}) collective-permute-start(bf16[256,512]{1,0:T(8,128)(2,1)S(1)} %collective-permute-done.5.refs_3_), channel_id=1, source_target_pairs={{0,14},{1,15},{2,0},{3,1},{4,2},{5,3},{6,4},{7,5},{8,6},{9,7},{10,... | collective-permute-start | bytes 786440 | tf_op jit(solution)/shard_map/ppermute | solution.py:245
  83.2 2.8 %collective-permute-start.12 = (bf16[256,512]{1,0:T(8,128)(2,1)}, bf16[256,512]{1,0:T(8,128)(2,1)}, u32[]{:S(2)}, u32[]{:S(2)}) collective-permute-start(bf16[256,512]{1,0:T(8,128)(2,1)} %collective-permute-done.8.refs_6_), channel_id=1, source_target_pairs={{0,2},{1,3},{2,4},{3,5},{4,6},{5,7},{6,8},{7,9},{8,10},{9,11},{10,... | collective-permute-start | bytes 786440 | tf_op jit(solution)/shard_map/ppermute | solution.py:241
  86.0 3.7 %collective-permute-start.15 = (bf16[256,512]{1,0:T(8,128)(2,1)}, bf16[256,512]{1,0:T(8,128)(2,1)}, u32[]{:S(2)}, u32[]{:S(2)}) collective-permute-start(bf16[256,512]{1,0:T(8,128)(2,1)} %collective-permute-done.11.refs_9_), channel_id=1, source_target_pairs={{0,14},{1,15},{2,0},{3,1},{4,2},{5,3},{6,4},{7,5},{8,6},{9,7},{10,... | collective-permute-start | bytes 786440 | tf_op jit(solution)/shard_map/ppermute | solution.py:245
  89.7 3.4 %collective-permute-start.13 = (bf16[256,512]{1,0:T(8,128)(2,1)}, bf16[256,512]{1,0:T(8,128)(2,1)}, u32[]{:S(2)}, u32[]{:S(2)}) collective-permute-start(bf16[256,512]{1,0:T(8,128)(2,1)} %collective-permute-done.9.refs_7_), channel_id=1, source_target_pairs={{0,14},{1,15},{2,0},{3,1},{4,2},{5,3},{6,4},{7,5},{8,6},{9,7},{10,... | collective-permute-start | bytes 786440 | tf_op jit(solution)/shard_map/ppermute | solution.py:245
  93.1 1.9 collective-permute-start.14
  95.1 12.5 %all_to_all.27 = f32[8,1,640]{2,1,0:T(1,128)} all-to-all(f32[8,1,640]{2,1,0:T(1,128)S(1)} %broadcast_in_dim.80), channel_id=1, replica_groups={{0,2,4,6,8,10,12,14},{1,3,5,7,9,11,13,15},{16,18,20,22,24,26,28,30},{17..., dimensions={0} | all-to-all | bytes 40960 | tf_op jit(solution)/shard_map/all_to_all | solution.py:176
  108.3 2.2 %collective-permute-start.21 = (bf16[256,512]{1,0:T(8,128)(2,1)}, bf16[256,512]{1,0:T(8,128)(2,1)S(1)}, u32[]{:S(2)}, u32[]{:S(2)}) collective-permute-start(bf16[256,512]{1,0:T(8,128)(2,1)} %collective-permute-done.12.refs_10_), channel_id=1, source_target_pairs={{0,2},{1,3},{2,4},{3,5},{4,6},{5,7},{6,8},{7,9},{8,10},{9,11},{10,... | collective-permute-start | bytes 786440 | tf_op jit(solution)/shard_map/ppermute | solution.py:241
  110.6 4.3 %collective-permute-start.22 = (bf16[256,512]{1,0:T(8,128)(2,1)}, bf16[256,512]{1,0:T(8,128)(2,1)S(1)}, u32[]{:S(2)}, u32[]{:S(2)}) collective-permute-start(bf16[256,512]{1,0:T(8,128)(2,1)} %collective-permute-done.15.refs_13_), channel_id=1, source_target_pairs={{0,14},{1,15},{2,0},{3,1},{4,2},{5,3},{6,4},{7,5},{8,6},{9,7},{10,... | collective-permute-start | bytes 786440 | tf_op jit(solution)/shard_map/ppermute | solution.py:245
  122.5 5.8 %shard_map.110 = (f32[512,256]{1,0:T(8,128)S(1)}, f32[128,256]{1,0:T(8,128)S(1)}, bf16[256,512]{1,0:T(8,128)(2,1)S(1)}) custom-call(s32[2]{0:T(128)S(1)} %pad_add_fusion.at_ref, bf16[2,64,4096]{2,1,0:T(8,128)(2,1)S(1)} %copy-done, bf16[2,64,4096]{2,1,0:T(8,128)(2,1)S(1)} %copy-done.1, bf16[64,4096]{1,0:T(8,128)(2,1)S(1)} %copy-done.3, ...), custom_call_target="tpu_custom_call" | custom-call | flops 1342177280 | bytes 8388608 | tf_op jit(solution)/shard_map/pallas_call | solution.py:263
  129.9 4.3 %all-to-all-start.2 = ((bf16[8,640,128]{2,1,0:T(8,128)(2,1)}), bf16[8,640,128]{2,1,0:T(8,128)(2,1)}, u32[]{:S(2)}, u32[]{:S(2)}) async-start(bf16[8,640,128]{2,1,0:T(8,128)(2,1)} %shard_map.111), calls=%async_computation.2 | async-start | bytes 2621440 | tf_op jit(solution)/shard_map/all_to_all | solution.py:293
  134.9 10.7 %collective-permute-start.23 = (bf16[2048,256]{1,0:T(8,128)(2,1)S(1)}, bf16[2048,256]{1,0:T(8,128)(2,1)}, u32[]{:S(2)}, u32[]{:S(2)}) collective-permute-start(bf16[2048,256]{1,0:T(8,128)(2,1)S(1)} %shard_map.112), channel_id=1, source_target_pairs={{0,1},{1,0},{2,3},{3,2},{4,5},{5,4},{6,7},{7,6},{8,9},{9,8},{10,11... | collective-permute-start | bytes 3145736 | tf_op jit(solution)/shard_map/ppermute | solution.py:218
  145.7 2.3 %collective-permute-done.23 = bf16[2048,256]{1,0:T(8,128)(2,1)} collective-permute-done((bf16[2048,256]{1,0:T(8,128)(2,1)S(1)}, bf16[2048,256]{1,0:T(8,128)(2,1)}, u32[]{:S(2)}, u32[]{:S(2)}) %collective-permute-start.23) | collective-permute-done | bytes 1048608 | tf_op jit(solution)/shard_map/ppermute | solution.py:218
  149.3 13.6 %all-to-all-done.2 = bf16[8,640,128]{2,1,0:T(8,128)(2,1)} async-done(((bf16[8,640,128]{2,1,0:T(8,128)(2,1)}), bf16[8,640,128]{2,1,0:T(8,128)(2,1)}, u32[]{:S(2)}, u32[]{:S(2)}) %all-to-all-start.2) | async-done | bytes 1310752 | tf_op jit(solution)/shard_map/all_to_all | solution.py:293
  162.8 2.8 %fusion = bf16[512,512]{1,0:T(8,128)(2,1)} fusion(bf16[8,640,128]{2,1,0:T(8,128)(2,1)} %all-to-all-done.2, bf16[8,128,256]{2,1,0:T(8,128)(2,1)S(1)} %bitcast.46, bf16[8,128,256]{2,1,0:T(8,128)(2,1)S(1)} %bitcast.44, pred[]{:T(512)S(6)} %eq.84), kind=kOutput, calls=%fused_computation.3 | convolution fusion | flops 541851648 | bytes 2621441 | tf_op jit(solution)/shard_map/dot_general | solution.py:295
  165.6 10.2 %all-to-all-start.3 = ((bf16[32,16,512]{2,1,0:T(8,128)(2,1)}), bf16[32,16,512]{2,1,0:T(8,128)(2,1)S(1)}, u32[]{:S(2)}, u32[]{:S(2)}) async-start(bf16[32,16,512]{2,1,0:T(8,128)(2,1)} %bitcast.16), calls=%async_computation.3 | async-start | bytes 1048576 | tf_op jit(solution)/shard_map/all_to_all | solution.py:296
  177.3 11.2 %all-to-all-done.3 = bf16[32,16,512]{2,1,0:T(8,128)(2,1)S(1)} async-done(((bf16[32,16,512]{2,1,0:T(8,128)(2,1)}), bf16[32,16,512]{2,1,0:T(8,128)(2,1)S(1)}, u32[]{:S(2)}, u32[]{:S(2)}) %all-to-all-start.3) | async-done | bytes 524320 | tf_op jit(solution)/shard_map/all_to_all | solution.py:296
  189.9 9.6 %collective-permute-start.24 = (f32[256,256]{1,0:T(8,128)S(1)}, f32[256,256]{1,0:T(8,128)S(1)}, u32[]{:S(2)}, u32[]{:S(2)}) collective-permute-start(f32[256,256]{1,0:T(8,128)S(1)} %slice_select_fusion), channel_id=1, source_target_pairs={{0,1},{1,0},{2,3},{3,2},{4,5},{5,4},{6,7},{7,6},{8,9},{9,8},{10,11... | collective-permute-start | bytes 786440 | tf_op jit(solution)/shard_map/ppermute | solution.py:317
  200.8 10.1 %all_to_all.28 = f32[16,1,256]{2,1,0:T(1,128)S(1)} all-to-all(f32[16,1,256]{2,1,0:T(1,128)S(1)} %broadcast_in_dim.81), channel_id=1, replica_groups=mesh['ep'=32,'tp'=16] {'tp'}, dimensions={0} | all-to-all | bytes 32768 | tf_op jit(solution)/shard_map/all_to_all | solution.py:320
  (144 shorter events, 41.0 us)
Async XLA Ops:
  0.0 23.5 %copy-start = (bf16[2,64,4096]{2,1,0:T(8,128)(2,1)S(1)}, bf16[2,64,4096]{2,1,0:T(8,128)(2,1)}, u32[]{:S(2)}) copy-start(bf16[2,64,4096]{2,1,0:T(8,128)(2,1)} %gate.1) | copy-start | bytes 3145732
  0.0 23.5 %copy-start.1 = (bf16[2,64,4096]{2,1,0:T(8,128)(2,1)S(1)}, bf16[2,64,4096]{2,1,0:T(8,128)(2,1)}, u32[]{:S(2)}) copy-start(bf16[2,64,4096]{2,1,0:T(8,128)(2,1)} %up.1) | copy-start | bytes 3145732
  0.0 23.5 %copy-start.3 = (bf16[64,4096]{1,0:T(8,128)(2,1)S(1)}, bf16[64,4096]{1,0:T(8,128)(2,1)}, u32[]{:S(2)}) copy-start(bf16[64,4096]{1,0:T(8,128)(2,1)} %s_gate.1) | copy-start | bytes 1572868
  1.9 10.6 %collective-permute-start.1 = (bf16[272,256]{1,0:T(8,128)(2,1)S(1)}, bf16[272,256]{1,0:T(8,128)(2,1)S(1)}, u32[]{:S(2)}, u32[]{:S(2)}) collective-permute-start(bf16[272,256]{1,0:T(8,128)(2,1)S(1)} %concatenate.57), channel_id=1, source_target_pairs={{0,1},{1,0},{2,3},{3,2},{4,5},{5,4},{6,7},{7,6},{8,9},{9,8},{10,11... | collective-permute-start | bytes 417800 | tf_op jit(solution)/shard_map/ppermute | solution.py:181
  15.7 38.9 %all-to-all-start = ((bf16[32,16,512]{2,1,0:T(8,128)(2,1)}), bf16[32,16,512]{2,1,0:T(8,128)(2,1)}, u32[]{:S(2)}, u32[]{:S(2)}) async-start(bf16[32,16,512]{2,1,0:T(8,128)(2,1)} %bitcast.43), calls=%async_computation | async-start | bytes 1048576 | tf_op jit(solution)/shard_map/all_to_all | solution.py:198
  25.7 89.4 %collective-permute-start = (bf16[256,4096]{1,0:T(8,128)(2,1)}, bf16[256,4096]{1,0:T(8,128)(2,1)}, u32[]{:S(2)}, u32[]{:S(2)}) collective-permute-start(bf16[256,4096]{1,0:T(8,128)(2,1)} %shard_map.109), channel_id=1, source_target_pairs={{0,1},{1,0},{2,3},{3,2},{4,5},{5,4},{6,7},{7,6},{8,9},{9,8},{10,11... | collective-permute-start | bytes 6291464 | tf_op jit(solution)/shard_map/ppermute | solution.py:253
  29.3 8.8 %collective-permute-start.2 = (bf16[128,512]{1,0:T(8,128)(2,1)S(1)}, bf16[128,512]{1,0:T(8,128)(2,1)S(1)}, u32[]{:S(2)}, u32[]{:S(2)}) collective-permute-start(bf16[128,512]{1,0:T(8,128)(2,1)S(1)} %get-tuple-element.26.refs_14_), channel_id=1, source_target_pairs={{0,2},{1,3},{2,4},{3,5},{4,6},{5,7},{6,8},{7,9},{8,10},{9,11},{10,... | collective-permute-start | bytes 393224 | tf_op jit(solution)/shard_map/ppermute | solution.py:207
  32.5 7.6 %collective-permute-start.3 = (bf16[128,512]{1,0:T(8,128)(2,1)S(1)}, bf16[128,512]{1,0:T(8,128)(2,1)S(1)}, u32[]{:S(2)}, u32[]{:S(2)}) collective-permute-start(bf16[128,512]{1,0:T(8,128)(2,1)S(1)} %get-tuple-element.26.refs_14_), channel_id=1, source_target_pairs={{0,14},{1,15},{2,0},{3,1},{4,2},{5,3},{6,4},{7,5},{8,6},{9,7},{10,... | collective-permute-start | bytes 393224 | tf_op jit(solution)/shard_map/ppermute | solution.py:210
  38.1 7.5 %collective-permute-start.16 = (bf16[128,512]{1,0:T(8,128)(2,1)S(1)}, bf16[128,512]{1,0:T(8,128)(2,1)S(1)}, u32[]{:S(2)}, u32[]{:S(2)}) collective-permute-start(bf16[128,512]{1,0:T(8,128)(2,1)S(1)} %collective-permute-done.2.refs_15_), channel_id=1, source_target_pairs={{0,2},{1,3},{2,4},{3,5},{4,6},{5,7},{6,8},{7,9},{8,10},{9,11},{10,... | collective-permute-start | bytes 393224 | tf_op jit(solution)/shard_map/ppermute | solution.py:207
  40.1 8.1 %collective-permute-start.17 = (bf16[128,512]{1,0:T(8,128)(2,1)S(1)}, bf16[128,512]{1,0:T(8,128)(2,1)}, u32[]{:S(2)}, u32[]{:S(2)}) collective-permute-start(bf16[128,512]{1,0:T(8,128)(2,1)S(1)} %collective-permute-done.3.refs_16_), channel_id=1, source_target_pairs={{0,14},{1,15},{2,0},{3,1},{4,2},{5,3},{6,4},{7,5},{8,6},{9,7},{10,... | collective-permute-start | bytes 393224 | tf_op jit(solution)/shard_map/ppermute | solution.py:210
  45.6 7.1 %collective-permute-start.18 = (bf16[128,512]{1,0:T(8,128)(2,1)S(1)}, bf16[128,512]{1,0:T(8,128)(2,1)}, u32[]{:S(2)}, u32[]{:S(2)}) collective-permute-start(bf16[128,512]{1,0:T(8,128)(2,1)S(1)} %collective-permute-done.16.refs_17_), channel_id=1, source_target_pairs={{0,2},{1,3},{2,4},{3,5},{4,6},{5,7},{6,8},{7,9},{8,10},{9,11},{10,... | collective-permute-start | bytes 393224 | tf_op jit(solution)/shard_map/ppermute | solution.py:207
  48.2 14.4 %collective-permute-start.19 = (bf16[128,512]{1,0:T(8,128)(2,1)}, bf16[128,512]{1,0:T(8,128)(2,1)}, u32[]{:S(2)}, u32[]{:S(2)}) collective-permute-start(bf16[128,512]{1,0:T(8,128)(2,1)} %collective-permute-done.17.refs_18_), channel_id=1, source_target_pairs={{0,14},{1,15},{2,0},{3,1},{4,2},{5,3},{6,4},{7,5},{8,6},{9,7},{10,... | collective-permute-start | bytes 393224 | tf_op jit(solution)/shard_map/ppermute | solution.py:210
  52.8 13.9 %collective-permute-start.20 = (bf16[128,512]{1,0:T(8,128)(2,1)}, bf16[128,512]{1,0:T(8,128)(2,1)}, u32[]{:S(2)}, u32[]{:S(2)}) collective-permute-start(bf16[128,512]{1,0:T(8,128)(2,1)} %collective-permute-done.18.refs_19_), channel_id=1, source_target_pairs={{0,2},{1,3},{2,4},{3,5},{4,6},{5,7},{6,8},{7,9},{8,10},{9,11},{10,... | collective-permute-start | bytes 393224 | tf_op jit(solution)/shard_map/ppermute | solution.py:207
  54.7 40.3 %copy-start.29 = (f32[128]{0:T(128)S(1)}, f32[128]{0:T(128)}, u32[]{:S(2)}) copy-start(f32[128]{0:T(128)} %get-tuple-element.25) | copy-start | bytes 1540
  56.0 12.5 %collective-permute-start.4 = (bf16[256,512]{1,0:T(8,128)(2,1)S(1)}, bf16[256,512]{1,0:T(8,128)(2,1)S(1)}, u32[]{:S(2)}, u32[]{:S(2)}) collective-permute-start(bf16[256,512]{1,0:T(8,128)(2,1)S(1)} %get-tuple-element.24.refs_0_), channel_id=1, source_target_pairs={{0,2},{1,3},{2,4},{3,5},{4,6},{5,7},{6,8},{7,9},{8,10},{9,11},{10,... | collective-permute-start | bytes 786440 | tf_op jit(solution)/shard_map/ppermute | solution.py:241
  58.0 14.1 %collective-permute-start.7 = (bf16[256,512]{1,0:T(8,128)(2,1)S(1)}, bf16[256,512]{1,0:T(8,128)(2,1)S(1)}, u32[]{:S(2)}, u32[]{:S(2)}) collective-permute-start(bf16[256,512]{1,0:T(8,128)(2,1)S(1)} %get-tuple-element.23.refs_1_), channel_id=1, source_target_pairs={{0,14},{1,15},{2,0},{3,1},{4,2},{5,3},{6,4},{7,5},{8,6},{9,7},{10,... | collective-permute-start | bytes 786440 | tf_op jit(solution)/shard_map/ppermute | solution.py:245
  62.6 13.9 %collective-permute-start.5 = (bf16[256,512]{1,0:T(8,128)(2,1)S(1)}, bf16[256,512]{1,0:T(8,128)(2,1)S(1)}, u32[]{:S(2)}, u32[]{:S(2)}) collective-permute-start(bf16[256,512]{1,0:T(8,128)(2,1)S(1)} %get-tuple-element.24.refs_0_), channel_id=1, source_target_pairs={{0,14},{1,15},{2,0},{3,1},{4,2},{5,3},{6,4},{7,5},{8,6},{9,7},{10,... | collective-permute-start | bytes 786440 | tf_op jit(solution)/shard_map/ppermute | solution.py:245
  66.7 13.9 %collective-permute-start.6 = (bf16[256,512]{1,0:T(8,128)(2,1)S(1)}, bf16[256,512]{1,0:T(8,128)(2,1)S(1)}, u32[]{:S(2)}, u32[]{:S(2)}) collective-permute-start(bf16[256,512]{1,0:T(8,128)(2,1)S(1)} %get-tuple-element.23.refs_1_), channel_id=1, source_target_pairs={{0,2},{1,3},{2,4},{3,5},{4,6},{5,7},{6,8},{7,9},{8,10},{9,11},{10,... | collective-permute-start | bytes 786440 | tf_op jit(solution)/shard_map/ppermute | solution.py:241
  68.6 14.6 %collective-permute-start.8 = (bf16[256,512]{1,0:T(8,128)(2,1)S(1)}, bf16[256,512]{1,0:T(8,128)(2,1)}, u32[]{:S(2)}, u32[]{:S(2)}) collective-permute-start(bf16[256,512]{1,0:T(8,128)(2,1)S(1)} %collective-permute-done.4.refs_2_), channel_id=1, source_target_pairs={{0,2},{1,3},{2,4},{3,5},{4,6},{5,7},{6,8},{7,9},{8,10},{9,11},{10,... | collective-permute-start | bytes 786440 | tf_op jit(solution)/shard_map/ppermute | solution.py:241
  72.1 13.9 %collective-permute-start.11 = (bf16[256,512]{1,0:T(8,128)(2,1)S(1)}, bf16[256,512]{1,0:T(8,128)(2,1)}, u32[]{:S(2)}, u32[]{:S(2)}) collective-permute-start(bf16[256,512]{1,0:T(8,128)(2,1)S(1)} %collective-permute-done.7.refs_5_), channel_id=1, source_target_pairs={{0,14},{1,15},{2,0},{3,1},{4,2},{5,3},{6,4},{7,5},{8,6},{9,7},{10,... | collective-permute-start | bytes 786440 | tf_op jit(solution)/shard_map/ppermute | solution.py:245
  76.5 13.2 %collective-permute-start.9 = (bf16[256,512]{1,0:T(8,128)(2,1)S(1)}, bf16[256,512]{1,0:T(8,128)(2,1)}, u32[]{:S(2)}, u32[]{:S(2)}) collective-permute-start(bf16[256,512]{1,0:T(8,128)(2,1)S(1)} %collective-permute-done.5.refs_3_), channel_id=1, source_target_pairs={{0,14},{1,15},{2,0},{3,1},{4,2},{5,3},{6,4},{7,5},{8,6},{9,7},{10,... | collective-permute-start | bytes 786440 | tf_op jit(solution)/shard_map/ppermute | solution.py:245
  80.5 12.6 %collective-permute-start.10 = (bf16[256,512]{1,0:T(8,128)(2,1)S(1)}, bf16[256,512]{1,0:T(8,128)(2,1)}, u32[]{:S(2)}, u32[]{:S(2)}) collective-permute-start(bf16[256,512]{1,0:T(8,128)(2,1)S(1)} %collective-permute-done.6.refs_4_), channel_id=1, source_target_pairs={{0,2},{1,3},{2,4},{3,5},{4,6},{5,7},{6,8},{7,9},{8,10},{9,11},{10,... | collective-permute-start | bytes 786440 | tf_op jit(solution)/shard_map/ppermute | solution.py:241
  83.2 25.1 %collective-permute-start.12 = (bf16[256,512]{1,0:T(8,128)(2,1)}, bf16[256,512]{1,0:T(8,128)(2,1)}, u32[]{:S(2)}, u32[]{:S(2)}) collective-permute-start(bf16[256,512]{1,0:T(8,128)(2,1)} %collective-permute-done.8.refs_6_), channel_id=1, source_target_pairs={{0,2},{1,3},{2,4},{3,5},{4,6},{5,7},{6,8},{7,9},{8,10},{9,11},{10,... | collective-permute-start | bytes 786440 | tf_op jit(solution)/shard_map/ppermute | solution.py:241
  86.0 24.5 %collective-permute-start.15 = (bf16[256,512]{1,0:T(8,128)(2,1)}, bf16[256,512]{1,0:T(8,128)(2,1)}, u32[]{:S(2)}, u32[]{:S(2)}) collective-permute-start(bf16[256,512]{1,0:T(8,128)(2,1)} %collective-permute-done.11.refs_9_), channel_id=1, source_target_pairs={{0,14},{1,15},{2,0},{3,1},{4,2},{5,3},{6,4},{7,5},{8,6},{9,7},{10,... | collective-permute-start | bytes 786440 | tf_op jit(solution)/shard_map/ppermute | solution.py:245
  89.7 25.3 %collective-permute-start.13 = (bf16[256,512]{1,0:T(8,128)(2,1)}, bf16[256,512]{1,0:T(8,128)(2,1)}, u32[]{:S(2)}, u32[]{:S(2)}) collective-permute-start(bf16[256,512]{1,0:T(8,128)(2,1)} %collective-permute-done.9.refs_7_), channel_id=1, source_target_pairs={{0,14},{1,15},{2,0},{3,1},{4,2},{5,3},{6,4},{7,5},{8,6},{9,7},{10,... | collective-permute-start | bytes 786440 | tf_op jit(solution)/shard_map/ppermute | solution.py:245
  93.1 21.9 %collective-permute-start.14 = (bf16[256,512]{1,0:T(8,128)(2,1)}, bf16[256,512]{1,0:T(8,128)(2,1)}, u32[]{:S(2)}, u32[]{:S(2)}) collective-permute-start(bf16[256,512]{1,0:T(8,128)(2,1)} %collective-permute-done.10.refs_8_), channel_id=1, source_target_pairs={{0,2},{1,3},{2,4},{3,5},{4,6},{5,7},{6,8},{7,9},{8,10},{9,11},{10,... | collective-permute-start | bytes 786440 | tf_op jit(solution)/shard_map/ppermute | solution.py:241
  108.3 20.0 %collective-permute-start.21 = (bf16[256,512]{1,0:T(8,128)(2,1)}, bf16[256,512]{1,0:T(8,128)(2,1)S(1)}, u32[]{:S(2)}, u32[]{:S(2)}) collective-permute-start(bf16[256,512]{1,0:T(8,128)(2,1)} %collective-permute-done.12.refs_10_), channel_id=1, source_target_pairs={{0,2},{1,3},{2,4},{3,5},{4,6},{5,7},{6,8},{7,9},{8,10},{9,11},{10,... | collective-permute-start | bytes 786440 | tf_op jit(solution)/shard_map/ppermute | solution.py:241
  110.6 17.8 %collective-permute-start.22 = (bf16[256,512]{1,0:T(8,128)(2,1)}, bf16[256,512]{1,0:T(8,128)(2,1)S(1)}, u32[]{:S(2)}, u32[]{:S(2)}) collective-permute-start(bf16[256,512]{1,0:T(8,128)(2,1)} %collective-permute-done.15.refs_13_), channel_id=1, source_target_pairs={{0,14},{1,15},{2,0},{3,1},{4,2},{5,3},{6,4},{7,5},{8,6},{9,7},{10,... | collective-permute-start | bytes 786440 | tf_op jit(solution)/shard_map/ppermute | solution.py:245
  129.9 32.9 %all-to-all-start.2 = ((bf16[8,640,128]{2,1,0:T(8,128)(2,1)}), bf16[8,640,128]{2,1,0:T(8,128)(2,1)}, u32[]{:S(2)}, u32[]{:S(2)}) async-start(bf16[8,640,128]{2,1,0:T(8,128)(2,1)} %shard_map.111), calls=%async_computation.2 | async-start | bytes 2621440 | tf_op jit(solution)/shard_map/all_to_all | solution.py:293
  134.9 13.1 %collective-permute-start.23 = (bf16[2048,256]{1,0:T(8,128)(2,1)S(1)}, bf16[2048,256]{1,0:T(8,128)(2,1)}, u32[]{:S(2)}, u32[]{:S(2)}) collective-permute-start(bf16[2048,256]{1,0:T(8,128)(2,1)S(1)} %shard_map.112), channel_id=1, source_target_pairs={{0,1},{1,0},{2,3},{3,2},{4,5},{5,4},{6,7},{7,6},{8,9},{9,8},{10,11... | collective-permute-start | bytes 3145736 | tf_op jit(solution)/shard_map/ppermute | solution.py:218
  165.6 22.9 %all-to-all-start.3 = ((bf16[32,16,512]{2,1,0:T(8,128)(2,1)}), bf16[32,16,512]{2,1,0:T(8,128)(2,1)S(1)}, u32[]{:S(2)}, u32[]{:S(2)}) async-start(bf16[32,16,512]{2,1,0:T(8,128)(2,1)} %bitcast.16), calls=%async_computation.3 | async-start | bytes 1048576 | tf_op jit(solution)/shard_map/all_to_all | solution.py:296
  189.9 10.8 %collective-permute-start.24 = (f32[256,256]{1,0:T(8,128)S(1)}, f32[256,256]{1,0:T(8,128)S(1)}, u32[]{:S(2)}, u32[]{:S(2)}) collective-permute-start(f32[256,256]{1,0:T(8,128)S(1)} %slice_select_fusion), channel_id=1, source_target_pairs={{0,1},{1,0},{2,3},{3,2},{4,5},{5,4},{6,7},{7,6},{8,9},{9,8},{10,11... | collective-permute-start | bytes 786440 | tf_op jit(solution)/shard_map/ppermute | solution.py:317
  (31 other events, 175.5 us)

commit v3 on v0

v3 whole, which is shorter than its diff:
```python
import functools

import jax
import jax.numpy as jnp
from jax import lax
from jax.experimental import pallas as pl
from jax.experimental.pallas import tpu as pltpu
from jax.sharding import PartitionSpec as P


EPSILON = 1e-06
BF = jnp.bfloat16
F32 = jnp.float32
SPARE = 8


VMEM = pl.BlockSpec(memory_space=pltpu.VMEM)
SMEM = pl.BlockSpec(memory_space=pltpu.SMEM)


def times(x, w):
    return lax.dot_general(x, w, (((1,), (1,)), ((), ())), preferred_element_type=F32)


def thirds(v):
    high = v.astype(BF)
    rest = v - high.astype(F32)
    middle = rest.astype(BF)
    return high, middle, (rest - middle.astype(F32)).astype(BF)


def picks(ids, core, n_ep, cap):
    tok = ids.shape[1]
    named = 2 * lax.broadcasted_iota(jnp.int32, (n_ep, tok), 0) + core
    member = ids[0:1, :] == named
    for k in range(1, ids.shape[0]):
        member = member | (ids[k : k + 1, :] == named)
    before = lax.broadcasted_iota(jnp.int32, (tok, tok), 0) < lax.broadcasted_iota(jnp.int32, (tok, tok), 1)
    one = jnp.where(member, 1.0, 0.0).astype(BF)
    rank = jnp.dot(one, jnp.where(before, 1.0, 0.0).astype(BF), preferred_element_type=F32)
    rank = jnp.where(member, rank, -1.0)
    spread = jnp.broadcast_to(rank[:, None, :], (n_ep, cap, tok))
    slot = lax.broadcasted_iota(jnp.int32, (n_ep, cap, tok), 1).astype(F32)
    return jnp.where(spread == slot, 1.0, 0.0).astype(BF).reshape(n_ep * cap, tok)


def route_kernel(n_ep, cap, at_ref, ids_ref, own_ref, other_ref, out_ref):
    core = at_ref[0]
    one_hot = picks(ids_ref[...], core, n_ep, cap)
    feat = own_ref.shape[1]
    for ref, where in ((own_ref, core), (other_ref, 1 - core)):
        at = pl.ds(pl.multiple_of(where * feat, feat), feat)
        out_ref[:, at] = jnp.dot(one_hot, ref[...], preferred_element_type=F32).astype(BF)


def arrive_kernel(at_ref, rows_ref, own_ref, other_ref, gain_ref, first_ref, second_ref):
    core = at_ref[0]
    slots, width = rows_ref.shape
    half, feat = own_ref.shape[0] // 2, own_ref.shape[1]
    n_sub = (slots + half) // 2
    mine = pl.ds(pl.multiple_of(core * half, half), half)
    own, other = own_ref[mine, :], other_ref[mine, :]
    own, other = jnp.where(core == 0, own, other), jnp.where(core == 0, other, own)
    split = slots - n_sub
    gain = gain_ref[...]

    def put(ref, at, rows, columns):
        raw = rows.astype(F32)
        ref[at : at + rows.shape[0], columns] = (raw * gain[:, columns]).astype(BF)
        return raw * raw

    every, left, right = slice(0, width), slice(0, feat), slice(feat, width)

    def total(squares):
        ones = jnp.ones((SPARE, squares.shape[1]), F32)
        return lax.dot_general(
            ones, squares, (((1,), (1,)), ((), ())), precision=lax.Precision.HIGHEST, preferred_element_type=F32
        )

    def spare(ref, at, sums):
        high, middle, low = thirds(sums)
        row = lax.broadcasted_iota(jnp.int32, sums.shape, 0)
        parts = jnp.where(row == 0, high.astype(F32), jnp.where(row == 1, middle.astype(F32), low.astype(F32)))
        ref[n_sub:, at : at + sums.shape[1]] = jnp.where(row < 3, parts, 0.0).astype(BF)

    for ref in (first_ref, second_ref):
        ref[n_sub:, :] = jnp.zeros((SPARE, width), BF)
    spare(first_ref, 0, total(put(first_ref, 0, rows_ref[:n_sub, :], every)))
    sums = total(put(second_ref, 0, rows_ref[n_sub:, :], every))
    tail = total(put(second_ref, split, own, left)) + total(put(second_ref, split, other, right))
    spare(second_ref, 0, jnp.concatenate([sums, tail], axis=1))


def early_kernel(places, spans, n_y, width, at_ref, gate, up, s_gate, s_up, got, *refs):
    n = len(places)
    pieces = refs[:n]
    total_ref, squares_ref, w_last, sw_last, w, sw = refs[n:]
    core, y = at_ref[0], at_ref[1]
    hid = s_gate.shape[0]
    n_sub = total_ref.shape[0] // 2
    own = pl.multiple_of(core * hid, hid)
    other = pl.multiple_of((1 - core) * hid, hid)
    for i, (mine, into, base) in enumerate(
        ((gate.at[core], w, 0), (up.at[core], w, 2 * hid), (s_gate, sw, 0), (s_up, sw, 2 * hid))
    ):
        into[pl.ds(base + own, hid), :] = mine[...]
        into[pl.ds(base + other, hid), :] = got[i * hid : (i + 1) * hid, :]

    def columns(offset):
        return pl.ds(pl.multiple_of(lax.rem(y + offset + n_y, n_y) * width, width), width)

    for half in range(2):
        total = [None] * len(spans[half])
        squares = jnp.zeros((SPARE, width), F32)
        for piece, (k, offset) in zip(pieces, places):
            if k != half:
                continue
            for j, (low, high, which) in enumerate(spans[half]):
                term = times(piece[low:high, :], (w, sw)[which][:, columns(offset)])
                total[j] = term if total[j] is None else total[j] + term
            squares = squares + piece[n_sub:, :].astype(F32)
        for (low, high, _), value in zip(spans[half], total):
            total_ref[half * n_sub + low : half * n_sub + high, :] = value
        squares_ref[half * SPARE : (half + 1) * SPARE, :] = squares
    w_last[...] = w[:, columns(n_y // 2)]
    sw_last[...] = sw[:, columns(n_y // 2)]


def late_kernel(spans, features, w_ref, sw_ref, total_ref, squares_ref, *refs):
    out_ref = refs[-1]
    n_sub = total_ref.shape[0] // 2
    for half in range(2):
        piece = refs[half]
        squares = squares_ref[half * SPARE : (half + 1) * SPARE, :] + piece[n_sub:, :].astype(F32)
        squares = jnp.sum(squares, axis=0, keepdims=True)
        scale = lax.rsqrt(squares / features + EPSILON)
        scale = jnp.broadcast_to(scale, (128, scale.shape[1])).T
        for low, high, which in spans[half]:
            rows = slice(half * n_sub + low, half * n_sub + high)
            total = total_ref[rows, :] + times(piece[low:high, :], (w_ref, sw_ref)[which][...])
            n = total.shape[1] // 2
            gate, up = total[:, :n] * scale[low:high, :n], total[:, n:] * scale[low:high, :n]
            hidden = (gate / (1.0 + jnp.exp(-gate)) * up).astype(BF)
            for j in range(out_ref.shape[0]):
                out_ref[j, rows, :] = hidden


def down_kernel(at_ref, hidden_ref, own_ref, got_ref, out_ref):
    core = at_ref[0]
    feat = own_ref.shape[2]
    slots = out_ref.shape[0]
    hidden = jnp.concatenate([hidden_ref[j, :slots, :] for j in range(hidden_ref.shape[0])], axis=1)
    for w, where in ((own_ref.at[core], core), (got_ref, 1 - core)):
        at = pl.ds(pl.multiple_of(where * feat, feat), feat)
        out_ref[:, at] = jnp.dot(
            hidden, w[: hidden.shape[1], :], preferred_element_type=F32
        ).astype(BF)


def pack_kernel(at_ref, *refs):
    arrays, out_ref = refs[:-1], refs[-1]
    rows = out_ref.shape[0] // len(arrays)
    for i, a in enumerate(arrays):
        part = a.at[1 - at_ref[0]] if len(a.shape) == 3 else a
        out_ref[i * rows : (i + 1) * rows, :] = part[...]


def call(kernel, out, args, flops, mib, scratch=()):
    return pl.pallas_call(
        kernel,
        out_shape=out,
        in_specs=[SMEM] + [VMEM] * (len(args) - 1),
        out_specs=jax.tree.map(lambda _: VMEM, out),
        scratch_shapes=scratch,
        cost_estimate=pl.CostEstimate(flops=flops, bytes_accessed=2**21, transcendentals=0),
        compiler_params=pltpu.CompilerParams(vmem_limit_bytes=mib * 2**20),
    )(*args)


def body(
    tokens,
    pre_gain,
    expert_ids,
    route_weight,
    expert_gate,
    expert_up,
    expert_down,
    shared_gate,
    shared_up,
    shared_down,
    out_gain,
):
    tok, top = expert_ids.shape
    n_ep = lax.axis_size("ep")
    n_tp = lax.axis_size("tp")
    n_y = n_tp // 2
    experts = expert_gate.shape[0] * n_ep
    cap = 4 * tok * top // (3 * experts)
    feat = tokens.shape[1]
    feat_all = feat * n_tp
    width = 2 * feat
    hid = expert_gate.shape[1]
    n_hid = expert_down.shape[1]
    half = tok // 2
    slots = n_ep * cap
    rows = slots + half
    n_sub = rows // 2
    tp = lax.axis_index("tp")
    core = lax.rem(tp, 2)
    y = lax.div(tp, 2)
    first = core == 0
    place = jnp.stack([core, y]).astype(jnp.int32)

    swap = [(i, i ^ 1) for i in range(n_tp)]
    y_groups = [[c + 2 * k for k in range(n_y)] for c in range(2)]

    def y_shift(d):
        return [(i, ((i // 2 + d) % n_y) * 2 + i % 2) for i in range(n_tp)]

    def own_first(mine, other, axis):
        return jnp.where(
            first,
            jnp.concatenate([mine, other], axis=axis),
            jnp.concatenate([other, mine], axis=axis),
        )

    partner = lax.ppermute(tokens, "tp", swap)
    ids = expert_ids.T
    outgoing = call(
        functools.partial(route_kernel, n_ep, cap),
        jax.ShapeDtypeStruct((slots, width), BF),
        (place, ids, tokens, partner),
        10**8,
        8,
    )
    arrived = lax.all_to_all(outgoing.reshape(n_ep, cap, width), "ep", 0, 0, tiled=True)
    arrived = arrived.reshape(slots, width)

    gain = own_first(pre_gain, lax.ppermute(pre_gain, "tp", swap), 0)[None, :]
    sent_in = call(
        pack_kernel,
        jax.ShapeDtypeStruct((4 * hid, feat_all), BF),
        (place, expert_gate, expert_up, shared_gate, shared_up),
        4 * 10**8,
        8,
    )
    got_in = lax.ppermute(sent_in, "tp", swap)
    sent_out = call(
        pack_kernel,
        jax.ShapeDtypeStruct((2 * n_hid, feat), BF),
        (place, expert_down, shared_down),
        4 * 10**8,
        6,
    )
    got_out = lax.ppermute(sent_out, "tp", swap)

    piece = jax.ShapeDtypeStruct((n_sub + SPARE, width), BF)
    fwd = call(arrive_kernel, (piece, piece), (place, arrived, tokens, partner, gain), 4 * 10**8, 8)
    fwd, bwd = list(fwd), list(fwd)
    spans = (((0, n_sub, 0),), ((0, slots - n_sub, 0), (slots - n_sub, n_sub, 1)))
    early, early_at = list(fwd), [(0, 0), (1, 0)]
    late, late_at = [], []
    for step in range(1, n_y // 2 + 1):
        last = step == n_y // 2
        pieces, at = (late, late_at) if last else (early, early_at)
        for k in range(2):
            if not last or k == 0:
                fwd[k] = lax.ppermute(fwd[k], "tp", y_shift(1))
                pieces.append(fwd[k])
                at.append((k, -step))
            if not last or k == 1:
                bwd[k] = lax.ppermute(bwd[k], "tp", y_shift(-1))
                pieces.append(bwd[k])
                at.append((k, step))

    flops = 2 * rows * feat_all * 4 * hid
    total, squares, w_last, sw_last = call(
        functools.partial(early_kernel, early_at, spans, n_y, width),
        (
            jax.ShapeDtypeStruct((rows, 4 * hid), F32),
            jax.ShapeDtypeStruct((2 * SPARE, width), F32),
            jax.ShapeDtypeStruct((4 * hid, width), BF),
            jax.ShapeDtypeStruct((4 * hid, width), BF),
        ),
        (place, expert_gate, expert_up, shared_gate, shared_up, got_in, *early),
        flops,
        20,
        [pltpu.VMEM((4 * hid, feat_all), BF), pltpu.VMEM((4 * hid, feat_all), BF)],
    )
    hidden = call(
        lambda _, *refs: late_kernel(spans, feat_all, *refs),
        jax.ShapeDtypeStruct((n_y, rows, 2 * hid), BF),
        (place, w_last, sw_last, total, squares, *late),
        flops // 8,
        8,
    )

    hidden_all = lax.all_to_all(hidden, "tp", 0, 0, axis_index_groups=y_groups, tiled=True)
    expert_out = call(
        down_kernel,
        jax.ShapeDtypeStruct((slots, width), BF),
        (place, hidden_all, expert_down, got_out),
        2 * slots * n_hid * width,
        12,
    )
    returned = lax.all_to_all(expert_out.reshape(n_ep, cap, width), "ep", 0, 0, tiled=True)
    returned = returned.reshape(slots, width)

    sdown_w = own_first(shared_down, got_out[n_hid:], 1).reshape(n_y, 2 * hid, width)
    contract = (((0, 2), (0, 1)), ((), ()))
    shared_out = lax.dot_general(hidden_all[:, slots:], sdown_w, contract, preferred_element_type=F32)
    named = 2 * jnp.arange(n_ep, dtype=jnp.int32)[:, None] + core
    hit = [(ids[k][None, :] == named) for k in range(top)]
    member = hit[0] | hit[1] | hit[2]
    earlier = (
        jnp.arange(tok, dtype=jnp.int32)[:, None] < jnp.arange(tok, dtype=jnp.int32)[None, :]
    ).astype(BF)
    rank = jnp.dot(member.astype(BF), earlier, preferred_element_type=F32)
    rank = jnp.where(member, rank, -1.0)
    slot_no = jnp.arange(cap, dtype=jnp.int32).astype(F32)
    pick = rank[:, None, :] == slot_no[None, :, None]
    weight = sum(jnp.where(hit[k], route_weight.T[k][None, :], 0.0) for k in range(top))
    mix = jnp.where(pick, weight[:, None, :], 0.0).reshape(slots, tok)
    high = lax.reduce_precision(mix, 8, 7)
    middle = lax.reduce_precision(mix - high, 8, 7)
    low = mix - high - middle
    part = sum(
        lax.dot_general(m.astype(BF), returned, (((0,), (0,)), ((), ())), preferred_element_type=F32)
        for m in (high, middle, low)
    )
    zero = jnp.zeros_like(shared_out)
    part = part + jnp.where(
        first,
        jnp.concatenate([shared_out, zero], axis=0),
        jnp.concatenate([zero, shared_out], axis=0),
    )
    away = jnp.where(first, part[:, feat:], part[:, :feat])
    home = jnp.where(first, part[:, :feat], part[:, feat:])
    summed = home + lax.ppermute(away, "tp", swap)
    own_square = jnp.sum(summed * summed, axis=1)
    sent = jnp.broadcast_to(own_square[None, :], (n_tp, tok))
    out_square = jnp.sum(lax.all_to_all(sent, "tp", 0, 0, tiled=True), axis=0)
    return (summed * lax.rsqrt(out_square[:, None] / feat_all + EPSILON) * out_gain).astype(BF)


def solution(mesh):
    return jax.shard_map(
        body,
        mesh=mesh,
        in_specs=(
            P("ep", "tp"),
            P("tp"),
            P("ep", None),
            P("ep", None),
            P("ep", "tp", None),
            P("ep", "tp", None),
            P("ep", None, "tp"),
            P("tp", None),
            P("tp", None),
            P(None, "tp"),
            P("tp"),
        ),
        out_specs=P("ep", "tp"),
        check_vma=False,
    )
```

time: 191 us -> 180 us (0.942)
  other arithmetic: 8.24 us -> 1.13 us
  starting transfers between devices: 100 us -> 95.8 us
  Pallas kernels: 9.87 us -> 13.8 us
    concatenate x4 -> x0, other arithmetic: 4.65 us -> none  [the longest x1 1.56 us: body(): jnp.concatenate([own_first(lax.dynamic_index_in_dim(e_gate, core, 0, keep...]
    unnamed x44 -> x36, local copies, waits for them, and re-layouts: 0.56 us -> 5.03 us
    pallas_call x2 -> x7, Pallas kernels: 9.87 us -> 13.8 us  [call(): pl.pallas_call(kernel, out_shape=out, in_specs=[SMEM] + [VMEM] * (len(arg...]
    ppermute x1, starting transfers between devices: 10.4 us -> 6.95 us  [body(): got_out = lax.ppermute(sent_out, 'tp', swap)]
    all_to_all x1, waiting for transfers between devices: 8.96 us -> 5.57 us  [body(): lax.all_to_all(outgoing.reshape(n_ep, cap, width), 'ep', 0, 0, tiled=True)]
    ppermute x7, starting transfers between devices: 28 us -> 31 us  [body(): bwd[k] = lax.ppermute(bwd[k], 'tp', y_shift(-1))]
    broadcast_in_dim x2 -> x0, local copies, waits for them, and re-layouts: 2.89 us -> none  [to_all_y(): sent = jnp.broadcast_to(v[None], (n_y,) + v.shape)]
    dot_general x2 -> x0, matrix products: 2.63 us -> none  [the longest x1 1.53 us: body(): lax.dot_general(hidden_all[:, :slots], down_w, contract, preferred_elemen...]
  transfers between devices with their start and end apart: 23 -> 22, of which waited for: 9 -> 13; matrix products, arithmetic and copies ran while one was open for 5% -> 1% of each run, Pallas kernels for 3% -> 5%
where the time goes in v3:
time: 180 us; the launch traced here: 179 us
  starting transfers between devices  95.8 us (53%)
  waiting for transfers between devices  49.1 us (27%)
  Pallas kernels  13.8 us (8%)
  blocking collectives  10.1 us (6%)
  local copies, waits for them, and re-layouts  5.09 us (3%)
  matrix products  3.01 us (2%)
    ppermute x7, starting transfers between devices, body(): bwd[k] = lax.ppermute(bwd[k], 'tp', y_shift(-1))  31 us
    all_to_all x1, waiting for transfers between devices, body(): lax.all_to_all(hidden, 'tp', 0, 0, axis_index_groups=y_groups, tiled=True)  20.9 us
    ppermute x7, starting transfers between devices, body(): fwd[k] = lax.ppermute(fwd[k], 'tp', y_shift(1))  15.2 us
    pallas_call x7, Pallas kernels, call(): pl.pallas_call(kernel, out_shape=out, in_specs=[SMEM] + [VMEM] * (len(arg...  13.8 us
    all_to_all x1, waiting for transfers between devices, body(): lax.all_to_all(expert_out.reshape(n_ep, cap, width), 'ep', 0, 0, tiled=True)  11.5 us
    all_to_all x1, blocking collectives, body(): out_square = jnp.sum(lax.all_to_all(sent, 'tp', 0, 0, tiled=True), axis=0)  10.1 us
    ppermute x1, starting transfers between devices, body(): partner = lax.ppermute(tokens, 'tp', swap)  8.87 us
    ppermute x1, starting transfers between devices, body(): summed = home + lax.ppermute(away, 'tp', swap)  8.31 us
  transfers between devices with their start and end apart: 22, of which 13 were waited for; matrix products, arithmetic and copies ran while one was open for 1% of the time, Pallas kernels for 5%

profile of v3, /device:TPU:1, one launch (start us, length us, event | category | flops | bytes accessed | tf_op | source)
XLA Modules:
  0.0 178.5 jit_solution(8437913230738684849)
XLA Ops:
  0.0 8.9 %collective-permute-start.1 = (bf16[256,256]{1,0:T(8,128)(2,1)}, bf16[256,256]{1,0:T(8,128)(2,1)S(1)}, u32[]{:S(2)}, u32[]{:S(2)}) collective-permute-start(bf16[256,256]{1,0:T(8,128)(2,1)} %own_ref.4), channel_id=1, source_target_pairs={{0,1},{1,0},{2,3},{3,2},{4,5},{5,4},{6,7},{7,6},{8,9},{9,8},{10,11... | collective-permute-start | bytes 393224 | tf_op jit(solution)/shard_map/ppermute | solution.py:227
  13.5 7.7 %all-to-all-start = ((bf16[32,16,512]{2,1,0:T(8,128)(2,1)}), bf16[32,16,512]{2,1,0:T(8,128)(2,1)}, u32[]{:S(2)}, u32[]{:S(2)}) async-start(bf16[32,16,512]{2,1,0:T(8,128)(2,1)} %bitcast.10), calls=%async_computation | async-start | bytes 1048576 | tf_op jit(solution)/shard_map/all_to_all | solution.py:236
  23.5 2.0 %shard_map.109 = bf16[256,4096]{1,0:T(8,128)(2,1)} custom-call(s32[2]{0:T(128)S(1)} %pad_add_fusion.at_ref._, bf16[2,64,4096]{2,1,0:T(8,128)(2,1)S(1)} %copy-done, bf16[2,64,4096]{2,1,0:T(8,128)(2,1)S(1)} %copy-done.1, bf16[64,4096]{1,0:T(8,128)(2,1)S(1)} %copy-done.5, bf16[64,4096]{1,0:T(8,128)(2,1)S(1)} %copy-done.6), custom_call_target="tpu_custom_call" | custom-call | flops 400000000 | bytes 2097152 | tf_op jit(solution)/shard_map/pallas_call | solution.py:169
  25.5 2.5 %collective-permute-start = (bf16[256,4096]{1,0:T(8,128)(2,1)}, bf16[256,4096]{1,0:T(8,128)(2,1)}, u32[]{:S(2)}, u32[]{:S(2)}) collective-permute-start(bf16[256,4096]{1,0:T(8,128)(2,1)} %shard_map.109), channel_id=1, source_target_pairs={{0,1},{1,0},{2,3},{3,2},{4,5},{5,4},{6,7},{7,6},{8,9},{9,8},{10,11... | collective-permute-start | bytes 6291464 | tf_op jit(solution)/shard_map/ppermute | solution.py:247
  28.1 1.9 %collective-permute-start.2 = (f32[256]{0:T(256)S(1)}, f32[256]{0:T(256)S(1)}, u32[]{:S(2)}, u32[]{:S(2)}) collective-permute-start(f32[256]{0:T(256)S(1)} %copy-done.16), channel_id=1, source_target_pairs={{0,1},{1,0},{2,3},{3,2},{4,5},{5,4},{6,7},{7,6},{8,9},{9,8},{10,11... | collective-permute-start | bytes 3080 | tf_op jit(solution)/shard_map/ppermute | solution.py:239
  30.0 2.2 %collective-permute-done.2 = f32[256]{0:T(256)S(1)} collective-permute-done((f32[256]{0:T(256)S(1)}, f32[256]{0:T(256)S(1)}, u32[]{:S(2)}, u32[]{:S(2)}) %collective-permute-start.2) | collective-permute-done | bytes 1056 | tf_op jit(solution)/shard_map/ppermute | solution.py:239
  32.2 5.6 %all-to-all-done = bf16[32,16,512]{2,1,0:T(8,128)(2,1)} async-done(((bf16[32,16,512]{2,1,0:T(8,128)(2,1)}), bf16[32,16,512]{2,1,0:T(8,128)(2,1)}, u32[]{:S(2)}, u32[]{:S(2)}) %all-to-all-start) | async-done | bytes 524320 | tf_op jit(solution)/shard_map/all_to_all | solution.py:236
  37.8 2.3 %shard_map.111 = (bf16[328,512]{1,0:T(8,128)(2,1)S(1)}, bf16[328,512]{1,0:T(8,128)(2,1)S(1)}) custom-call(s32[2]{0:T(128)S(1)} %pad_add_fusion.at_ref._, bf16[512,512]{1,0:T(8,128)(2,1)} %bitcast.11.rows_ref, bf16[256,256]{1,0:T(8,128)(2,1)S(1)} %copy-done.11, bf16[256,256]{1,0:T(8,128)(2,1)S(1)} %collective-permute-done.1.other_ref, ...), custom_call_target="tpu_custom_call" | custom-call | flops 400000000 | bytes 2097152 | tf_op jit(solution)/shard_map/pallas_call | solution.py:169
  40.0 3.2 %collective-permute-start.3 = (bf16[328,512]{1,0:T(8,128)(2,1)S(1)}, bf16[328,512]{1,0:T(8,128)(2,1)S(1)}, u32[]{:S(2)}, u32[]{:S(2)}) collective-permute-start(bf16[328,512]{1,0:T(8,128)(2,1)S(1)} %get-tuple-element.11.refs_0_), channel_id=1, source_target_pairs={{0,2},{1,3},{2,4},{3,5},{4,6},{5,7},{6,8},{7,9},{8,10},{9,11},{10,... | collective-permute-start | bytes 1007624 | tf_op jit(solution)/shard_map/ppermute | solution.py:268
  43.2 3.8 %collective-permute-start.6 = (bf16[328,512]{1,0:T(8,128)(2,1)S(1)}, bf16[328,512]{1,0:T(8,128)(2,1)S(1)}, u32[]{:S(2)}, u32[]{:S(2)}) collective-permute-start(bf16[328,512]{1,0:T(8,128)(2,1)S(1)} %get-tuple-element.12.refs_1_), channel_id=1, source_target_pairs={{0,14},{1,15},{2,0},{3,1},{4,2},{5,3},{6,4},{7,5},{8,6},{9,7},{10,... | collective-permute-start | bytes 1007624 | tf_op jit(solution)/shard_map/ppermute | solution.py:272
  47.1 3.4 %collective-permute-start.4 = (bf16[328,512]{1,0:T(8,128)(2,1)S(1)}, bf16[328,512]{1,0:T(8,128)(2,1)S(1)}, u32[]{:S(2)}, u32[]{:S(2)}) collective-permute-start(bf16[328,512]{1,0:T(8,128)(2,1)S(1)} %get-tuple-element.11.refs_0_), channel_id=1, source_target_pairs={{0,14},{1,15},{2,0},{3,1},{4,2},{5,3},{6,4},{7,5},{8,6},{9,7},{10,... | collective-permute-start | bytes 1007624 | tf_op jit(solution)/shard_map/ppermute | solution.py:272
  50.4 1.9 %collective-permute-start.5 = (bf16[328,512]{1,0:T(8,128)(2,1)S(1)}, bf16[328,512]{1,0:T(8,128)(2,1)S(1)}, u32[]{:S(2)}, u32[]{:S(2)}) collective-permute-start(bf16[328,512]{1,0:T(8,128)(2,1)S(1)} %get-tuple-element.12.refs_1_), channel_id=1, source_target_pairs={{0,2},{1,3},{2,4},{3,5},{4,6},{5,7},{6,8},{7,9},{8,10},{9,11},{10,... | collective-permute-start | bytes 1007624 | tf_op jit(solution)/shard_map/ppermute | solution.py:268
  52.4 1.9 %collective-permute-start.7 = (bf16[328,512]{1,0:T(8,128)(2,1)S(1)}, bf16[328,512]{1,0:T(8,128)(2,1)S(1)}, u32[]{:S(2)}, u32[]{:S(2)}) collective-permute-start(bf16[328,512]{1,0:T(8,128)(2,1)S(1)} %collective-permute-done.3.refs_2_), channel_id=1, source_target_pairs={{0,2},{1,3},{2,4},{3,5},{4,6},{5,7},{6,8},{7,9},{8,10},{9,11},{10,... | collective-permute-start | bytes 1007624 | tf_op jit(solution)/shard_map/ppermute | solution.py:268
  54.3 4.6 %collective-permute-start.10 = (bf16[328,512]{1,0:T(8,128)(2,1)S(1)}, bf16[328,512]{1,0:T(8,128)(2,1)S(1)}, u32[]{:S(2)}, u32[]{:S(2)}) collective-permute-start(bf16[328,512]{1,0:T(8,128)(2,1)S(1)} %collective-permute-done.6.refs_5_), channel_id=1, source_target_pairs={{0,14},{1,15},{2,0},{3,1},{4,2},{5,3},{6,4},{7,5},{8,6},{9,7},{10,... | collective-permute-start | bytes 1007624 | tf_op jit(solution)/shard_map/ppermute | solution.py:272
  59.3 5.3 %collective-permute-start.8 = (bf16[328,512]{1,0:T(8,128)(2,1)S(1)}, bf16[328,512]{1,0:T(8,128)(2,1)S(1)}, u32[]{:S(2)}, u32[]{:S(2)}) collective-permute-start(bf16[328,512]{1,0:T(8,128)(2,1)S(1)} %collective-permute-done.4.refs_3_), channel_id=1, source_target_pairs={{0,14},{1,15},{2,0},{3,1},{4,2},{5,3},{6,4},{7,5},{8,6},{9,7},{10,... | collective-permute-start | bytes 1007624 | tf_op jit(solution)/shard_map/ppermute | solution.py:272
  64.6 1.9 %collective-permute-start.9 = (bf16[328,512]{1,0:T(8,128)(2,1)S(1)}, bf16[328,512]{1,0:T(8,128)(2,1)S(1)}, u32[]{:S(2)}, u32[]{:S(2)}) collective-permute-start(bf16[328,512]{1,0:T(8,128)(2,1)S(1)} %collective-permute-done.5.refs_4_), channel_id=1, source_target_pairs={{0,2},{1,3},{2,4},{3,5},{4,6},{5,7},{6,8},{7,9},{8,10},{9,11},{10,... | collective-permute-start | bytes 1007624 | tf_op jit(solution)/shard_map/ppermute | solution.py:268
  67.2 1.9 %collective-permute-start.11 = (bf16[328,512]{1,0:T(8,128)(2,1)S(1)}, bf16[328,512]{1,0:T(8,128)(2,1)S(1)}, u32[]{:S(2)}, u32[]{:S(2)}) collective-permute-start(bf16[328,512]{1,0:T(8,128)(2,1)S(1)} %collective-permute-done.7.refs_6_), channel_id=1, source_target_pairs={{0,2},{1,3},{2,4},{3,5},{4,6},{5,7},{6,8},{7,9},{8,10},{9,11},{10,... | collective-permute-start | bytes 1007624 | tf_op jit(solution)/shard_map/ppermute | solution.py:268
  69.1 4.6 %collective-permute-start.14 = (bf16[328,512]{1,0:T(8,128)(2,1)S(1)}, bf16[328,512]{1,0:T(8,128)(2,1)S(1)}, u32[]{:S(2)}, u32[]{:S(2)}) collective-permute-start(bf16[328,512]{1,0:T(8,128)(2,1)S(1)} %collective-permute-done.10.refs_9_), channel_id=1, source_target_pairs={{0,14},{1,15},{2,0},{3,1},{4,2},{5,3},{6,4},{7,5},{8,6},{9,7},{10,... | collective-permute-start | bytes 1007624 | tf_op jit(solution)/shard_map/ppermute | solution.py:272
  73.8 5.3 %collective-permute-start.12 = (bf16[328,512]{1,0:T(8,128)(2,1)S(1)}, bf16[328,512]{1,0:T(8,128)(2,1)S(1)}, u32[]{:S(2)}, u32[]{:S(2)}) collective-permute-start(bf16[328,512]{1,0:T(8,128)(2,1)S(1)} %collective-permute-done.8.refs_7_), channel_id=1, source_target_pairs={{0,14},{1,15},{2,0},{3,1},{4,2},{5,3},{6,4},{7,5},{8,6},{9,7},{10,... | collective-permute-start | bytes 1007624 | tf_op jit(solution)/shard_map/ppermute | solution.py:272
  79.1 1.9 %collective-permute-start.13 = (bf16[328,512]{1,0:T(8,128)(2,1)S(1)}, bf16[328,512]{1,0:T(8,128)(2,1)S(1)}, u32[]{:S(2)}, u32[]{:S(2)}) collective-permute-start(bf16[328,512]{1,0:T(8,128)(2,1)S(1)} %collective-permute-done.9.refs_8_), channel_id=1, source_target_pairs={{0,2},{1,3},{2,4},{3,5},{4,6},{5,7},{6,8},{7,9},{8,10},{9,11},{10,... | collective-permute-start | bytes 1007624 | tf_op jit(solution)/shard_map/ppermute | solution.py:268
  81.0 2.4 %collective-permute-start.15 = (bf16[328,512]{1,0:T(8,128)(2,1)S(1)}, bf16[328,512]{1,0:T(8,128)(2,1)S(1)}, u32[]{:S(2)}, u32[]{:S(2)}) collective-permute-start(bf16[328,512]{1,0:T(8,128)(2,1)S(1)} %collective-permute-done.11.refs_10_), channel_id=1, source_target_pairs={{0,2},{1,3},{2,4},{3,5},{4,6},{5,7},{6,8},{7,9},{8,10},{9,11},{10,... | collective-permute-start | bytes 1007624 | tf_op jit(solution)/shard_map/ppermute | solution.py:268
  83.5 4.1 %collective-permute-start.16 = (bf16[328,512]{1,0:T(8,128)(2,1)S(1)}, bf16[328,512]{1,0:T(8,128)(2,1)S(1)}, u32[]{:S(2)}, u32[]{:S(2)}) collective-permute-start(bf16[328,512]{1,0:T(8,128)(2,1)S(1)} %collective-permute-done.14.refs_13_), channel_id=1, source_target_pairs={{0,14},{1,15},{2,0},{3,1},{4,2},{5,3},{6,4},{7,5},{8,6},{9,7},{10,... | collective-permute-start | bytes 1007624 | tf_op jit(solution)/shard_map/ppermute | solution.py:272
  88.3 3.7 %shard_map.112 = (f32[640,256]{1,0:T(8,128)S(1)}, f32[16,512]{1,0:T(8,128)S(1)}, bf16[256,512]{1,0:T(8,128)(2,1)S(1)}, bf16[256,512]{1,0:T(8,128)(2,1)S(1)}) custom-call(s32[2]{0:T(128)S(1)} %pad_add_fusion.at_ref._, bf16[2,64,4096]{2,1,0:T(8,128)(2,1)S(1)} %copy-done, bf16[2,64,4096]{2,1,0:T(8,128)(2,1)S(1)} %copy-done.2, bf16[64,4096]{1,0:T(8,128)(2,1)S(1)} %copy-done.5, ...), custom_call_target="tpu_custom_call" | custom-call | flops 1342177280 | bytes 2097152 | tf_op jit(solution)/shard_map/pallas_call | solution.py:169
  94.6 2.1 %shard_map.113 = bf16[8,640,128]{2,1,0:T(8,128)(2,1)} custom-call(s32[2]{0:T(128)S(1)} %pad_add_fusion.at_ref._, bf16[256,512]{1,0:T(8,128)(2,1)S(1)} %get-tuple-element.13.refs_0_, bf16[256,512]{1,0:T(8,128)(2,1)S(1)} %get-tuple-element.14.refs_1_, f32[640,256]{1,0:T(8,128)S(1)} %get-tuple-element.15.refs_2_, f32[16,512]{1,0:T(8,128)S(1)} %get-tuple-element.16.refs_3_, ...), custom_call_target="tpu_custom_call" | custom-call | flops 167772160 | bytes 2097152 | tf_op jit(solution)/shard_map/pallas_call | solution.py:169
  96.7 6.9 %all-to-all-start.1 = ((bf16[8,640,128]{2,1,0:T(8,128)(2,1)}), bf16[8,640,128]{2,1,0:T(8,128)(2,1)S(1)}, u32[]{:S(2)}, u32[]{:S(2)}) async-start(bf16[8,640,128]{2,1,0:T(8,128)(2,1)} %shard_map.113), calls=%async_computation.1 | async-start | bytes 2621440 | tf_op jit(solution)/shard_map/all_to_all | solution.py:298
  104.2 7.0 %collective-permute-start.17 = (bf16[2048,256]{1,0:T(8,128)(2,1)S(1)}, bf16[2048,256]{1,0:T(8,128)(2,1)S(1)}, u32[]{:S(2)}, u32[]{:S(2)}) collective-permute-start(bf16[2048,256]{1,0:T(8,128)(2,1)S(1)} %shard_map.114), channel_id=1, source_target_pairs={{0,1},{1,0},{2,3},{3,2},{4,5},{5,4},{6,7},{7,6},{8,9},{9,8},{10,11... | collective-permute-start | bytes 3145736 | tf_op jit(solution)/shard_map/ppermute | solution.py:255
  111.2 2.2 %collective-permute-done.17.got_ref = bf16[2048,256]{1,0:T(8,128)(2,1)S(1)} collective-permute-done((bf16[2048,256]{1,0:T(8,128)(2,1)S(1)}, bf16[2048,256]{1,0:T(8,128)(2,1)S(1)}, u32[]{:S(2)}, u32[]{:S(2)}) %collective-permute-start.17) | collective-permute-done | bytes 1048608 | tf_op jit(solution)/shard_map/ppermute | solution.py:255
  113.5 20.9 %all-to-all-done.1.hidden_ref = bf16[8,640,128]{2,1,0:T(8,128)(2,1)S(1)} async-done(((bf16[8,640,128]{2,1,0:T(8,128)(2,1)}), bf16[8,640,128]{2,1,0:T(8,128)(2,1)S(1)}, u32[]{:S(2)}, u32[]{:S(2)}) %all-to-all-start.1) | async-done | bytes 1310752 | tf_op jit(solution)/shard_map/all_to_all | solution.py:298
  136.4 6.5 %all-to-all-start.2 = ((bf16[32,16,512]{2,1,0:T(8,128)(2,1)}), bf16[32,16,512]{2,1,0:T(8,128)(2,1)S(1)}, u32[]{:S(2)}, u32[]{:S(2)}) async-start(bf16[32,16,512]{2,1,0:T(8,128)(2,1)} %bitcast.31), calls=%async_computation.2 | async-start | bytes 1048576 | tf_op jit(solution)/shard_map/all_to_all | solution.py:306
  144.3 11.5 %all-to-all-done.2 = bf16[32,16,512]{2,1,0:T(8,128)(2,1)S(1)} async-done(((bf16[32,16,512]{2,1,0:T(8,128)(2,1)}), bf16[32,16,512]{2,1,0:T(8,128)(2,1)S(1)}, u32[]{:S(2)}, u32[]{:S(2)}) %all-to-all-start.2) | async-done | bytes 524320 | tf_op jit(solution)/shard_map/all_to_all | solution.py:306
  158.0 8.3 %collective-permute-start.18 = (f32[256,256]{1,0:T(8,128)S(1)}, f32[256,256]{1,0:T(8,128)S(1)}, u32[]{:S(2)}, u32[]{:S(2)}) collective-permute-start(f32[256,256]{1,0:T(8,128)S(1)} %slice_select_fusion), channel_id=1, source_target_pairs={{0,1},{1,0},{2,3},{3,2},{4,5},{5,4},{6,7},{7,6},{8,9},{9,8},{10,11... | collective-permute-start | bytes 786440 | tf_op jit(solution)/shard_map/ppermute | solution.py:339
  167.6 10.1 %all_to_all.21 = f32[16,1,256]{2,1,0:T(1,128)S(1)} all-to-all(f32[16,1,256]{2,1,0:T(1,128)S(1)} %broadcast_in_dim.72), channel_id=1, replica_groups=mesh['ep'=32,'tp'=16] {'tp'}, dimensions={0} | all-to-all | bytes 32768 | tf_op jit(solution)/shard_map/all_to_all | solution.py:342
  (75 shorter events, 19.7 us)
Async XLA Ops:
  0.0 21.2 %copy-start = (bf16[2,64,4096]{2,1,0:T(8,128)(2,1)S(1)}, bf16[2,64,4096]{2,1,0:T(8,128)(2,1)}, u32[]{:S(2)}) copy-start(bf16[2,64,4096]{2,1,0:T(8,128)(2,1)} %gate.1) | copy-start | bytes 3145732
  0.0 21.2 %copy-start.5 = (bf16[64,4096]{1,0:T(8,128)(2,1)S(1)}, bf16[64,4096]{1,0:T(8,128)(2,1)}, u32[]{:S(2)}) copy-start(bf16[64,4096]{1,0:T(8,128)(2,1)} %s_gate.1) | copy-start | bytes 1572868
  0.0 10.1 %collective-permute-start.1 = (bf16[256,256]{1,0:T(8,128)(2,1)}, bf16[256,256]{1,0:T(8,128)(2,1)S(1)}, u32[]{:S(2)}, u32[]{:S(2)}) collective-permute-start(bf16[256,256]{1,0:T(8,128)(2,1)} %own_ref.4), channel_id=1, source_target_pairs={{0,1},{1,0},{2,3},{3,2},{4,5},{5,4},{6,7},{7,6},{8,9},{9,8},{10,11... | collective-permute-start | bytes 393224 | tf_op jit(solution)/shard_map/ppermute | solution.py:227
  13.5 24.3 %all-to-all-start = ((bf16[32,16,512]{2,1,0:T(8,128)(2,1)}), bf16[32,16,512]{2,1,0:T(8,128)(2,1)}, u32[]{:S(2)}, u32[]{:S(2)}) async-start(bf16[32,16,512]{2,1,0:T(8,128)(2,1)} %bitcast.10), calls=%async_computation | async-start | bytes 1048576 | tf_op jit(solution)/shard_map/all_to_all | solution.py:236
  23.5 14.3 %copy-start.11 = (bf16[256,256]{1,0:T(8,128)(2,1)S(1)}, bf16[256,256]{1,0:T(8,128)(2,1)}, u32[]{:S(2)}) copy-start(bf16[256,256]{1,0:T(8,128)(2,1)} %own_ref.4) | copy-start | bytes 393220
  23.5 64.9 %copy-start.2 = (bf16[2,64,4096]{2,1,0:T(8,128)(2,1)S(1)}, bf16[2,64,4096]{2,1,0:T(8,128)(2,1)}, u32[]{:S(2)}) copy-start(bf16[2,64,4096]{2,1,0:T(8,128)(2,1)} %up.1) | copy-start | bytes 3145732
  23.5 64.9 %copy-start.7 = (bf16[64,4096]{1,0:T(8,128)(2,1)S(1)}, bf16[64,4096]{1,0:T(8,128)(2,1)}, u32[]{:S(2)}) copy-start(bf16[64,4096]{1,0:T(8,128)(2,1)} %s_up.1) | copy-start | bytes 1572868
  25.5 62.0 %collective-permute-start = (bf16[256,4096]{1,0:T(8,128)(2,1)}, bf16[256,4096]{1,0:T(8,128)(2,1)}, u32[]{:S(2)}, u32[]{:S(2)}) collective-permute-start(bf16[256,4096]{1,0:T(8,128)(2,1)} %shard_map.109), channel_id=1, source_target_pairs={{0,1},{1,0},{2,3},{3,2},{4,5},{5,4},{6,7},{7,6},{8,9},{9,8},{10,11... | collective-permute-start | bytes 6291464 | tf_op jit(solution)/shard_map/ppermute | solution.py:247
  28.1 4.1 %collective-permute-start.2 = (f32[256]{0:T(256)S(1)}, f32[256]{0:T(256)S(1)}, u32[]{:S(2)}, u32[]{:S(2)}) collective-permute-start(f32[256]{0:T(256)S(1)} %copy-done.16), channel_id=1, source_target_pairs={{0,1},{1,0},{2,3},{3,2},{4,5},{5,4},{6,7},{7,6},{8,9},{9,8},{10,11... | collective-permute-start | bytes 3080 | tf_op jit(solution)/shard_map/ppermute | solution.py:239
  40.0 12.3 %collective-permute-start.3 = (bf16[328,512]{1,0:T(8,128)(2,1)S(1)}, bf16[328,512]{1,0:T(8,128)(2,1)S(1)}, u32[]{:S(2)}, u32[]{:S(2)}) collective-permute-start(bf16[328,512]{1,0:T(8,128)(2,1)S(1)} %get-tuple-element.11.refs_0_), channel_id=1, source_target_pairs={{0,2},{1,3},{2,4},{3,5},{4,6},{5,7},{6,8},{7,9},{8,10},{9,11},{10,... | collective-permute-start | bytes 1007624 | tf_op jit(solution)/shard_map/ppermute | solution.py:268
  43.2 11.1 %collective-permute-start.6 = (bf16[328,512]{1,0:T(8,128)(2,1)S(1)}, bf16[328,512]{1,0:T(8,128)(2,1)S(1)}, u32[]{:S(2)}, u32[]{:S(2)}) collective-permute-start(bf16[328,512]{1,0:T(8,128)(2,1)S(1)} %get-tuple-element.12.refs_1_), channel_id=1, source_target_pairs={{0,14},{1,15},{2,0},{3,1},{4,2},{5,3},{6,4},{7,5},{8,6},{9,7},{10,... | collective-permute-start | bytes 1007624 | tf_op jit(solution)/shard_map/ppermute | solution.py:272
  47.1 12.3 %collective-permute-start.4 = (bf16[328,512]{1,0:T(8,128)(2,1)S(1)}, bf16[328,512]{1,0:T(8,128)(2,1)S(1)}, u32[]{:S(2)}, u32[]{:S(2)}) collective-permute-start(bf16[328,512]{1,0:T(8,128)(2,1)S(1)} %get-tuple-element.11.refs_0_), channel_id=1, source_target_pairs={{0,14},{1,15},{2,0},{3,1},{4,2},{5,3},{6,4},{7,5},{8,6},{9,7},{10,... | collective-permute-start | bytes 1007624 | tf_op jit(solution)/shard_map/ppermute | solution.py:272
  50.4 14.2 %collective-permute-start.5 = (bf16[328,512]{1,0:T(8,128)(2,1)S(1)}, bf16[328,512]{1,0:T(8,128)(2,1)S(1)}, u32[]{:S(2)}, u32[]{:S(2)}) collective-permute-start(bf16[328,512]{1,0:T(8,128)(2,1)S(1)} %get-tuple-element.12.refs_1_), channel_id=1, source_target_pairs={{0,2},{1,3},{2,4},{3,5},{4,6},{5,7},{6,8},{7,9},{8,10},{9,11},{10,... | collective-permute-start | bytes 1007624 | tf_op jit(solution)/shard_map/ppermute | solution.py:268
  52.4 14.8 %collective-permute-start.7 = (bf16[328,512]{1,0:T(8,128)(2,1)S(1)}, bf16[328,512]{1,0:T(8,128)(2,1)S(1)}, u32[]{:S(2)}, u32[]{:S(2)}) collective-permute-start(bf16[328,512]{1,0:T(8,128)(2,1)S(1)} %collective-permute-done.3.refs_2_), channel_id=1, source_target_pairs={{0,2},{1,3},{2,4},{3,5},{4,6},{5,7},{6,8},{7,9},{8,10},{9,11},{10,... | collective-permute-start | bytes 1007624 | tf_op jit(solution)/shard_map/ppermute | solution.py:268
  54.3 14.8 %collective-permute-start.10 = (bf16[328,512]{1,0:T(8,128)(2,1)S(1)}, bf16[328,512]{1,0:T(8,128)(2,1)S(1)}, u32[]{:S(2)}, u32[]{:S(2)}) collective-permute-start(bf16[328,512]{1,0:T(8,128)(2,1)S(1)} %collective-permute-done.6.refs_5_), channel_id=1, source_target_pairs={{0,14},{1,15},{2,0},{3,1},{4,2},{5,3},{6,4},{7,5},{8,6},{9,7},{10,... | collective-permute-start | bytes 1007624 | tf_op jit(solution)/shard_map/ppermute | solution.py:272
  59.3 14.4 %collective-permute-start.8 = (bf16[328,512]{1,0:T(8,128)(2,1)S(1)}, bf16[328,512]{1,0:T(8,128)(2,1)S(1)}, u32[]{:S(2)}, u32[]{:S(2)}) collective-permute-start(bf16[328,512]{1,0:T(8,128)(2,1)S(1)} %collective-permute-done.4.refs_3_), channel_id=1, source_target_pairs={{0,14},{1,15},{2,0},{3,1},{4,2},{5,3},{6,4},{7,5},{8,6},{9,7},{10,... | collective-permute-start | bytes 1007624 | tf_op jit(solution)/shard_map/ppermute | solution.py:272
  64.6 14.4 %collective-permute-start.9 = (bf16[328,512]{1,0:T(8,128)(2,1)S(1)}, bf16[328,512]{1,0:T(8,128)(2,1)S(1)}, u32[]{:S(2)}, u32[]{:S(2)}) collective-permute-start(bf16[328,512]{1,0:T(8,128)(2,1)S(1)} %collective-permute-done.5.refs_4_), channel_id=1, source_target_pairs={{0,2},{1,3},{2,4},{3,5},{4,6},{5,7},{6,8},{7,9},{8,10},{9,11},{10,... | collective-permute-start | bytes 1007624 | tf_op jit(solution)/shard_map/ppermute | solution.py:268
  67.2 13.8 %collective-permute-start.11 = (bf16[328,512]{1,0:T(8,128)(2,1)S(1)}, bf16[328,512]{1,0:T(8,128)(2,1)S(1)}, u32[]{:S(2)}, u32[]{:S(2)}) collective-permute-start(bf16[328,512]{1,0:T(8,128)(2,1)S(1)} %collective-permute-done.7.refs_6_), channel_id=1, source_target_pairs={{0,2},{1,3},{2,4},{3,5},{4,6},{5,7},{6,8},{7,9},{8,10},{9,11},{10,... | collective-permute-start | bytes 1007624 | tf_op jit(solution)/shard_map/ppermute | solution.py:268
  69.1 14.4 %collective-permute-start.14 = (bf16[328,512]{1,0:T(8,128)(2,1)S(1)}, bf16[328,512]{1,0:T(8,128)(2,1)S(1)}, u32[]{:S(2)}, u32[]{:S(2)}) collective-permute-start(bf16[328,512]{1,0:T(8,128)(2,1)S(1)} %collective-permute-done.10.refs_9_), channel_id=1, source_target_pairs={{0,14},{1,15},{2,0},{3,1},{4,2},{5,3},{6,4},{7,5},{8,6},{9,7},{10,... | collective-permute-start | bytes 1007624 | tf_op jit(solution)/shard_map/ppermute | solution.py:272
  73.8 13.8 %collective-permute-start.12 = (bf16[328,512]{1,0:T(8,128)(2,1)S(1)}, bf16[328,512]{1,0:T(8,128)(2,1)S(1)}, u32[]{:S(2)}, u32[]{:S(2)}) collective-permute-start(bf16[328,512]{1,0:T(8,128)(2,1)S(1)} %collective-permute-done.8.refs_7_), channel_id=1, source_target_pairs={{0,14},{1,15},{2,0},{3,1},{4,2},{5,3},{6,4},{7,5},{8,6},{9,7},{10,... | collective-permute-start | bytes 1007624 | tf_op jit(solution)/shard_map/ppermute | solution.py:272
  79.1 9.2 %collective-permute-start.13 = (bf16[328,512]{1,0:T(8,128)(2,1)S(1)}, bf16[328,512]{1,0:T(8,128)(2,1)S(1)}, u32[]{:S(2)}, u32[]{:S(2)}) collective-permute-start(bf16[328,512]{1,0:T(8,128)(2,1)S(1)} %collective-permute-done.9.refs_8_), channel_id=1, source_target_pairs={{0,2},{1,3},{2,4},{3,5},{4,6},{5,7},{6,8},{7,9},{8,10},{9,11},{10,... | collective-permute-start | bytes 1007624 | tf_op jit(solution)/shard_map/ppermute | solution.py:268
  81.0 12.7 %collective-permute-start.15 = (bf16[328,512]{1,0:T(8,128)(2,1)S(1)}, bf16[328,512]{1,0:T(8,128)(2,1)S(1)}, u32[]{:S(2)}, u32[]{:S(2)}) collective-permute-start(bf16[328,512]{1,0:T(8,128)(2,1)S(1)} %collective-permute-done.11.refs_10_), channel_id=1, source_target_pairs={{0,2},{1,3},{2,4},{3,5},{4,6},{5,7},{6,8},{7,9},{8,10},{9,11},{10,... | collective-permute-start | bytes 1007624 | tf_op jit(solution)/shard_map/ppermute | solution.py:268
  83.5 11.1 %collective-permute-start.16 = (bf16[328,512]{1,0:T(8,128)(2,1)S(1)}, bf16[328,512]{1,0:T(8,128)(2,1)S(1)}, u32[]{:S(2)}, u32[]{:S(2)}) collective-permute-start(bf16[328,512]{1,0:T(8,128)(2,1)S(1)} %collective-permute-done.14.refs_13_), channel_id=1, source_target_pairs={{0,14},{1,15},{2,0},{3,1},{4,2},{5,3},{6,4},{7,5},{8,6},{9,7},{10,... | collective-permute-start | bytes 1007624 | tf_op jit(solution)/shard_map/ppermute | solution.py:272
  96.7 6.9 %copy-start.3 = (bf16[2,1024,256]{2,1,0:T(8,128)(2,1)S(1)}, bf16[2,1024,256]{2,1,0:T(8,128)(2,1)}, u32[]{:S(2)}) copy-start(bf16[2,1024,256]{2,1,0:T(8,128)(2,1)} %own_ref.5) | copy-start | bytes 3145732
  96.7 6.9 %copy-start.8 = (bf16[1024,256]{1,0:T(8,128)(2,1)S(1)}, bf16[1024,256]{1,0:T(8,128)(2,1)}, u32[]{:S(2)}) copy-start(bf16[1024,256]{1,0:T(8,128)(2,1)} %refs_1_.3) | copy-start | bytes 1572868
  96.7 14.5 %copy-start.13 = (s32[256,3]{0,1:T(4,128)S(1)}, s32[256,3]{0,1:T(4,128)}, u32[]{:S(2)}) copy-start(s32[256,3]{0,1:T(4,128)} %param.13) | copy-start | bytes 9220
  96.7 37.6 %all-to-all-start.1 = ((bf16[8,640,128]{2,1,0:T(8,128)(2,1)}), bf16[8,640,128]{2,1,0:T(8,128)(2,1)S(1)}, u32[]{:S(2)}, u32[]{:S(2)}) async-start(bf16[8,640,128]{2,1,0:T(8,128)(2,1)} %shard_map.113), calls=%async_computation.1 | async-start | bytes 2621440 | tf_op jit(solution)/shard_map/all_to_all | solution.py:298
  104.2 9.2 %collective-permute-start.17 = (bf16[2048,256]{1,0:T(8,128)(2,1)S(1)}, bf16[2048,256]{1,0:T(8,128)(2,1)S(1)}, u32[]{:S(2)}, u32[]{:S(2)}) collective-permute-start(bf16[2048,256]{1,0:T(8,128)(2,1)S(1)} %shard_map.114), channel_id=1, source_target_pairs={{0,1},{1,0},{2,3},{3,2},{4,5},{5,4},{6,7},{7,6},{8,9},{9,8},{10,11... | collective-permute-start | bytes 3145736 | tf_op jit(solution)/shard_map/ppermute | solution.py:255
  111.2 31.6 %copy-start.14 = (f32[256,3]{0,1:T(4,128)S(1)}, f32[256,3]{0,1:T(4,128)}, u32[]{:S(2)}) copy-start(f32[256,3]{0,1:T(4,128)} %param.14) | copy-start | bytes 9220
  136.4 19.4 %all-to-all-start.2 = ((bf16[32,16,512]{2,1,0:T(8,128)(2,1)}), bf16[32,16,512]{2,1,0:T(8,128)(2,1)S(1)}, u32[]{:S(2)}, u32[]{:S(2)}) async-start(bf16[32,16,512]{2,1,0:T(8,128)(2,1)} %bitcast.31), calls=%async_computation.2 | async-start | bytes 1048576 | tf_op jit(solution)/shard_map/all_to_all | solution.py:306
  157.3 20.4 %copy-start.15 = (f32[256]{0:T(256)S(1)}, f32[256]{0:T(256)}, u32[]{:S(2)}) copy-start(f32[256]{0:T(256)} %param.21) | copy-start | bytes 3076
  158.0 9.5 %collective-permute-start.18 = (f32[256,256]{1,0:T(8,128)S(1)}, f32[256,256]{1,0:T(8,128)S(1)}, u32[]{:S(2)}, u32[]{:S(2)}) collective-permute-start(f32[256,256]{1,0:T(8,128)S(1)} %slice_select_fusion), channel_id=1, source_target_pairs={{0,1},{1,0},{2,3},{3,2},{4,5},{5,4},{6,7},{7,6},{8,9},{9,8},{10,11... | collective-permute-start | bytes 786440 | tf_op jit(solution)/shard_map/ppermute | solution.py:339
  (8 other events, 17.0 us)

commit v4 on v3

--- a/solution.py
+++ b/solution.py
@@ -29,7 +29,7 @@
     return high, middle, (rest - middle.astype(F32)).astype(BF)
 
 
-def picks(ids, core, n_ep, cap):
+def picks(ids, core, n_ep, cap, weight=None):
     tok = ids.shape[1]
     named = 2 * lax.broadcasted_iota(jnp.int32, (n_ep, tok), 0) + core
     member = ids[0:1, :] == named
@@ -41,7 +41,35 @@
     rank = jnp.where(member, rank, -1.0)
     spread = jnp.broadcast_to(rank[:, None, :], (n_ep, cap, tok))
     slot = lax.broadcasted_iota(jnp.int32, (n_ep, cap, tok), 1).astype(F32)
-    return jnp.where(spread == slot, 1.0, 0.0).astype(BF).reshape(n_ep * cap, tok)
+    if weight is None:
+        return jnp.where(spread == slot, 1.0, 0.0).astype(BF).reshape(n_ep * cap, tok)
+    value = jnp.where(ids[0:1, :] == named, weight[0:1, :], 0.0)
+    for k in range(1, ids.shape[0]):
+        value = value + jnp.where(ids[k : k + 1, :] == named, weight[k : k + 1, :], 0.0)
+    value = jnp.broadcast_to(value[:, None, :], (n_ep, cap, tok))
+    return jnp.where(spread == slot, value, 0.0).reshape(n_ep * cap, tok)
+
+
+def mix_kernel(n_ep, cap, at_ref, ids_ref, weight_ref, *out_refs):
+    mix = picks(ids_ref[...], at_ref[0], n_ep, cap, weight_ref[...]).T
+    for ref, value in zip(out_refs, thirds(mix)):
+        ref[...] = value
+
+
+def combine_kernel(at_ref, high, middle, low, rows_ref, shared_ref, home_ref, away_ref):
+    core = at_ref[0]
+    rows = rows_ref[...]
+    part = jnp.dot(high[...], rows, preferred_element_type=F32)
+    part = part + jnp.dot(middle[...], rows, preferred_element_type=F32)
+    part = part + jnp.dot(low[...], rows, preferred_element_type=F32)
+    shared = shared_ref[...]
+    half, feat = shared.shape[0], home_ref.shape[1]
+    top = part[:half] + jnp.where(core == 0, shared, 0.0)
+    bottom = part[half:] + jnp.where(core == 0, 0.0, shared)
+    for at, value in ((slice(0, half), top), (slice(half, 2 * half), bottom)):
+        left, right = value[:, :feat], value[:, feat:]
+        home_ref[at, :] = jnp.where(core == 0, left, right)
+        away_ref[at, :] = jnp.where(core == 0, right, left)
 
 
 def route_kernel(n_ep, cap, at_ref, ids_ref, own_ref, other_ref, out_ref):
@@ -231,7 +259,7 @@
         jax.ShapeDtypeStruct((slots, width), BF),
         (place, ids, tokens, partner),
         10**8,
-        8,
+        60,
     )
     arrived = lax.all_to_all(outgoing.reshape(n_ep, cap, width), "ep", 0, 0, tiled=True)
     arrived = arrived.reshape(slots, width)
@@ -309,33 +337,18 @@
     sdown_w = own_first(shared_down, got_out[n_hid:], 1).reshape(n_y, 2 * hid, width)
     contract = (((0, 2), (0, 1)), ((), ()))
     shared_out = lax.dot_general(hidden_all[:, slots:], sdown_w, contract, preferred_element_type=F32)
-    named = 2 * jnp.arange(n_ep, dtype=jnp.int32)[:, None] + core
-    hit = [(ids[k][None, :] == named) for k in range(top)]
-    member = hit[0] | hit[1] | hit[2]
-    earlier = (
-        jnp.arange(tok, dtype=jnp.int32)[:, None] < jnp.arange(tok, dtype=jnp.int32)[None, :]
-    ).astype(BF)
-    rank = jnp.dot(member.astype(BF), earlier, preferred_element_type=F32)
-    rank = jnp.where(member, rank, -1.0)
-    slot_no = jnp.arange(cap, dtype=jnp.int32).astype(F32)
-    pick = rank[:, None, :] == slot_no[None, :, None]
-    weight = sum(jnp.where(hit[k], route_weight.T[k][None, :], 0.0) for k in range(top))
-    mix = jnp.where(pick, weight[:, None, :], 0.0).reshape(slots, tok)
-    high = lax.reduce_precision(mix, 8, 7)
-    middle = lax.reduce_precision(mix - high, 8, 7)
-    low = mix - high - middle
-    part = sum(
-        lax.dot_general(m.astype(BF), returned, (((0,), (0,)), ((), ())), preferred_element_type=F32)
-        for m in (high, middle, low)
-    )
-    zero = jnp.zeros_like(shared_out)
-    part = part + jnp.where(
-        first,
-        jnp.concatenate([shared_out, zero], axis=0),
-        jnp.concatenate([zero, shared_out], axis=0),
-    )
-    away = jnp.where(first, part[:, feat:], part[:, :feat])
-    home = jnp.where(first, part[:, :feat], part[:, feat:])
+    third = jax.ShapeDtypeStruct((tok, slots), BF)
+    mix = call(
+        functools.partial(mix_kernel, n_ep, cap),
+        (third, third, third),
+        (place, ids, route_weight.T),
+        4 * 10**8,
+        8,
+    )
+    value = jax.ShapeDtypeStruct((tok, feat), F32)
+    home, away = call(
+        combine_kernel, (value, value), (place, *mix, returned, shared_out), 6 * tok * slots * width, 8
+    )
     summed = home + lax.ppermute(away, "tp", swap)
     own_square = jnp.sum(summed * summed, axis=1)
     sent = jnp.broadcast_to(own_square[None, :], (n_tp, tok))

time: 180 us -> 179 us (level)
  waiting for transfers between devices: 49.1 us -> 45 us
  Pallas kernels: 13.8 us -> 16.3 us
  local copies, waits for them, and re-layouts: 5.09 us -> 7.54 us
  matrix products: 3.01 us -> 1.09 us
    all_to_all x1, waiting for transfers between devices: 11.5 us -> 8.72 us  [body(): lax.all_to_all(expert_out.reshape(n_ep, cap, width), 'ep', 0, 0, tiled=True)]
    unnamed x36 -> x52, local copies, waits for them, and re-layouts: 5.03 us -> 7.49 us
    pallas_call x7 -> x9, Pallas kernels: 13.8 us -> 16.3 us  [call(): pl.pallas_call(kernel, out_shape=out, in_specs=[SMEM] + [VMEM] * (len(arg...]
    dot_general x4 -> x0, matrix products: 1.94 us -> none  [the longest x3 1.75 us: body(): lax.dot_general(m.astype(BF), returned, (((0,), (0,)), ((), ())), preferr...]
where the time goes in v4:
time: 179 us; the launch traced here: 178 us
  starting transfers between devices  95.8 us (54%)
  waiting for transfers between devices  45 us (25%)
  Pallas kernels  16.3 us (9%)
  blocking collectives  10.1 us (6%)
  local copies, waits for them, and re-layouts  7.54 us (4%)
    ppermute x7, starting transfers between devices, body(): bwd[k] = lax.ppermute(bwd[k], 'tp', y_shift(-1))  31 us
    all_to_all x1, waiting for transfers between devices, body(): lax.all_to_all(hidden, 'tp', 0, 0, axis_index_groups=y_groups, tiled=True)  20.8 us
    pallas_call x9, Pallas kernels, call(): pl.pallas_call(kernel, out_shape=out, in_specs=[SMEM] + [VMEM] * (len(arg...  16.3 us
    ppermute x7, starting transfers between devices, body(): fwd[k] = lax.ppermute(fwd[k], 'tp', y_shift(1))  15.2 us
    all_to_all x1, blocking collectives, body(): out_square = jnp.sum(lax.all_to_all(sent, 'tp', 0, 0, tiled=True), axis=0)  10.1 us
    ppermute x1, starting transfers between devices, body(): partner = lax.ppermute(tokens, 'tp', swap)  8.87 us
    all_to_all x1, waiting for transfers between devices, body(): lax.all_to_all(expert_out.reshape(n_ep, cap, width), 'ep', 0, 0, tiled=True)  8.72 us
    ppermute x1, starting transfers between devices, body(): summed = home + lax.ppermute(away, 'tp', swap)  8.31 us
  transfers between devices with their start and end apart: 22, of which 13 were waited for; matrix products, arithmetic and copies ran while one was open for 1% of the time, Pallas kernels for 5%

profile of v4, /device:TPU:1, one launch (start us, length us, event | category | flops | bytes accessed | tf_op | source)
XLA Modules:
  0.0 177.9 jit_solution(13439344002022450705)
XLA Ops:
  0.0 8.9 %collective-permute-start.1 = (bf16[256,256]{1,0:T(8,128)(2,1)}, bf16[256,256]{1,0:T(8,128)(2,1)S(1)}, u32[]{:S(2)}, u32[]{:S(2)}) collective-permute-start(bf16[256,256]{1,0:T(8,128)(2,1)} %own_ref.4), channel_id=1, source_target_pairs={{0,1},{1,0},{2,3},{3,2},{4,5},{5,4},{6,7},{7,6},{8,9},{9,8},{10,11... | collective-permute-start | bytes 393224 | tf_op jit(solution)/shard_map/ppermute | solution.py:255
  10.7 2.3 %shard_map.111 = bf16[512,512]{1,0:T(8,128)(2,1)} custom-call(s32[2]{0:T(128)} %pad_add_fusion.at_ref._, s32[3,256]{1,0:T(4,128)} %bitcast.17, bf16[256,256]{1,0:T(8,128)(2,1)} %own_ref.4, bf16[256,256]{1,0:T(8,128)(2,1)} %copy-done.18), custom_call_target="tpu_custom_call" | custom-call | flops 100000000 | bytes 2097152 | tf_op jit(solution)/shard_map/pallas_call | solution.py:197
  13.0 7.7 %all-to-all-start = ((bf16[32,16,512]{2,1,0:T(8,128)(2,1)}), bf16[32,16,512]{2,1,0:T(8,128)(2,1)}, u32[]{:S(2)}, u32[]{:S(2)}) async-start(bf16[32,16,512]{2,1,0:T(8,128)(2,1)} %bitcast.20), calls=%async_computation | async-start | bytes 1048576 | tf_op jit(solution)/shard_map/all_to_all | solution.py:264
  23.7 2.0 %shard_map.110 = bf16[256,4096]{1,0:T(8,128)(2,1)} custom-call(s32[2]{0:T(128)S(1)} %copy-done.20, bf16[2,64,4096]{2,1,0:T(8,128)(2,1)S(1)} %copy-done, bf16[2,64,4096]{2,1,0:T(8,128)(2,1)S(1)} %copy-done.1, bf16[64,4096]{1,0:T(8,128)(2,1)S(1)} %copy-done.5, bf16[64,4096]{1,0:T(8,128)(2,1)S(1)} %copy-done.6), custom_call_target="tpu_custom_call" | custom-call | flops 400000000 | bytes 2097152 | tf_op jit(solution)/shard_map/pallas_call | solution.py:197
  25.7 2.5 %collective-permute-start = (bf16[256,4096]{1,0:T(8,128)(2,1)}, bf16[256,4096]{1,0:T(8,128)(2,1)}, u32[]{:S(2)}, u32[]{:S(2)}) collective-permute-start(bf16[256,4096]{1,0:T(8,128)(2,1)} %shard_map.110), channel_id=1, source_target_pairs={{0,1},{1,0},{2,3},{3,2},{4,5},{5,4},{6,7},{7,6},{8,9},{9,8},{10,11... | collective-permute-start | bytes 6291464 | tf_op jit(solution)/shard_map/ppermute | solution.py:275
  28.3 1.9 %collective-permute-start.2 = (f32[256]{0:T(256)S(1)}, f32[256]{0:T(256)S(1)}, u32[]{:S(2)}, u32[]{:S(2)}) collective-permute-start(f32[256]{0:T(256)S(1)} %copy-done.25), channel_id=1, source_target_pairs={{0,1},{1,0},{2,3},{3,2},{4,5},{5,4},{6,7},{7,6},{8,9},{9,8},{10,11... | collective-permute-start | bytes 3080 | tf_op jit(solution)/shard_map/ppermute | solution.py:267
  30.2 2.2 %collective-permute-done.2 = f32[256]{0:T(256)S(1)} collective-permute-done((f32[256]{0:T(256)S(1)}, f32[256]{0:T(256)S(1)}, u32[]{:S(2)}, u32[]{:S(2)}) %collective-permute-start.2) | collective-permute-done | bytes 1056 | tf_op jit(solution)/shard_map/ppermute | solution.py:267
  32.4 4.9 %all-to-all-done = bf16[32,16,512]{2,1,0:T(8,128)(2,1)} async-done(((bf16[32,16,512]{2,1,0:T(8,128)(2,1)}), bf16[32,16,512]{2,1,0:T(8,128)(2,1)}, u32[]{:S(2)}, u32[]{:S(2)}) %all-to-all-start) | async-done | bytes 524320 | tf_op jit(solution)/shard_map/all_to_all | solution.py:264
  37.3 2.3 %shard_map.112 = (bf16[328,512]{1,0:T(8,128)(2,1)S(1)}, bf16[328,512]{1,0:T(8,128)(2,1)S(1)}) custom-call(s32[2]{0:T(128)S(1)} %copy-done.21, bf16[512,512]{1,0:T(8,128)(2,1)} %bitcast.5.rows_ref, bf16[256,256]{1,0:T(8,128)(2,1)S(1)} %copy-done.17, bf16[256,256]{1,0:T(8,128)(2,1)S(1)} %copy-done.19, f32[1,512]{1,0:T(1,128)S(1)} %broadcast_select_fusion.gain_ref), custom_call_target="tpu_custom_call" | custom-call | flops 400000000 | bytes 2097152 | tf_op jit(solution)/shard_map/pallas_call | solution.py:197
  39.6 3.2 %collective-permute-start.3 = (bf16[328,512]{1,0:T(8,128)(2,1)S(1)}, bf16[328,512]{1,0:T(8,128)(2,1)S(1)}, u32[]{:S(2)}, u32[]{:S(2)}) collective-permute-start(bf16[328,512]{1,0:T(8,128)(2,1)S(1)} %get-tuple-element.19.refs_0_), channel_id=1, source_target_pairs={{0,2},{1,3},{2,4},{3,5},{4,6},{5,7},{6,8},{7,9},{8,10},{9,11},{10,... | collective-permute-start | bytes 1007624 | tf_op jit(solution)/shard_map/ppermute | solution.py:296
  42.8 3.8 %collective-permute-start.6 = (bf16[328,512]{1,0:T(8,128)(2,1)S(1)}, bf16[328,512]{1,0:T(8,128)(2,1)S(1)}, u32[]{:S(2)}, u32[]{:S(2)}) collective-permute-start(bf16[328,512]{1,0:T(8,128)(2,1)S(1)} %get-tuple-element.20.refs_1_), channel_id=1, source_target_pairs={{0,14},{1,15},{2,0},{3,1},{4,2},{5,3},{6,4},{7,5},{8,6},{9,7},{10,... | collective-permute-start | bytes 1007624 | tf_op jit(solution)/shard_map/ppermute | solution.py:300
  46.6 3.4 %collective-permute-start.4 = (bf16[328,512]{1,0:T(8,128)(2,1)S(1)}, bf16[328,512]{1,0:T(8,128)(2,1)S(1)}, u32[]{:S(2)}, u32[]{:S(2)}) collective-permute-start(bf16[328,512]{1,0:T(8,128)(2,1)S(1)} %get-tuple-element.19.refs_0_), channel_id=1, source_target_pairs={{0,14},{1,15},{2,0},{3,1},{4,2},{5,3},{6,4},{7,5},{8,6},{9,7},{10,... | collective-permute-start | bytes 1007624 | tf_op jit(solution)/shard_map/ppermute | solution.py:300
  50.0 1.9 %collective-permute-start.5 = (bf16[328,512]{1,0:T(8,128)(2,1)S(1)}, bf16[328,512]{1,0:T(8,128)(2,1)S(1)}, u32[]{:S(2)}, u32[]{:S(2)}) collective-permute-start(bf16[328,512]{1,0:T(8,128)(2,1)S(1)} %get-tuple-element.20.refs_1_), channel_id=1, source_target_pairs={{0,2},{1,3},{2,4},{3,5},{4,6},{5,7},{6,8},{7,9},{8,10},{9,11},{10,... | collective-permute-start | bytes 1007624 | tf_op jit(solution)/shard_map/ppermute | solution.py:296
  51.9 1.9 %collective-permute-start.7 = (bf16[328,512]{1,0:T(8,128)(2,1)S(1)}, bf16[328,512]{1,0:T(8,128)(2,1)S(1)}, u32[]{:S(2)}, u32[]{:S(2)}) collective-permute-start(bf16[328,512]{1,0:T(8,128)(2,1)S(1)} %collective-permute-done.3.refs_2_), channel_id=1, source_target_pairs={{0,2},{1,3},{2,4},{3,5},{4,6},{5,7},{6,8},{7,9},{8,10},{9,11},{10,... | collective-permute-start | bytes 1007624 | tf_op jit(solution)/shard_map/ppermute | solution.py:296
  53.8 4.6 %collective-permute-start.10 = (bf16[328,512]{1,0:T(8,128)(2,1)S(1)}, bf16[328,512]{1,0:T(8,128)(2,1)S(1)}, u32[]{:S(2)}, u32[]{:S(2)}) collective-permute-start(bf16[328,512]{1,0:T(8,128)(2,1)S(1)} %collective-permute-done.6.refs_5_), channel_id=1, source_target_pairs={{0,14},{1,15},{2,0},{3,1},{4,2},{5,3},{6,4},{7,5},{8,6},{9,7},{10,... | collective-permute-start | bytes 1007624 | tf_op jit(solution)/shard_map/ppermute | solution.py:300
  58.9 5.3 %collective-permute-start.8 = (bf16[328,512]{1,0:T(8,128)(2,1)S(1)}, bf16[328,512]{1,0:T(8,128)(2,1)S(1)}, u32[]{:S(2)}, u32[]{:S(2)}) collective-permute-start(bf16[328,512]{1,0:T(8,128)(2,1)S(1)} %collective-permute-done.4.refs_3_), channel_id=1, source_target_pairs={{0,14},{1,15},{2,0},{3,1},{4,2},{5,3},{6,4},{7,5},{8,6},{9,7},{10,... | collective-permute-start | bytes 1007624 | tf_op jit(solution)/shard_map/ppermute | solution.py:300
  64.2 1.9 %collective-permute-start.9 = (bf16[328,512]{1,0:T(8,128)(2,1)S(1)}, bf16[328,512]{1,0:T(8,128)(2,1)S(1)}, u32[]{:S(2)}, u32[]{:S(2)}) collective-permute-start(bf16[328,512]{1,0:T(8,128)(2,1)S(1)} %collective-permute-done.5.refs_4_), channel_id=1, source_target_pairs={{0,2},{1,3},{2,4},{3,5},{4,6},{5,7},{6,8},{7,9},{8,10},{9,11},{10,... | collective-permute-start | bytes 1007624 | tf_op jit(solution)/shard_map/ppermute | solution.py:296
  68.6 4.6 %collective-permute-start.14 = (bf16[328,512]{1,0:T(8,128)(2,1)S(1)}, bf16[328,512]{1,0:T(8,128)(2,1)S(1)}, u32[]{:S(2)}, u32[]{:S(2)}) collective-permute-start(bf16[328,512]{1,0:T(8,128)(2,1)S(1)} %collective-permute-done.10.refs_9_), channel_id=1, source_target_pairs={{0,14},{1,15},{2,0},{3,1},{4,2},{5,3},{6,4},{7,5},{8,6},{9,7},{10,... | collective-permute-start | bytes 1007624 | tf_op jit(solution)/shard_map/ppermute | solution.py:300
  73.3 5.3 %collective-permute-start.12 = (bf16[328,512]{1,0:T(8,128)(2,1)S(1)}, bf16[328,512]{1,0:T(8,128)(2,1)S(1)}, u32[]{:S(2)}, u32[]{:S(2)}) collective-permute-start(bf16[328,512]{1,0:T(8,128)(2,1)S(1)} %collective-permute-done.8.refs_7_), channel_id=1, source_target_pairs={{0,14},{1,15},{2,0},{3,1},{4,2},{5,3},{6,4},{7,5},{8,6},{9,7},{10,... | collective-permute-start | bytes 1007624 | tf_op jit(solution)/shard_map/ppermute | solution.py:300
  78.6 1.9 %collective-permute-start.13 = (bf16[328,512]{1,0:T(8,128)(2,1)S(1)}, bf16[328,512]{1,0:T(8,128)(2,1)S(1)}, u32[]{:S(2)}, u32[]{:S(2)}) collective-permute-start(bf16[328,512]{1,0:T(8,128)(2,1)S(1)} %collective-permute-done.9.refs_8_), channel_id=1, source_target_pairs={{0,2},{1,3},{2,4},{3,5},{4,6},{5,7},{6,8},{7,9},{8,10},{9,11},{10,... | collective-permute-start | bytes 1007624 | tf_op jit(solution)/shard_map/ppermute | solution.py:296
  80.6 2.4 %collective-permute-start.15 = (bf16[328,512]{1,0:T(8,128)(2,1)S(1)}, bf16[328,512]{1,0:T(8,128)(2,1)S(1)}, u32[]{:S(2)}, u32[]{:S(2)}) collective-permute-start(bf16[328,512]{1,0:T(8,128)(2,1)S(1)} %collective-permute-done.11.refs_10_), channel_id=1, source_target_pairs={{0,2},{1,3},{2,4},{3,5},{4,6},{5,7},{6,8},{7,9},{8,10},{9,11},{10,... | collective-permute-start | bytes 1007624 | tf_op jit(solution)/shard_map/ppermute | solution.py:296
  83.0 4.1 %collective-permute-start.16 = (bf16[328,512]{1,0:T(8,128)(2,1)S(1)}, bf16[328,512]{1,0:T(8,128)(2,1)S(1)}, u32[]{:S(2)}, u32[]{:S(2)}) collective-permute-start(bf16[328,512]{1,0:T(8,128)(2,1)S(1)} %collective-permute-done.14.refs_13_), channel_id=1, source_target_pairs={{0,14},{1,15},{2,0},{3,1},{4,2},{5,3},{6,4},{7,5},{8,6},{9,7},{10,... | collective-permute-start | bytes 1007624 | tf_op jit(solution)/shard_map/ppermute | solution.py:300
  87.9 3.7 %shard_map.113 = (f32[640,256]{1,0:T(8,128)S(1)}, f32[16,512]{1,0:T(8,128)S(1)}, bf16[256,512]{1,0:T(8,128)(2,1)S(1)}, bf16[256,512]{1,0:T(8,128)(2,1)S(1)}) custom-call(s32[2]{0:T(128)S(1)} %copy-done.21, bf16[2,64,4096]{2,1,0:T(8,128)(2,1)S(1)} %copy-done, bf16[2,64,4096]{2,1,0:T(8,128)(2,1)S(1)} %copy-done.2, bf16[64,4096]{1,0:T(8,128)(2,1)S(1)} %copy-done.5, ...), custom_call_target="tpu_custom_call" | custom-call | flops 1342177280 | bytes 2097152 | tf_op jit(solution)/shard_map/pallas_call | solution.py:197
  94.2 2.1 %shard_map.114 = bf16[8,640,128]{2,1,0:T(8,128)(2,1)} custom-call(s32[2]{0:T(128)S(1)} %copy-done.21, bf16[256,512]{1,0:T(8,128)(2,1)S(1)} %get-tuple-element.21.refs_0_, bf16[256,512]{1,0:T(8,128)(2,1)S(1)} %get-tuple-element.22.refs_1_, f32[640,256]{1,0:T(8,128)S(1)} %get-tuple-element.23.refs_2_, f32[16,512]{1,0:T(8,128)S(1)} %get-tuple-element.24.refs_3_, ...), custom_call_target="tpu_custom_call" | custom-call | flops 167772160 | bytes 2097152 | tf_op jit(solution)/shard_map/pallas_call | solution.py:197
  96.3 6.9 %all-to-all-start.1 = ((bf16[8,640,128]{2,1,0:T(8,128)(2,1)}), bf16[8,640,128]{2,1,0:T(8,128)(2,1)S(1)}, u32[]{:S(2)}, u32[]{:S(2)}) async-start(bf16[8,640,128]{2,1,0:T(8,128)(2,1)} %shard_map.114), calls=%async_computation.1 | async-start | bytes 2621440 | tf_op jit(solution)/shard_map/all_to_all | solution.py:326
  103.8 7.0 %collective-permute-start.17 = (bf16[2048,256]{1,0:T(8,128)(2,1)S(1)}, bf16[2048,256]{1,0:T(8,128)(2,1)S(1)}, u32[]{:S(2)}, u32[]{:S(2)}) collective-permute-start(bf16[2048,256]{1,0:T(8,128)(2,1)S(1)} %shard_map.115), channel_id=1, source_target_pairs={{0,1},{1,0},{2,3},{3,2},{4,5},{5,4},{6,7},{7,6},{8,9},{9,8},{10,11... | collective-permute-start | bytes 3145736 | tf_op jit(solution)/shard_map/ppermute | solution.py:283
  110.7 2.3 %collective-permute-done.17.got_ref = bf16[2048,256]{1,0:T(8,128)(2,1)S(1)} collective-permute-done((bf16[2048,256]{1,0:T(8,128)(2,1)S(1)}, bf16[2048,256]{1,0:T(8,128)(2,1)S(1)}, u32[]{:S(2)}, u32[]{:S(2)}) %collective-permute-start.17) | collective-permute-done | bytes 1048608 | tf_op jit(solution)/shard_map/ppermute | solution.py:283
  113.0 20.8 %all-to-all-done.1.hidden_ref = bf16[8,640,128]{2,1,0:T(8,128)(2,1)S(1)} async-done(((bf16[8,640,128]{2,1,0:T(8,128)(2,1)}), bf16[8,640,128]{2,1,0:T(8,128)(2,1)S(1)}, u32[]{:S(2)}, u32[]{:S(2)}) %all-to-all-start.1) | async-done | bytes 1310752 | tf_op jit(solution)/shard_map/all_to_all | solution.py:326
  135.9 6.5 %all-to-all-start.2 = ((bf16[32,16,512]{2,1,0:T(8,128)(2,1)}), bf16[32,16,512]{2,1,0:T(8,128)(2,1)S(1)}, u32[]{:S(2)}, u32[]{:S(2)}) async-start(bf16[32,16,512]{2,1,0:T(8,128)(2,1)} %bitcast.14), calls=%async_computation.2 | async-start | bytes 1048576 | tf_op jit(solution)/shard_map/all_to_all | solution.py:334
  146.6 8.7 %all-to-all-done.2 = bf16[32,16,512]{2,1,0:T(8,128)(2,1)S(1)} async-done(((bf16[32,16,512]{2,1,0:T(8,128)(2,1)}), bf16[32,16,512]{2,1,0:T(8,128)(2,1)S(1)}, u32[]{:S(2)}, u32[]{:S(2)}) %all-to-all-start.2) | async-done | bytes 524320 | tf_op jit(solution)/shard_map/all_to_all | solution.py:334
  157.4 8.3 %collective-permute-start.18 = (f32[256,256]{1,0:T(8,128)S(1)}, f32[256,256]{1,0:T(8,128)S(1)}, u32[]{:S(2)}, u32[]{:S(2)}) collective-permute-start(f32[256,256]{1,0:T(8,128)S(1)} %get-tuple-element.26), channel_id=1, source_target_pairs={{0,1},{1,0},{2,3},{3,2},{4,5},{5,4},{6,7},{7,6},{8,9},{9,8},{10,11... | collective-permute-start | bytes 786440 | tf_op jit(solution)/shard_map/ppermute | solution.py:352
  167.0 10.1 %all_to_all.21 = f32[16,1,256]{2,1,0:T(1,128)S(1)} all-to-all(f32[16,1,256]{2,1,0:T(1,128)S(1)} %broadcast_in_dim.2), channel_id=1, replica_groups=mesh['ep'=32,'tp'=16] {'tp'}, dimensions={0} | all-to-all | bytes 32768 | tf_op jit(solution)/shard_map/all_to_all | solution.py:355
  (83 shorter events, 22.2 us)
Async XLA Ops:
  0.0 20.7 %copy-start = (bf16[2,64,4096]{2,1,0:T(8,128)(2,1)S(1)}, bf16[2,64,4096]{2,1,0:T(8,128)(2,1)}, u32[]{:S(2)}) copy-start(bf16[2,64,4096]{2,1,0:T(8,128)(2,1)} %gate.1) | copy-start | bytes 3145732
  0.0 20.7 %copy-start.5 = (bf16[64,4096]{1,0:T(8,128)(2,1)S(1)}, bf16[64,4096]{1,0:T(8,128)(2,1)}, u32[]{:S(2)}) copy-start(bf16[64,4096]{1,0:T(8,128)(2,1)} %s_gate.1) | copy-start | bytes 1572868
  0.0 10.1 %collective-permute-start.1 = (bf16[256,256]{1,0:T(8,128)(2,1)}, bf16[256,256]{1,0:T(8,128)(2,1)S(1)}, u32[]{:S(2)}, u32[]{:S(2)}) collective-permute-start(bf16[256,256]{1,0:T(8,128)(2,1)} %own_ref.4), channel_id=1, source_target_pairs={{0,1},{1,0},{2,3},{3,2},{4,5},{5,4},{6,7},{7,6},{8,9},{9,8},{10,11... | collective-permute-start | bytes 393224 | tf_op jit(solution)/shard_map/ppermute | solution.py:255
  13.0 24.3 %all-to-all-start = ((bf16[32,16,512]{2,1,0:T(8,128)(2,1)}), bf16[32,16,512]{2,1,0:T(8,128)(2,1)}, u32[]{:S(2)}, u32[]{:S(2)}) async-start(bf16[32,16,512]{2,1,0:T(8,128)(2,1)} %bitcast.20), calls=%async_computation | async-start | bytes 1048576 | tf_op jit(solution)/shard_map/all_to_all | solution.py:264
  23.7 13.6 %copy-start.17 = (bf16[256,256]{1,0:T(8,128)(2,1)S(1)}, bf16[256,256]{1,0:T(8,128)(2,1)}, u32[]{:S(2)}) copy-start(bf16[256,256]{1,0:T(8,128)(2,1)} %own_ref.4) | copy-start | bytes 393220
  23.7 13.6 %copy-start.19 = (bf16[256,256]{1,0:T(8,128)(2,1)S(1)}, bf16[256,256]{1,0:T(8,128)(2,1)}, u32[]{:S(2)}) copy-start(bf16[256,256]{1,0:T(8,128)(2,1)} %copy-done.18) | copy-start | bytes 393220
  23.7 13.6 %copy-start.21 = (s32[2]{0:T(128)S(1)}, s32[2]{0:T(128)}, u32[]{:S(2)}) copy-start(s32[2]{0:T(128)} %pad_add_fusion.at_ref._) | copy-start | bytes 28
  23.7 64.2 %copy-start.2 = (bf16[2,64,4096]{2,1,0:T(8,128)(2,1)S(1)}, bf16[2,64,4096]{2,1,0:T(8,128)(2,1)}, u32[]{:S(2)}) copy-start(bf16[2,64,4096]{2,1,0:T(8,128)(2,1)} %up.1) | copy-start | bytes 3145732
  23.7 64.2 %copy-start.7 = (bf16[64,4096]{1,0:T(8,128)(2,1)S(1)}, bf16[64,4096]{1,0:T(8,128)(2,1)}, u32[]{:S(2)}) copy-start(bf16[64,4096]{1,0:T(8,128)(2,1)} %s_up.1) | copy-start | bytes 1572868
  25.7 61.4 %collective-permute-start = (bf16[256,4096]{1,0:T(8,128)(2,1)}, bf16[256,4096]{1,0:T(8,128)(2,1)}, u32[]{:S(2)}, u32[]{:S(2)}) collective-permute-start(bf16[256,4096]{1,0:T(8,128)(2,1)} %shard_map.110), channel_id=1, source_target_pairs={{0,1},{1,0},{2,3},{3,2},{4,5},{5,4},{6,7},{7,6},{8,9},{9,8},{10,11... | collective-permute-start | bytes 6291464 | tf_op jit(solution)/shard_map/ppermute | solution.py:275
  28.3 4.1 %collective-permute-start.2 = (f32[256]{0:T(256)S(1)}, f32[256]{0:T(256)S(1)}, u32[]{:S(2)}, u32[]{:S(2)}) collective-permute-start(f32[256]{0:T(256)S(1)} %copy-done.25), channel_id=1, source_target_pairs={{0,1},{1,0},{2,3},{3,2},{4,5},{5,4},{6,7},{7,6},{8,9},{9,8},{10,11... | collective-permute-start | bytes 3080 | tf_op jit(solution)/shard_map/ppermute | solution.py:267
  39.6 12.3 %collective-permute-start.3 = (bf16[328,512]{1,0:T(8,128)(2,1)S(1)}, bf16[328,512]{1,0:T(8,128)(2,1)S(1)}, u32[]{:S(2)}, u32[]{:S(2)}) collective-permute-start(bf16[328,512]{1,0:T(8,128)(2,1)S(1)} %get-tuple-element.19.refs_0_), channel_id=1, source_target_pairs={{0,2},{1,3},{2,4},{3,5},{4,6},{5,7},{6,8},{7,9},{8,10},{9,11},{10,... | collective-permute-start | bytes 1007624 | tf_op jit(solution)/shard_map/ppermute | solution.py:296
  42.8 11.1 %collective-permute-start.6 = (bf16[328,512]{1,0:T(8,128)(2,1)S(1)}, bf16[328,512]{1,0:T(8,128)(2,1)S(1)}, u32[]{:S(2)}, u32[]{:S(2)}) collective-permute-start(bf16[328,512]{1,0:T(8,128)(2,1)S(1)} %get-tuple-element.20.refs_1_), channel_id=1, source_target_pairs={{0,14},{1,15},{2,0},{3,1},{4,2},{5,3},{6,4},{7,5},{8,6},{9,7},{10,... | collective-permute-start | bytes 1007624 | tf_op jit(solution)/shard_map/ppermute | solution.py:300
  46.6 12.3 %collective-permute-start.4 = (bf16[328,512]{1,0:T(8,128)(2,1)S(1)}, bf16[328,512]{1,0:T(8,128)(2,1)S(1)}, u32[]{:S(2)}, u32[]{:S(2)}) collective-permute-start(bf16[328,512]{1,0:T(8,128)(2,1)S(1)} %get-tuple-element.19.refs_0_), channel_id=1, source_target_pairs={{0,14},{1,15},{2,0},{3,1},{4,2},{5,3},{6,4},{7,5},{8,6},{9,7},{10,... | collective-permute-start | bytes 1007624 | tf_op jit(solution)/shard_map/ppermute | solution.py:300
  50.0 14.2 %collective-permute-start.5 = (bf16[328,512]{1,0:T(8,128)(2,1)S(1)}, bf16[328,512]{1,0:T(8,128)(2,1)S(1)}, u32[]{:S(2)}, u32[]{:S(2)}) collective-permute-start(bf16[328,512]{1,0:T(8,128)(2,1)S(1)} %get-tuple-element.20.refs_1_), channel_id=1, source_target_pairs={{0,2},{1,3},{2,4},{3,5},{4,6},{5,7},{6,8},{7,9},{8,10},{9,11},{10,... | collective-permute-start | bytes 1007624 | tf_op jit(solution)/shard_map/ppermute | solution.py:296
  51.9 14.8 %collective-permute-start.7 = (bf16[328,512]{1,0:T(8,128)(2,1)S(1)}, bf16[328,512]{1,0:T(8,128)(2,1)S(1)}, u32[]{:S(2)}, u32[]{:S(2)}) collective-permute-start(bf16[328,512]{1,0:T(8,128)(2,1)S(1)} %collective-permute-done.3.refs_2_), channel_id=1, source_target_pairs={{0,2},{1,3},{2,4},{3,5},{4,6},{5,7},{6,8},{7,9},{8,10},{9,11},{10,... | collective-permute-start | bytes 1007624 | tf_op jit(solution)/shard_map/ppermute | solution.py:296
  53.8 14.8 %collective-permute-start.10 = (bf16[328,512]{1,0:T(8,128)(2,1)S(1)}, bf16[328,512]{1,0:T(8,128)(2,1)S(1)}, u32[]{:S(2)}, u32[]{:S(2)}) collective-permute-start(bf16[328,512]{1,0:T(8,128)(2,1)S(1)} %collective-permute-done.6.refs_5_), channel_id=1, source_target_pairs={{0,14},{1,15},{2,0},{3,1},{4,2},{5,3},{6,4},{7,5},{8,6},{9,7},{10,... | collective-permute-start | bytes 1007624 | tf_op jit(solution)/shard_map/ppermute | solution.py:300
  58.9 14.4 %collective-permute-start.8 = (bf16[328,512]{1,0:T(8,128)(2,1)S(1)}, bf16[328,512]{1,0:T(8,128)(2,1)S(1)}, u32[]{:S(2)}, u32[]{:S(2)}) collective-permute-start(bf16[328,512]{1,0:T(8,128)(2,1)S(1)} %collective-permute-done.4.refs_3_), channel_id=1, source_target_pairs={{0,14},{1,15},{2,0},{3,1},{4,2},{5,3},{6,4},{7,5},{8,6},{9,7},{10,... | collective-permute-start | bytes 1007624 | tf_op jit(solution)/shard_map/ppermute | solution.py:300
  64.2 14.4 %collective-permute-start.9 = (bf16[328,512]{1,0:T(8,128)(2,1)S(1)}, bf16[328,512]{1,0:T(8,128)(2,1)S(1)}, u32[]{:S(2)}, u32[]{:S(2)}) collective-permute-start(bf16[328,512]{1,0:T(8,128)(2,1)S(1)} %collective-permute-done.5.refs_4_), channel_id=1, source_target_pairs={{0,2},{1,3},{2,4},{3,5},{4,6},{5,7},{6,8},{7,9},{8,10},{9,11},{10,... | collective-permute-start | bytes 1007624 | tf_op jit(solution)/shard_map/ppermute | solution.py:296
  66.7 13.8 %collective-permute-start.11 = (bf16[328,512]{1,0:T(8,128)(2,1)S(1)}, bf16[328,512]{1,0:T(8,128)(2,1)S(1)}, u32[]{:S(2)}, u32[]{:S(2)}) collective-permute-start(bf16[328,512]{1,0:T(8,128)(2,1)S(1)} %collective-permute-done.7.refs_6_), channel_id=1, source_target_pairs={{0,2},{1,3},{2,4},{3,5},{4,6},{5,7},{6,8},{7,9},{8,10},{9,11},{10,... | collective-permute-start | bytes 1007624 | tf_op jit(solution)/shard_map/ppermute | solution.py:296
  68.6 14.4 %collective-permute-start.14 = (bf16[328,512]{1,0:T(8,128)(2,1)S(1)}, bf16[328,512]{1,0:T(8,128)(2,1)S(1)}, u32[]{:S(2)}, u32[]{:S(2)}) collective-permute-start(bf16[328,512]{1,0:T(8,128)(2,1)S(1)} %collective-permute-done.10.refs_9_), channel_id=1, source_target_pairs={{0,14},{1,15},{2,0},{3,1},{4,2},{5,3},{6,4},{7,5},{8,6},{9,7},{10,... | collective-permute-start | bytes 1007624 | tf_op jit(solution)/shard_map/ppermute | solution.py:300
  73.3 13.8 %collective-permute-start.12 = (bf16[328,512]{1,0:T(8,128)(2,1)S(1)}, bf16[328,512]{1,0:T(8,128)(2,1)S(1)}, u32[]{:S(2)}, u32[]{:S(2)}) collective-permute-start(bf16[328,512]{1,0:T(8,128)(2,1)S(1)} %collective-permute-done.8.refs_7_), channel_id=1, source_target_pairs={{0,14},{1,15},{2,0},{3,1},{4,2},{5,3},{6,4},{7,5},{8,6},{9,7},{10,... | collective-permute-start | bytes 1007624 | tf_op jit(solution)/shard_map/ppermute | solution.py:300
  78.6 9.2 %collective-permute-start.13 = (bf16[328,512]{1,0:T(8,128)(2,1)S(1)}, bf16[328,512]{1,0:T(8,128)(2,1)S(1)}, u32[]{:S(2)}, u32[]{:S(2)}) collective-permute-start(bf16[328,512]{1,0:T(8,128)(2,1)S(1)} %collective-permute-done.9.refs_8_), channel_id=1, source_target_pairs={{0,2},{1,3},{2,4},{3,5},{4,6},{5,7},{6,8},{7,9},{8,10},{9,11},{10,... | collective-permute-start | bytes 1007624 | tf_op jit(solution)/shard_map/ppermute | solution.py:296
  80.6 12.7 %collective-permute-start.15 = (bf16[328,512]{1,0:T(8,128)(2,1)S(1)}, bf16[328,512]{1,0:T(8,128)(2,1)S(1)}, u32[]{:S(2)}, u32[]{:S(2)}) collective-permute-start(bf16[328,512]{1,0:T(8,128)(2,1)S(1)} %collective-permute-done.11.refs_10_), channel_id=1, source_target_pairs={{0,2},{1,3},{2,4},{3,5},{4,6},{5,7},{6,8},{7,9},{8,10},{9,11},{10,... | collective-permute-start | bytes 1007624 | tf_op jit(solution)/shard_map/ppermute | solution.py:296
  83.0 11.1 %collective-permute-start.16 = (bf16[328,512]{1,0:T(8,128)(2,1)S(1)}, bf16[328,512]{1,0:T(8,128)(2,1)S(1)}, u32[]{:S(2)}, u32[]{:S(2)}) collective-permute-start(bf16[328,512]{1,0:T(8,128)(2,1)S(1)} %collective-permute-done.14.refs_13_), channel_id=1, source_target_pairs={{0,14},{1,15},{2,0},{3,1},{4,2},{5,3},{6,4},{7,5},{8,6},{9,7},{10,... | collective-permute-start | bytes 1007624 | tf_op jit(solution)/shard_map/ppermute | solution.py:300
  96.3 37.6 %all-to-all-start.1 = ((bf16[8,640,128]{2,1,0:T(8,128)(2,1)}), bf16[8,640,128]{2,1,0:T(8,128)(2,1)S(1)}, u32[]{:S(2)}, u32[]{:S(2)}) async-start(bf16[8,640,128]{2,1,0:T(8,128)(2,1)} %shard_map.114), calls=%async_computation.1 | async-start | bytes 2621440 | tf_op jit(solution)/shard_map/all_to_all | solution.py:326
  103.7 38.6 %copy-start.22 = (s32[256,3]{0,1:T(4,128)S(1)}, s32[256,3]{0,1:T(4,128)}, u32[]{:S(2)}) copy-start(s32[256,3]{0,1:T(4,128)} %param.13) | copy-start | bytes 9220
  103.8 38.6 %copy-start.23 = (f32[256,3]{0,1:T(4,128)S(1)}, f32[256,3]{0,1:T(4,128)}, u32[]{:S(2)}) copy-start(f32[256,3]{0,1:T(4,128)} %param.14) | copy-start | bytes 9220
  103.8 9.2 %collective-permute-start.17 = (bf16[2048,256]{1,0:T(8,128)(2,1)S(1)}, bf16[2048,256]{1,0:T(8,128)(2,1)S(1)}, u32[]{:S(2)}, u32[]{:S(2)}) collective-permute-start(bf16[2048,256]{1,0:T(8,128)(2,1)S(1)} %shard_map.115), channel_id=1, source_target_pairs={{0,1},{1,0},{2,3},{3,2},{4,5},{5,4},{6,7},{7,6},{8,9},{9,8},{10,11... | collective-permute-start | bytes 3145736 | tf_op jit(solution)/shard_map/ppermute | solution.py:283
  135.9 19.4 %all-to-all-start.2 = ((bf16[32,16,512]{2,1,0:T(8,128)(2,1)}), bf16[32,16,512]{2,1,0:T(8,128)(2,1)S(1)}, u32[]{:S(2)}, u32[]{:S(2)}) async-start(bf16[32,16,512]{2,1,0:T(8,128)(2,1)} %bitcast.14), calls=%async_computation.2 | async-start | bytes 1048576 | tf_op jit(solution)/shard_map/all_to_all | solution.py:334
  146.6 30.6 %copy-start.24 = (f32[256]{0:T(256)S(1)}, f32[256]{0:T(256)}, u32[]{:S(2)}) copy-start(f32[256]{0:T(256)} %param.21) | copy-start | bytes 3076
  157.4 9.5 %collective-permute-start.18 = (f32[256,256]{1,0:T(8,128)S(1)}, f32[256,256]{1,0:T(8,128)S(1)}, u32[]{:S(2)}, u32[]{:S(2)}) collective-permute-start(f32[256,256]{1,0:T(8,128)S(1)} %get-tuple-element.26), channel_id=1, source_target_pairs={{0,1},{1,0},{2,3},{3,2},{4,5},{5,4},{6,7},{7,6},{8,9},{9,8},{10,11... | collective-permute-start | bytes 786440 | tf_op jit(solution)/shard_map/ppermute | solution.py:352
  (16 other events, 64.9 us)

commit v5 on v4

--- a/solution.py
+++ b/solution.py
@@ -15,11 +15,15 @@
 
 
 VMEM = pl.BlockSpec(memory_space=pltpu.VMEM)
-SMEM = pl.BlockSpec(memory_space=pltpu.SMEM)
 
 
 def times(x, w):
     return lax.dot_general(x, w, (((1,), (1,)), ((), ())), preferred_element_type=F32)
+
+
+def here():
+    tp = lax.axis_index("tp")
+    return lax.rem(tp, 2), lax.div(tp, 2)
 
 
 def thirds(v):
@@ -50,14 +54,14 @@
     return jnp.where(spread == slot, value, 0.0).reshape(n_ep * cap, tok)
 
 
-def mix_kernel(n_ep, cap, at_ref, ids_ref, weight_ref, *out_refs):
-    mix = picks(ids_ref[...], at_ref[0], n_ep, cap, weight_ref[...]).T
+def mix_kernel(n_ep, cap, ids_ref, weight_ref, *out_refs):
+    mix = picks(ids_ref[...], here()[0], n_ep, cap, weight_ref[...]).T
     for ref, value in zip(out_refs, thirds(mix)):
         ref[...] = value
 
 
-def combine_kernel(at_ref, high, middle, low, rows_ref, shared_ref, home_ref, away_ref):
-    core = at_ref[0]
+def combine_kernel(high, middle, low, rows_ref, shared_ref, home_ref, away_ref):
+    core, _ = here()
     rows = rows_ref[...]
     part = jnp.dot(high[...], rows, preferred_element_type=F32)
     part = part + jnp.dot(middle[...], rows, preferred_element_type=F32)
@@ -72,8 +76,8 @@
         away_ref[at, :] = jnp.where(core == 0, right, left)
 
 
-def route_kernel(n_ep, cap, at_ref, ids_ref, own_ref, other_ref, out_ref):
-    core = at_ref[0]
+def route_kernel(n_ep, cap, ids_ref, own_ref, other_ref, out_ref):
+    core, _ = here()
     one_hot = picks(ids_ref[...], core, n_ep, cap)
     feat = own_ref.shape[1]
     for ref, where in ((own_ref, core), (other_ref, 1 - core)):
@@ -81,8 +85,8 @@
         out_ref[:, at] = jnp.dot(one_hot, ref[...], preferred_element_type=F32).astype(BF)
 
 
-def arrive_kernel(at_ref, rows_ref, own_ref, other_ref, gain_ref, first_ref, second_ref):
-    core = at_ref[0]
+def arrive_kernel(rows_ref, own_ref, other_ref, gain_ref, first_ref, second_ref):
+    core, _ = here()
     slots, width = rows_ref.shape
     half, feat = own_ref.shape[0] // 2, own_ref.shape[1]
     n_sub = (slots + half) // 2
@@ -119,11 +123,11 @@
     spare(second_ref, 0, jnp.concatenate([sums, tail], axis=1))
 
 
-def early_kernel(places, spans, n_y, width, at_ref, gate, up, s_gate, s_up, got, *refs):
+def early_kernel(places, spans, n_y, width, gate, up, s_gate, s_up, got, *refs):
     n = len(places)
     pieces = refs[:n]
     total_ref, squares_ref, w_last, sw_last, w, sw = refs[n:]
-    core, y = at_ref[0], at_ref[1]
+    core, y = here()
     hid = s_gate.shape[0]
     n_sub = total_ref.shape[0] // 2
     own = pl.multiple_of(core * hid, hid)
@@ -135,7 +139,7 @@
         into[pl.ds(base + other, hid), :] = got[i * hid : (i + 1) * hid, :]
 
     def columns(offset):
-        return pl.ds(pl.multiple_of(lax.rem(y + offset + n_y, n_y) * width, width), width)
+        return pl.ds(pl.multiple_of(lax.rem(y + offset * (1 - 2 * core) + n_y, n_y) * width, width), width)
 
     for half in range(2):
         total = [None] * len(spans[half])
@@ -173,8 +177,8 @@
                 out_ref[j, rows, :] = hidden
 
 
-def down_kernel(at_ref, hidden_ref, own_ref, got_ref, out_ref):
-    core = at_ref[0]
+def down_kernel(hidden_ref, own_ref, got_ref, out_ref):
+    core, _ = here()
     feat = own_ref.shape[2]
     slots = out_ref.shape[0]
     hidden = jnp.concatenate([hidden_ref[j, :slots, :] for j in range(hidden_ref.shape[0])], axis=1)
@@ -185,11 +189,11 @@
         ).astype(BF)
 
 
-def pack_kernel(at_ref, *refs):
+def pack_kernel(*refs):
     arrays, out_ref = refs[:-1], refs[-1]
     rows = out_ref.shape[0] // len(arrays)
     for i, a in enumerate(arrays):
-        part = a.at[1 - at_ref[0]] if len(a.shape) == 3 else a
+        part = a.at[1 - here()[0]] if len(a.shape) == 3 else a
         out_ref[i * rows : (i + 1) * rows, :] = part[...]
 
 
@@ -197,7 +201,7 @@
     return pl.pallas_call(
         kernel,
         out_shape=out,
-        in_specs=[SMEM] + [VMEM] * (len(args) - 1),
+        in_specs=[VMEM] * len(args),
         out_specs=jax.tree.map(lambda _: VMEM, out),
         scratch_shapes=scratch,
         cost_estimate=pl.CostEstimate(flops=flops, bytes_accessed=2**21, transcendentals=0),
@@ -237,13 +241,12 @@
     core = lax.rem(tp, 2)
     y = lax.div(tp, 2)
     first = core == 0
-    place = jnp.stack([core, y]).astype(jnp.int32)
 
     swap = [(i, i ^ 1) for i in range(n_tp)]
     y_groups = [[c + 2 * k for k in range(n_y)] for c in range(2)]
 
     def y_shift(d):
-        return [(i, ((i // 2 + d) % n_y) * 2 + i % 2) for i in range(n_tp)]
+        return [(i, ((i // 2 + d * (1 - 2 * (i % 2))) % n_y) * 2 + i % 2) for i in range(n_tp)]
 
     def own_first(mine, other, axis):
         return jnp.where(
@@ -257,7 +260,7 @@
     outgoing = call(
         functools.partial(route_kernel, n_ep, cap),
         jax.ShapeDtypeStruct((slots, width), BF),
-        (place, ids, tokens, partner),
+        (ids, tokens, partner),
         10**8,
         60,
     )
@@ -268,7 +271,7 @@
     sent_in = call(
         pack_kernel,
         jax.ShapeDtypeStruct((4 * hid, feat_all), BF),
-        (place, expert_gate, expert_up, shared_gate, shared_up),
+        (expert_gate, expert_up, shared_gate, shared_up),
         4 * 10**8,
         8,
     )
@@ -276,14 +279,16 @@
     sent_out = call(
         pack_kernel,
         jax.ShapeDtypeStruct((2 * n_hid, feat), BF),
-        (place, expert_down, shared_down),
+        (expert_down, shared_down),
         4 * 10**8,
         6,
     )
     got_out = lax.ppermute(sent_out, "tp", swap)
 
     piece = jax.ShapeDtypeStruct((n_sub + SPARE, width), BF)
-    fwd = call(arrive_kernel, (piece, piece), (place, arrived, tokens, partner, gain), 4 * 10**8, 8)
+    fwd = call(
+        arrive_kernel, (piece, piece), (arrived, tokens, partner, gain), 4 * 10**8, 8
+    )
     fwd, bwd = list(fwd), list(fwd)
     spans = (((0, n_sub, 0),), ((0, slots - n_sub, 0), (slots - n_sub, n_sub, 1)))
     early, early_at = list(fwd), [(0, 0), (1, 0)]
@@ -310,15 +315,15 @@
             jax.ShapeDtypeStruct((4 * hid, width), BF),
             jax.ShapeDtypeStruct((4 * hid, width), BF),
         ),
-        (place, expert_gate, expert_up, shared_gate, shared_up, got_in, *early),
+        (expert_gate, expert_up, shared_gate, shared_up, got_in, *early),
         flops,
         20,
         [pltpu.VMEM((4 * hid, feat_all), BF), pltpu.VMEM((4 * hid, feat_all), BF)],
     )
     hidden = call(
-        lambda _, *refs: late_kernel(spans, feat_all, *refs),
+        functools.partial(late_kernel, spans, feat_all),
         jax.ShapeDtypeStruct((n_y, rows, 2 * hid), BF),
-        (place, w_last, sw_last, total, squares, *late),
+        (w_last, sw_last, total, squares, *late),
         flops // 8,
         8,
     )
@@ -327,7 +332,7 @@
     expert_out = call(
         down_kernel,
         jax.ShapeDtypeStruct((slots, width), BF),
-        (place, hidden_all, expert_down, got_out),
+        (hidden_all, expert_down, got_out),
         2 * slots * n_hid * width,
         12,
     )
@@ -341,13 +346,13 @@
     mix = call(
         functools.partial(mix_kernel, n_ep, cap),
         (third, third, third),
-        (place, ids, route_weight.T),
+        (ids, route_weight.T),
         4 * 10**8,
         8,
     )
     value = jax.ShapeDtypeStruct((tok, feat), F32)
     home, away = call(
-        combine_kernel, (value, value), (place, *mix, returned, shared_out), 6 * tok * slots * width, 8
+        combine_kernel, (value, value), (*mix, returned, shared_out), 6 * tok * slots * width, 8
     )
     summed = home + lax.ppermute(away, "tp", swap)
     own_square = jnp.sum(summed * summed, axis=1)

time: 179 us -> 180 us (level)
  waiting for transfers between devices: 45 us -> 60.4 us
  starting transfers between devices: 95.8 us -> 87.7 us
  Pallas kernels: 16.3 us -> 13 us
    ppermute x7, starting transfers between devices: 31 us -> 15.4 us  [body(): bwd[k] = lax.ppermute(bwd[k], 'tp', y_shift(-1))]
    ppermute x7, starting transfers between devices: 15.2 us -> 29.3 us  [body(): fwd[k] = lax.ppermute(fwd[k], 'tp', y_shift(1))]
    all_to_all x1, waiting for transfers between devices: 8.72 us -> 13.5 us  [body(): lax.all_to_all(expert_out.reshape(n_ep, cap, width), 'ep', 0, 0, tiled=True)]
    ppermute x7, waiting for transfers between devices: 1.48 us -> 6.11 us  [body(): bwd[k] = lax.ppermute(bwd[k], 'tp', y_shift(-1))]
    ppermute x1, starting transfers between devices: 8.31 us -> 4.15 us  [body(): summed = home + lax.ppermute(away, 'tp', swap)]
    all_to_all x1, waiting for transfers between devices: 20.8 us -> 24.8 us  [body(): lax.all_to_all(hidden, 'tp', 0, 0, axis_index_groups=y_groups, tiled=True)]
    pallas_call x9, Pallas kernels: 16.3 us -> 13 us  [call(): pl.pallas_call(kernel, out_shape=out, in_specs=[VMEM] * len(args), out_sp...]
    unnamed x52 -> x46, local copies, waits for them, and re-layouts: 7.49 us -> 5.9 us
  transfers between devices with their start and end apart: 22 -> 22, of which waited for: 13 -> 15; matrix products, arithmetic and copies ran while one was open for 1% -> 0% of each run, Pallas kernels for 5% -> 4%
where the time goes in v5:
time: 180 us; the launch traced here: 179 us
  starting transfers between devices  87.7 us (49%)
  waiting for transfers between devices  60.4 us (34%)
  Pallas kernels  13 us (7%)
  blocking collectives  10.1 us (6%)
  local copies, waits for them, and re-layouts  5.94 us (3%)
    ppermute x7, starting transfers between devices, body(): fwd[k] = lax.ppermute(fwd[k], 'tp', y_shift(1))  29.3 us
    all_to_all x1, waiting for transfers between devices, body(): lax.all_to_all(hidden, 'tp', 0, 0, axis_index_groups=y_groups, tiled=True)  24.8 us
    ppermute x7, starting transfers between devices, body(): bwd[k] = lax.ppermute(bwd[k], 'tp', y_shift(-1))  15.4 us
    all_to_all x1, waiting for transfers between devices, body(): lax.all_to_all(expert_out.reshape(n_ep, cap, width), 'ep', 0, 0, tiled=True)  13.5 us
    pallas_call x9, Pallas kernels, call(): pl.pallas_call(kernel, out_shape=out, in_specs=[VMEM] * len(args), out_sp...  13 us
    all_to_all x1, blocking collectives, body(): out_square = jnp.sum(lax.all_to_all(sent, 'tp', 0, 0, tiled=True), axis=0)  10.1 us
    ppermute x1, starting transfers between devices, body(): partner = lax.ppermute(tokens, 'tp', swap)  8.87 us
    all_to_all x1, starting transfers between devices, body(): lax.all_to_all(outgoing.reshape(n_ep, cap, width), 'ep', 0, 0, tiled=True)  7.67 us
  transfers between devices with their start and end apart: 22, of which 15 were waited for; matrix products, arithmetic and copies ran while one was open for 0% of the time, Pallas kernels for 4%

profile of v5, /device:TPU:1, one launch (start us, length us, event | category | flops | bytes accessed | tf_op | source)
XLA Modules:
  0.0 179.0 jit_solution(1554240570498546428)
XLA Ops:
  0.0 8.9 %collective-permute-start.1 = (bf16[256,256]{1,0:T(8,128)(2,1)}, bf16[256,256]{1,0:T(8,128)(2,1)S(1)}, u32[]{:S(2)}, u32[]{:S(2)}) collective-permute-start(bf16[256,256]{1,0:T(8,128)(2,1)} %own_ref.4), channel_id=1, source_target_pairs={{0,1},{1,0},{2,3},{3,2},{4,5},{5,4},{6,7},{7,6},{8,9},{9,8},{10,11... | collective-permute-start | bytes 393224 | tf_op jit(solution)/shard_map/ppermute | solution.py:258
  10.7 2.3 %shard_map.111 = bf16[512,512]{1,0:T(8,128)(2,1)} custom-call(s32[3,256]{1,0:T(4,128)} %bitcast.15, bf16[256,256]{1,0:T(8,128)(2,1)} %own_ref.4, bf16[256,256]{1,0:T(8,128)(2,1)} %copy-done.17), custom_call_target="tpu_custom_call" | custom-call | flops 100000000 | bytes 2097152 | tf_op jit(solution)/shard_map/pallas_call | solution.py:201
  13.0 7.7 %all-to-all-start = ((bf16[32,16,512]{2,1,0:T(8,128)(2,1)}), bf16[32,16,512]{2,1,0:T(8,128)(2,1)}, u32[]{:S(2)}, u32[]{:S(2)}) async-start(bf16[32,16,512]{2,1,0:T(8,128)(2,1)} %bitcast.18), calls=%async_computation | async-start | bytes 1048576 | tf_op jit(solution)/shard_map/all_to_all | solution.py:267
  24.5 2.5 %collective-permute-start = (bf16[256,4096]{1,0:T(8,128)(2,1)}, bf16[256,4096]{1,0:T(8,128)(2,1)}, u32[]{:S(2)}, u32[]{:S(2)}) collective-permute-start(bf16[256,4096]{1,0:T(8,128)(2,1)} %shard_map.110), channel_id=1, source_target_pairs={{0,1},{1,0},{2,3},{3,2},{4,5},{5,4},{6,7},{7,6},{8,9},{9,8},{10,11... | collective-permute-start | bytes 6291464 | tf_op jit(solution)/shard_map/ppermute | solution.py:278
  27.0 1.9 %collective-permute-start.2 = (f32[256]{0:T(256)S(1)}, f32[256]{0:T(256)S(1)}, u32[]{:S(2)}, u32[]{:S(2)}) collective-permute-start(f32[256]{0:T(256)S(1)} %copy-done.22), channel_id=1, source_target_pairs={{0,1},{1,0},{2,3},{3,2},{4,5},{5,4},{6,7},{7,6},{8,9},{9,8},{10,11... | collective-permute-start | bytes 3080 | tf_op jit(solution)/shard_map/ppermute | solution.py:270
  29.0 2.2 %collective-permute-done.2 = f32[256]{0:T(256)S(1)} collective-permute-done((f32[256]{0:T(256)S(1)}, f32[256]{0:T(256)S(1)}, u32[]{:S(2)}, u32[]{:S(2)}) %collective-permute-start.2) | collective-permute-done | bytes 1056 | tf_op jit(solution)/shard_map/ppermute | solution.py:270
  31.1 6.1 %all-to-all-done = bf16[32,16,512]{2,1,0:T(8,128)(2,1)} async-done(((bf16[32,16,512]{2,1,0:T(8,128)(2,1)}), bf16[32,16,512]{2,1,0:T(8,128)(2,1)}, u32[]{:S(2)}, u32[]{:S(2)}) %all-to-all-start) | async-done | bytes 524320 | tf_op jit(solution)/shard_map/all_to_all | solution.py:267
  37.3 2.3 %shard_map.112 = (bf16[328,512]{1,0:T(8,128)(2,1)S(1)}, bf16[328,512]{1,0:T(8,128)(2,1)S(1)}) custom-call(bf16[512,512]{1,0:T(8,128)(2,1)} %bitcast.3.rows_ref, bf16[256,256]{1,0:T(8,128)(2,1)S(1)} %copy-done.16, bf16[256,256]{1,0:T(8,128)(2,1)S(1)} %copy-done.18, f32[1,512]{1,0:T(1,128)S(1)} %broadcast_select_fusion.gain_ref), custom_call_target="tpu_custom_call" | custom-call | flops 400000000 | bytes 2097152 | tf_op jit(solution)/shard_map/pallas_call | solution.py:201
  39.5 5.1 %collective-permute-start.3 = (bf16[328,512]{1,0:T(8,128)(2,1)S(1)}, bf16[328,512]{1,0:T(8,128)(2,1)S(1)}, u32[]{:S(2)}, u32[]{:S(2)}) collective-permute-start(bf16[328,512]{1,0:T(8,128)(2,1)S(1)} %get-tuple-element.19.refs_0_), channel_id=1, source_target_pairs={{0,2},{1,15},{2,4},{3,1},{4,6},{5,3},{6,8},{7,5},{8,10},{9,7},{10,... | collective-permute-start | bytes 1007624 | tf_op jit(solution)/shard_map/ppermute | solution.py:301
  44.6 1.9 %collective-permute-start.6 = (bf16[328,512]{1,0:T(8,128)(2,1)S(1)}, bf16[328,512]{1,0:T(8,128)(2,1)S(1)}, u32[]{:S(2)}, u32[]{:S(2)}) collective-permute-start(bf16[328,512]{1,0:T(8,128)(2,1)S(1)} %get-tuple-element.20.refs_1_), channel_id=1, source_target_pairs={{0,14},{1,3},{2,0},{3,5},{4,2},{5,7},{6,4},{7,9},{8,6},{9,11},{10,... | collective-permute-start | bytes 1007624 | tf_op jit(solution)/shard_map/ppermute | solution.py:305
  46.6 1.9 %collective-permute-start.4 = (bf16[328,512]{1,0:T(8,128)(2,1)S(1)}, bf16[328,512]{1,0:T(8,128)(2,1)S(1)}, u32[]{:S(2)}, u32[]{:S(2)}) collective-permute-start(bf16[328,512]{1,0:T(8,128)(2,1)S(1)} %get-tuple-element.19.refs_0_), channel_id=1, source_target_pairs={{0,14},{1,3},{2,0},{3,5},{4,2},{5,7},{6,4},{7,9},{8,6},{9,11},{10,... | collective-permute-start | bytes 1007624 | tf_op jit(solution)/shard_map/ppermute | solution.py:305
  48.5 4.6 %collective-permute-start.5 = (bf16[328,512]{1,0:T(8,128)(2,1)S(1)}, bf16[328,512]{1,0:T(8,128)(2,1)S(1)}, u32[]{:S(2)}, u32[]{:S(2)}) collective-permute-start(bf16[328,512]{1,0:T(8,128)(2,1)S(1)} %get-tuple-element.20.refs_1_), channel_id=1, source_target_pairs={{0,2},{1,15},{2,4},{3,1},{4,6},{5,3},{6,8},{7,5},{8,10},{9,7},{10,... | collective-permute-start | bytes 1007624 | tf_op jit(solution)/shard_map/ppermute | solution.py:301
  53.1 3.4 %collective-permute-start.7 = (bf16[328,512]{1,0:T(8,128)(2,1)S(1)}, bf16[328,512]{1,0:T(8,128)(2,1)S(1)}, u32[]{:S(2)}, u32[]{:S(2)}) collective-permute-start(bf16[328,512]{1,0:T(8,128)(2,1)S(1)} %collective-permute-done.3.refs_2_), channel_id=1, source_target_pairs={{0,2},{1,15},{2,4},{3,1},{4,6},{5,3},{6,8},{7,5},{8,10},{9,7},{10,... | collective-permute-start | bytes 1007624 | tf_op jit(solution)/shard_map/ppermute | solution.py:301
  56.5 1.9 %collective-permute-start.10 = (bf16[328,512]{1,0:T(8,128)(2,1)S(1)}, bf16[328,512]{1,0:T(8,128)(2,1)S(1)}, u32[]{:S(2)}, u32[]{:S(2)}) collective-permute-start(bf16[328,512]{1,0:T(8,128)(2,1)S(1)} %collective-permute-done.6.refs_5_), channel_id=1, source_target_pairs={{0,14},{1,3},{2,0},{3,5},{4,2},{5,7},{6,4},{7,9},{8,6},{9,11},{10,... | collective-permute-start | bytes 1007624 | tf_op jit(solution)/shard_map/ppermute | solution.py:305
  58.7 3.1 %collective-permute-start.8 = (bf16[328,512]{1,0:T(8,128)(2,1)S(1)}, bf16[328,512]{1,0:T(8,128)(2,1)S(1)}, u32[]{:S(2)}, u32[]{:S(2)}) collective-permute-start(bf16[328,512]{1,0:T(8,128)(2,1)S(1)} %collective-permute-done.4.refs_3_), channel_id=1, source_target_pairs={{0,14},{1,3},{2,0},{3,5},{4,2},{5,7},{6,4},{7,9},{8,6},{9,11},{10,... | collective-permute-start | bytes 1007624 | tf_op jit(solution)/shard_map/ppermute | solution.py:305
  61.9 4.4 %collective-permute-start.9 = (bf16[328,512]{1,0:T(8,128)(2,1)S(1)}, bf16[328,512]{1,0:T(8,128)(2,1)S(1)}, u32[]{:S(2)}, u32[]{:S(2)}) collective-permute-start(bf16[328,512]{1,0:T(8,128)(2,1)S(1)} %collective-permute-done.5.refs_4_), channel_id=1, source_target_pairs={{0,2},{1,15},{2,4},{3,1},{4,6},{5,3},{6,8},{7,5},{8,10},{9,7},{10,... | collective-permute-start | bytes 1007624 | tf_op jit(solution)/shard_map/ppermute | solution.py:301
  66.8 4.6 %collective-permute-start.11 = (bf16[328,512]{1,0:T(8,128)(2,1)S(1)}, bf16[328,512]{1,0:T(8,128)(2,1)S(1)}, u32[]{:S(2)}, u32[]{:S(2)}) collective-permute-start(bf16[328,512]{1,0:T(8,128)(2,1)S(1)} %collective-permute-done.7.refs_6_), channel_id=1, source_target_pairs={{0,2},{1,15},{2,4},{3,1},{4,6},{5,3},{6,8},{7,5},{8,10},{9,7},{10,... | collective-permute-start | bytes 1007624 | tf_op jit(solution)/shard_map/ppermute | solution.py:301
  71.4 1.9 %collective-permute-start.14 = (bf16[328,512]{1,0:T(8,128)(2,1)S(1)}, bf16[328,512]{1,0:T(8,128)(2,1)S(1)}, u32[]{:S(2)}, u32[]{:S(2)}) collective-permute-start(bf16[328,512]{1,0:T(8,128)(2,1)S(1)} %collective-permute-done.10.refs_9_), channel_id=1, source_target_pairs={{0,14},{1,3},{2,0},{3,5},{4,2},{5,7},{6,4},{7,9},{8,6},{9,11},{10,... | collective-permute-start | bytes 1007624 | tf_op jit(solution)/shard_map/ppermute | solution.py:305
  74.1 2.6 %collective-permute-start.12 = (bf16[328,512]{1,0:T(8,128)(2,1)S(1)}, bf16[328,512]{1,0:T(8,128)(2,1)S(1)}, u32[]{:S(2)}, u32[]{:S(2)}) collective-permute-start(bf16[328,512]{1,0:T(8,128)(2,1)S(1)} %collective-permute-done.8.refs_7_), channel_id=1, source_target_pairs={{0,14},{1,3},{2,0},{3,5},{4,2},{5,7},{6,4},{7,9},{8,6},{9,11},{10,... | collective-permute-start | bytes 1007624 | tf_op jit(solution)/shard_map/ppermute | solution.py:305
  76.8 3.8 %collective-permute-start.13 = (bf16[328,512]{1,0:T(8,128)(2,1)S(1)}, bf16[328,512]{1,0:T(8,128)(2,1)S(1)}, u32[]{:S(2)}, u32[]{:S(2)}) collective-permute-start(bf16[328,512]{1,0:T(8,128)(2,1)S(1)} %collective-permute-done.9.refs_8_), channel_id=1, source_target_pairs={{0,2},{1,15},{2,4},{3,1},{4,6},{5,3},{6,8},{7,5},{8,10},{9,7},{10,... | collective-permute-start | bytes 1007624 | tf_op jit(solution)/shard_map/ppermute | solution.py:301
  80.7 3.5 %collective-permute-start.15 = (bf16[328,512]{1,0:T(8,128)(2,1)S(1)}, bf16[328,512]{1,0:T(8,128)(2,1)S(1)}, u32[]{:S(2)}, u32[]{:S(2)}) collective-permute-start(bf16[328,512]{1,0:T(8,128)(2,1)S(1)} %collective-permute-done.11.refs_10_), channel_id=1, source_target_pairs={{0,2},{1,15},{2,4},{3,1},{4,6},{5,3},{6,8},{7,5},{8,10},{9,7},{10,... | collective-permute-start | bytes 1007624 | tf_op jit(solution)/shard_map/ppermute | solution.py:301
  84.4 1.9 %collective-permute-start.16 = (bf16[328,512]{1,0:T(8,128)(2,1)S(1)}, bf16[328,512]{1,0:T(8,128)(2,1)S(1)}, u32[]{:S(2)}, u32[]{:S(2)}) collective-permute-start(bf16[328,512]{1,0:T(8,128)(2,1)S(1)} %collective-permute-done.14.refs_13_), channel_id=1, source_target_pairs={{0,14},{1,3},{2,0},{3,5},{4,2},{5,7},{6,4},{7,9},{8,6},{9,11},{10,... | collective-permute-start | bytes 1007624 | tf_op jit(solution)/shard_map/ppermute | solution.py:305
  88.6 3.7 %shard_map.113 = (f32[640,256]{1,0:T(8,128)S(1)}, f32[16,512]{1,0:T(8,128)S(1)}, bf16[256,512]{1,0:T(8,128)(2,1)S(1)}, bf16[256,512]{1,0:T(8,128)(2,1)S(1)}) custom-call(bf16[2,64,4096]{2,1,0:T(8,128)(2,1)S(1)} %copy-done, bf16[2,64,4096]{2,1,0:T(8,128)(2,1)S(1)} %copy-done.2, bf16[64,4096]{1,0:T(8,128)(2,1)S(1)} %copy-done.4, ...), custom_call_target="tpu_custom_call" | custom-call | flops 1342177280 | bytes 2097152 | tf_op jit(solution)/shard_map/pallas_call | solution.py:201
  94.0 3.4 %collective-permute-done.16.refs_1_ = bf16[328,512]{1,0:T(8,128)(2,1)S(1)} collective-permute-done((bf16[328,512]{1,0:T(8,128)(2,1)S(1)}, bf16[328,512]{1,0:T(8,128)(2,1)S(1)}, u32[]{:S(2)}, u32[]{:S(2)}) %collective-permute-start.16) | collective-permute-done | bytes 335904 | tf_op jit(solution)/shard_map/ppermute | solution.py:305
  98.9 5.8 %all-to-all-start.1 = ((bf16[8,640,128]{2,1,0:T(8,128)(2,1)}), bf16[8,640,128]{2,1,0:T(8,128)(2,1)S(1)}, u32[]{:S(2)}, u32[]{:S(2)}) async-start(bf16[8,640,128]{2,1,0:T(8,128)(2,1)} %shard_map.114), calls=%async_computation.1 | async-start | bytes 2621440 | tf_op jit(solution)/shard_map/all_to_all | solution.py:331
  104.9 5.4 %collective-permute-start.17 = (bf16[2048,256]{1,0:T(8,128)(2,1)S(1)}, bf16[2048,256]{1,0:T(8,128)(2,1)S(1)}, u32[]{:S(2)}, u32[]{:S(2)}) collective-permute-start(bf16[2048,256]{1,0:T(8,128)(2,1)S(1)} %shard_map.115), channel_id=1, source_target_pairs={{0,1},{1,0},{2,3},{3,2},{4,5},{5,4},{6,7},{7,6},{8,9},{9,8},{10,11... | collective-permute-start | bytes 3145736 | tf_op jit(solution)/shard_map/ppermute | solution.py:286
  110.3 2.3 %collective-permute-done.17.got_ref = bf16[2048,256]{1,0:T(8,128)(2,1)S(1)} collective-permute-done((bf16[2048,256]{1,0:T(8,128)(2,1)S(1)}, bf16[2048,256]{1,0:T(8,128)(2,1)S(1)}, u32[]{:S(2)}, u32[]{:S(2)}) %collective-permute-start.17) | collective-permute-done | bytes 1048608 | tf_op jit(solution)/shard_map/ppermute | solution.py:286
  112.5 24.8 %all-to-all-done.1.hidden_ref = bf16[8,640,128]{2,1,0:T(8,128)(2,1)S(1)} async-done(((bf16[8,640,128]{2,1,0:T(8,128)(2,1)}), bf16[8,640,128]{2,1,0:T(8,128)(2,1)S(1)}, u32[]{:S(2)}, u32[]{:S(2)}) %all-to-all-start.1) | async-done | bytes 1310752 | tf_op jit(solution)/shard_map/all_to_all | solution.py:331
  138.8 6.7 %all-to-all-start.2 = ((bf16[32,16,512]{2,1,0:T(8,128)(2,1)}), bf16[32,16,512]{2,1,0:T(8,128)(2,1)S(1)}, u32[]{:S(2)}, u32[]{:S(2)}) async-start(bf16[32,16,512]{2,1,0:T(8,128)(2,1)} %bitcast.13), calls=%async_computation.2 | async-start | bytes 1048576 | tf_op jit(solution)/shard_map/all_to_all | solution.py:339
  148.5 13.5 %all-to-all-done.2 = bf16[32,16,512]{2,1,0:T(8,128)(2,1)S(1)} async-done(((bf16[32,16,512]{2,1,0:T(8,128)(2,1)}), bf16[32,16,512]{2,1,0:T(8,128)(2,1)S(1)}, u32[]{:S(2)}, u32[]{:S(2)}) %all-to-all-start.2) | async-done | bytes 524320 | tf_op jit(solution)/shard_map/all_to_all | solution.py:339
  162.6 4.2 %collective-permute-start.18 = (f32[256,256]{1,0:T(8,128)S(1)}, f32[256,256]{1,0:T(8,128)S(1)}, u32[]{:S(2)}, u32[]{:S(2)}) collective-permute-start(f32[256,256]{1,0:T(8,128)S(1)} %get-tuple-element.26), channel_id=1, source_target_pairs={{0,1},{1,0},{2,3},{3,2},{4,5},{5,4},{6,7},{7,6},{8,9},{9,8},{10,11... | collective-permute-start | bytes 786440 | tf_op jit(solution)/shard_map/ppermute | solution.py:357
  168.0 10.1 %all_to_all.21 = f32[16,1,256]{2,1,0:T(1,128)S(1)} all-to-all(f32[16,1,256]{2,1,0:T(1,128)S(1)} %broadcast_in_dim.2), channel_id=1, replica_groups=mesh['ep'=32,'tp'=16] {'tp'}, dimensions={0} | all-to-all | bytes 32768 | tf_op jit(solution)/shard_map/all_to_all | solution.py:360
  (76 shorter events, 20.2 us)
Async XLA Ops:
  0.0 20.7 %copy-start = (bf16[2,64,4096]{2,1,0:T(8,128)(2,1)S(1)}, bf16[2,64,4096]{2,1,0:T(8,128)(2,1)}, u32[]{:S(2)}) copy-start(bf16[2,64,4096]{2,1,0:T(8,128)(2,1)} %gate.1) | copy-start | bytes 3145732
  0.0 20.7 %copy-start.4 = (bf16[64,4096]{1,0:T(8,128)(2,1)S(1)}, bf16[64,4096]{1,0:T(8,128)(2,1)}, u32[]{:S(2)}) copy-start(bf16[64,4096]{1,0:T(8,128)(2,1)} %s_gate.1) | copy-start | bytes 1572868
  0.0 10.1 %collective-permute-start.1 = (bf16[256,256]{1,0:T(8,128)(2,1)}, bf16[256,256]{1,0:T(8,128)(2,1)S(1)}, u32[]{:S(2)}, u32[]{:S(2)}) collective-permute-start(bf16[256,256]{1,0:T(8,128)(2,1)} %own_ref.4), channel_id=1, source_target_pairs={{0,1},{1,0},{2,3},{3,2},{4,5},{5,4},{6,7},{7,6},{8,9},{9,8},{10,11... | collective-permute-start | bytes 393224 | tf_op jit(solution)/shard_map/ppermute | solution.py:258
  13.0 24.3 %all-to-all-start = ((bf16[32,16,512]{2,1,0:T(8,128)(2,1)}), bf16[32,16,512]{2,1,0:T(8,128)(2,1)}, u32[]{:S(2)}, u32[]{:S(2)}) async-start(bf16[32,16,512]{2,1,0:T(8,128)(2,1)} %bitcast.18), calls=%async_computation | async-start | bytes 1048576 | tf_op jit(solution)/shard_map/all_to_all | solution.py:267
  23.0 14.3 %copy-start.16 = (bf16[256,256]{1,0:T(8,128)(2,1)S(1)}, bf16[256,256]{1,0:T(8,128)(2,1)}, u32[]{:S(2)}) copy-start(bf16[256,256]{1,0:T(8,128)(2,1)} %own_ref.4) | copy-start | bytes 393220
  23.0 14.3 %copy-start.18 = (bf16[256,256]{1,0:T(8,128)(2,1)S(1)}, bf16[256,256]{1,0:T(8,128)(2,1)}, u32[]{:S(2)}) copy-start(bf16[256,256]{1,0:T(8,128)(2,1)} %copy-done.17) | copy-start | bytes 393220
  23.0 65.6 %copy-start.2 = (bf16[2,64,4096]{2,1,0:T(8,128)(2,1)S(1)}, bf16[2,64,4096]{2,1,0:T(8,128)(2,1)}, u32[]{:S(2)}) copy-start(bf16[2,64,4096]{2,1,0:T(8,128)(2,1)} %up.1) | copy-start | bytes 3145732
  23.0 65.6 %copy-start.6 = (bf16[64,4096]{1,0:T(8,128)(2,1)S(1)}, bf16[64,4096]{1,0:T(8,128)(2,1)}, u32[]{:S(2)}) copy-start(bf16[64,4096]{1,0:T(8,128)(2,1)} %s_up.1) | copy-start | bytes 1572868
  24.5 61.8 %collective-permute-start = (bf16[256,4096]{1,0:T(8,128)(2,1)}, bf16[256,4096]{1,0:T(8,128)(2,1)}, u32[]{:S(2)}, u32[]{:S(2)}) collective-permute-start(bf16[256,4096]{1,0:T(8,128)(2,1)} %shard_map.110), channel_id=1, source_target_pairs={{0,1},{1,0},{2,3},{3,2},{4,5},{5,4},{6,7},{7,6},{8,9},{9,8},{10,11... | collective-permute-start | bytes 6291464 | tf_op jit(solution)/shard_map/ppermute | solution.py:278
  27.0 4.1 %collective-permute-start.2 = (f32[256]{0:T(256)S(1)}, f32[256]{0:T(256)S(1)}, u32[]{:S(2)}, u32[]{:S(2)}) collective-permute-start(f32[256]{0:T(256)S(1)} %copy-done.22), channel_id=1, source_target_pairs={{0,1},{1,0},{2,3},{3,2},{4,5},{5,4},{6,7},{7,6},{8,9},{9,8},{10,11... | collective-permute-start | bytes 3080 | tf_op jit(solution)/shard_map/ppermute | solution.py:270
  39.5 13.5 %collective-permute-start.3 = (bf16[328,512]{1,0:T(8,128)(2,1)S(1)}, bf16[328,512]{1,0:T(8,128)(2,1)S(1)}, u32[]{:S(2)}, u32[]{:S(2)}) collective-permute-start(bf16[328,512]{1,0:T(8,128)(2,1)S(1)} %get-tuple-element.19.refs_0_), channel_id=1, source_target_pairs={{0,2},{1,15},{2,4},{3,1},{4,6},{5,3},{6,8},{7,5},{8,10},{9,7},{10,... | collective-permute-start | bytes 1007624 | tf_op jit(solution)/shard_map/ppermute | solution.py:301
  44.6 11.8 %collective-permute-start.6 = (bf16[328,512]{1,0:T(8,128)(2,1)S(1)}, bf16[328,512]{1,0:T(8,128)(2,1)S(1)}, u32[]{:S(2)}, u32[]{:S(2)}) collective-permute-start(bf16[328,512]{1,0:T(8,128)(2,1)S(1)} %get-tuple-element.20.refs_1_), channel_id=1, source_target_pairs={{0,14},{1,3},{2,0},{3,5},{4,2},{5,7},{6,4},{7,9},{8,6},{9,11},{10,... | collective-permute-start | bytes 1007624 | tf_op jit(solution)/shard_map/ppermute | solution.py:305
  46.6 12.1 %collective-permute-start.4 = (bf16[328,512]{1,0:T(8,128)(2,1)S(1)}, bf16[328,512]{1,0:T(8,128)(2,1)S(1)}, u32[]{:S(2)}, u32[]{:S(2)}) collective-permute-start(bf16[328,512]{1,0:T(8,128)(2,1)S(1)} %get-tuple-element.19.refs_0_), channel_id=1, source_target_pairs={{0,14},{1,3},{2,0},{3,5},{4,2},{5,7},{6,4},{7,9},{8,6},{9,11},{10,... | collective-permute-start | bytes 1007624 | tf_op jit(solution)/shard_map/ppermute | solution.py:305
  48.5 13.4 %collective-permute-start.5 = (bf16[328,512]{1,0:T(8,128)(2,1)S(1)}, bf16[328,512]{1,0:T(8,128)(2,1)S(1)}, u32[]{:S(2)}, u32[]{:S(2)}) collective-permute-start(bf16[328,512]{1,0:T(8,128)(2,1)S(1)} %get-tuple-element.20.refs_1_), channel_id=1, source_target_pairs={{0,2},{1,15},{2,4},{3,1},{4,6},{5,3},{6,8},{7,5},{8,10},{9,7},{10,... | collective-permute-start | bytes 1007624 | tf_op jit(solution)/shard_map/ppermute | solution.py:301
  53.1 13.7 %collective-permute-start.7 = (bf16[328,512]{1,0:T(8,128)(2,1)S(1)}, bf16[328,512]{1,0:T(8,128)(2,1)S(1)}, u32[]{:S(2)}, u32[]{:S(2)}) collective-permute-start(bf16[328,512]{1,0:T(8,128)(2,1)S(1)} %collective-permute-done.3.refs_2_), channel_id=1, source_target_pairs={{0,2},{1,15},{2,4},{3,1},{4,6},{5,3},{6,8},{7,5},{8,10},{9,7},{10,... | collective-permute-start | bytes 1007624 | tf_op jit(solution)/shard_map/ppermute | solution.py:301
  56.5 14.9 %collective-permute-start.10 = (bf16[328,512]{1,0:T(8,128)(2,1)S(1)}, bf16[328,512]{1,0:T(8,128)(2,1)S(1)}, u32[]{:S(2)}, u32[]{:S(2)}) collective-permute-start(bf16[328,512]{1,0:T(8,128)(2,1)S(1)} %collective-permute-done.6.refs_5_), channel_id=1, source_target_pairs={{0,14},{1,3},{2,0},{3,5},{4,2},{5,7},{6,4},{7,9},{8,6},{9,11},{10,... | collective-permute-start | bytes 1007624 | tf_op jit(solution)/shard_map/ppermute | solution.py:305
  58.7 15.4 %collective-permute-start.8 = (bf16[328,512]{1,0:T(8,128)(2,1)S(1)}, bf16[328,512]{1,0:T(8,128)(2,1)S(1)}, u32[]{:S(2)}, u32[]{:S(2)}) collective-permute-start(bf16[328,512]{1,0:T(8,128)(2,1)S(1)} %collective-permute-done.4.refs_3_), channel_id=1, source_target_pairs={{0,14},{1,3},{2,0},{3,5},{4,2},{5,7},{6,4},{7,9},{8,6},{9,11},{10,... | collective-permute-start | bytes 1007624 | tf_op jit(solution)/shard_map/ppermute | solution.py:305
  61.9 14.9 %collective-permute-start.9 = (bf16[328,512]{1,0:T(8,128)(2,1)S(1)}, bf16[328,512]{1,0:T(8,128)(2,1)S(1)}, u32[]{:S(2)}, u32[]{:S(2)}) collective-permute-start(bf16[328,512]{1,0:T(8,128)(2,1)S(1)} %collective-permute-done.5.refs_4_), channel_id=1, source_target_pairs={{0,2},{1,15},{2,4},{3,1},{4,6},{5,3},{6,8},{7,5},{8,10},{9,7},{10,... | collective-permute-start | bytes 1007624 | tf_op jit(solution)/shard_map/ppermute | solution.py:301
  66.8 13.8 %collective-permute-start.11 = (bf16[328,512]{1,0:T(8,128)(2,1)S(1)}, bf16[328,512]{1,0:T(8,128)(2,1)S(1)}, u32[]{:S(2)}, u32[]{:S(2)}) collective-permute-start(bf16[328,512]{1,0:T(8,128)(2,1)S(1)} %collective-permute-done.7.refs_6_), channel_id=1, source_target_pairs={{0,2},{1,15},{2,4},{3,1},{4,6},{5,3},{6,8},{7,5},{8,10},{9,7},{10,... | collective-permute-start | bytes 1007624 | tf_op jit(solution)/shard_map/ppermute | solution.py:301
  71.4 13.0 %collective-permute-start.14 = (bf16[328,512]{1,0:T(8,128)(2,1)S(1)}, bf16[328,512]{1,0:T(8,128)(2,1)S(1)}, u32[]{:S(2)}, u32[]{:S(2)}) collective-permute-start(bf16[328,512]{1,0:T(8,128)(2,1)S(1)} %collective-permute-done.10.refs_9_), channel_id=1, source_target_pairs={{0,14},{1,3},{2,0},{3,5},{4,2},{5,7},{6,4},{7,9},{8,6},{9,11},{10,... | collective-permute-start | bytes 1007624 | tf_op jit(solution)/shard_map/ppermute | solution.py:305
  74.1 13.6 %collective-permute-start.12 = (bf16[328,512]{1,0:T(8,128)(2,1)S(1)}, bf16[328,512]{1,0:T(8,128)(2,1)S(1)}, u32[]{:S(2)}, u32[]{:S(2)}) collective-permute-start(bf16[328,512]{1,0:T(8,128)(2,1)S(1)} %collective-permute-done.8.refs_7_), channel_id=1, source_target_pairs={{0,14},{1,3},{2,0},{3,5},{4,2},{5,7},{6,4},{7,9},{8,6},{9,11},{10,... | collective-permute-start | bytes 1007624 | tf_op jit(solution)/shard_map/ppermute | solution.py:305
  76.8 11.8 %collective-permute-start.13 = (bf16[328,512]{1,0:T(8,128)(2,1)S(1)}, bf16[328,512]{1,0:T(8,128)(2,1)S(1)}, u32[]{:S(2)}, u32[]{:S(2)}) collective-permute-start(bf16[328,512]{1,0:T(8,128)(2,1)S(1)} %collective-permute-done.9.refs_8_), channel_id=1, source_target_pairs={{0,2},{1,15},{2,4},{3,1},{4,6},{5,3},{6,8},{7,5},{8,10},{9,7},{10,... | collective-permute-start | bytes 1007624 | tf_op jit(solution)/shard_map/ppermute | solution.py:301
  80.7 13.3 %collective-permute-start.15 = (bf16[328,512]{1,0:T(8,128)(2,1)S(1)}, bf16[328,512]{1,0:T(8,128)(2,1)S(1)}, u32[]{:S(2)}, u32[]{:S(2)}) collective-permute-start(bf16[328,512]{1,0:T(8,128)(2,1)S(1)} %collective-permute-done.11.refs_10_), channel_id=1, source_target_pairs={{0,2},{1,15},{2,4},{3,1},{4,6},{5,3},{6,8},{7,5},{8,10},{9,7},{10,... | collective-permute-start | bytes 1007624 | tf_op jit(solution)/shard_map/ppermute | solution.py:301
  84.4 13.0 %collective-permute-start.16 = (bf16[328,512]{1,0:T(8,128)(2,1)S(1)}, bf16[328,512]{1,0:T(8,128)(2,1)S(1)}, u32[]{:S(2)}, u32[]{:S(2)}) collective-permute-start(bf16[328,512]{1,0:T(8,128)(2,1)S(1)} %collective-permute-done.14.refs_13_), channel_id=1, source_target_pairs={{0,14},{1,3},{2,0},{3,5},{4,2},{5,7},{6,4},{7,9},{8,6},{9,11},{10,... | collective-permute-start | bytes 1007624 | tf_op jit(solution)/shard_map/ppermute | solution.py:305
  98.9 38.4 %all-to-all-start.1 = ((bf16[8,640,128]{2,1,0:T(8,128)(2,1)}), bf16[8,640,128]{2,1,0:T(8,128)(2,1)S(1)}, u32[]{:S(2)}, u32[]{:S(2)}) async-start(bf16[8,640,128]{2,1,0:T(8,128)(2,1)} %shard_map.114), calls=%async_computation.1 | async-start | bytes 2621440 | tf_op jit(solution)/shard_map/all_to_all | solution.py:331
  104.9 40.6 %copy-start.19 = (s32[256,3]{0,1:T(4,128)S(1)}, s32[256,3]{0,1:T(4,128)}, u32[]{:S(2)}) copy-start(s32[256,3]{0,1:T(4,128)} %param.13) | copy-start | bytes 9220
  104.9 40.6 %copy-start.20 = (f32[256,3]{0,1:T(4,128)S(1)}, f32[256,3]{0,1:T(4,128)}, u32[]{:S(2)}) copy-start(f32[256,3]{0,1:T(4,128)} %param.14) | copy-start | bytes 9220
  104.9 7.6 %collective-permute-start.17 = (bf16[2048,256]{1,0:T(8,128)(2,1)S(1)}, bf16[2048,256]{1,0:T(8,128)(2,1)S(1)}, u32[]{:S(2)}, u32[]{:S(2)}) collective-permute-start(bf16[2048,256]{1,0:T(8,128)(2,1)S(1)} %shard_map.115), channel_id=1, source_target_pairs={{0,1},{1,0},{2,3},{3,2},{4,5},{5,4},{6,7},{7,6},{8,9},{9,8},{10,11... | collective-permute-start | bytes 3145736 | tf_op jit(solution)/shard_map/ppermute | solution.py:286
  138.8 23.2 %all-to-all-start.2 = ((bf16[32,16,512]{2,1,0:T(8,128)(2,1)}), bf16[32,16,512]{2,1,0:T(8,128)(2,1)S(1)}, u32[]{:S(2)}, u32[]{:S(2)}) async-start(bf16[32,16,512]{2,1,0:T(8,128)(2,1)} %bitcast.13), calls=%async_computation.2 | async-start | bytes 1048576 | tf_op jit(solution)/shard_map/all_to_all | solution.py:339
  148.1 13.9 %copy-start.11 = (bf16[256,512]{1,0:T(8,128)(2,1)S(1)}, bf16[256,512]{1,0:T(8,128)(2,1)}, u32[]{:S(2)}) copy-start(bf16[256,512]{1,0:T(8,128)(2,1)} %copy-done.10) | copy-start | bytes 786436
  148.5 29.7 %copy-start.21 = (f32[256]{0:T(256)S(1)}, f32[256]{0:T(256)}, u32[]{:S(2)}) copy-start(f32[256]{0:T(256)} %param.21) | copy-start | bytes 3076
  162.6 5.3 %collective-permute-start.18 = (f32[256,256]{1,0:T(8,128)S(1)}, f32[256,256]{1,0:T(8,128)S(1)}, u32[]{:S(2)}, u32[]{:S(2)}) collective-permute-start(f32[256,256]{1,0:T(8,128)S(1)} %get-tuple-element.26), channel_id=1, source_target_pairs={{0,1},{1,0},{2,3},{3,2},{4,5},{5,4},{6,7},{7,6},{8,9},{9,8},{10,11... | collective-permute-start | bytes 786440 | tf_op jit(solution)/shard_map/ppermute | solution.py:357
  (13 other events, 58.6 us)

commit v6 on v5

--- a/solution.py
+++ b/solution.py
@@ -104,10 +104,9 @@
     every, left, right = slice(0, width), slice(0, feat), slice(feat, width)
 
     def total(squares):
-        ones = jnp.ones((SPARE, squares.shape[1]), F32)
-        return lax.dot_general(
-            ones, squares, (((1,), (1,)), ((), ())), precision=lax.Precision.HIGHEST, preferred_element_type=F32
-        )
+        ones = jnp.ones((SPARE, squares.shape[1]), BF)
+        high, middle, low = (times(ones, part) for part in thirds(squares))
+        return high + middle + low
 
     def spare(ref, at, sums):
         high, middle, low = thirds(sums)
@@ -139,7 +138,7 @@
         into[pl.ds(base + other, hid), :] = got[i * hid : (i + 1) * hid, :]
 
     def columns(offset):
-        return pl.ds(pl.multiple_of(lax.rem(y + offset * (1 - 2 * core) + n_y, n_y) * width, width), width)
+        return pl.ds(pl.multiple_of(lax.rem(y + offset + n_y, n_y) * width, width), width)
 
     for half in range(2):
         total = [None] * len(spans[half])
@@ -246,7 +245,7 @@
     y_groups = [[c + 2 * k for k in range(n_y)] for c in range(2)]
 
     def y_shift(d):
-        return [(i, ((i // 2 + d * (1 - 2 * (i % 2))) % n_y) * 2 + i % 2) for i in range(n_tp)]
+        return [(i, ((i // 2 + d) % n_y) * 2 + i % 2) for i in range(n_tp)]
 
     def own_first(mine, other, axis):
         return jnp.where(
@@ -348,7 +347,7 @@
         (third, third, third),
         (ids, route_weight.T),
         4 * 10**8,
-        8,
+        60,
     )
     value = jax.ShapeDtypeStruct((tok, feat), F32)
     home, away = call(

time: 180 us -> 176 us (0.978)
  waiting for transfers between devices: 60.4 us -> 49.1 us
  starting transfers between devices: 87.7 us -> 95.9 us
  local copies, waits for them, and re-layouts: 5.94 us -> 3.79 us
    ppermute x7, starting transfers between devices: 15.4 us -> 31 us  [body(): bwd[k] = lax.ppermute(bwd[k], 'tp', y_shift(-1))]
    ppermute x7, starting transfers between devices: 29.3 us -> 15.2 us  [body(): fwd[k] = lax.ppermute(fwd[k], 'tp', y_shift(1))]
    ppermute x7, waiting for transfers between devices: 6.11 us -> 1.48 us  [body(): bwd[k] = lax.ppermute(bwd[k], 'tp', y_shift(-1))]
    ppermute x1, starting transfers between devices: 4.15 us -> 8.42 us  [body(): summed = home + lax.ppermute(away, 'tp', swap)]
    all_to_all x1, waiting for transfers between devices: 24.8 us -> 21.4 us  [body(): lax.all_to_all(hidden, 'tp', 0, 0, axis_index_groups=y_groups, tiled=True)]
    all_to_all x1, waiting for transfers between devices: 13.5 us -> 10.4 us  [body(): lax.all_to_all(expert_out.reshape(n_ep, cap, width), 'ep', 0, 0, tiled=True)]
    unnamed x46 -> x36, local copies, waits for them, and re-layouts: 5.9 us -> 3.74 us
  transfers between devices with their start and end apart: 22 -> 22, of which waited for: 15 -> 13; matrix products, arithmetic and copies ran while one was open for 0% -> 0% of each run, Pallas kernels for 4% -> 5%
where the time goes in v6:
time: 176 us; the launch traced here: 175 us
  starting transfers between devices  95.9 us (54%)
  waiting for transfers between devices  49.1 us (28%)
  Pallas kernels  14.2 us (8%)
  blocking collectives  10.1 us (6%)
  local copies, waits for them, and re-layouts  3.79 us (2%)
    ppermute x7, starting transfers between devices, body(): bwd[k] = lax.ppermute(bwd[k], 'tp', y_shift(-1))  31 us
    all_to_all x1, waiting for transfers between devices, body(): lax.all_to_all(hidden, 'tp', 0, 0, axis_index_groups=y_groups, tiled=True)  21.4 us
    ppermute x7, starting transfers between devices, body(): fwd[k] = lax.ppermute(fwd[k], 'tp', y_shift(1))  15.2 us
    pallas_call x9, Pallas kernels, call(): pl.pallas_call(kernel, out_shape=out, in_specs=[VMEM] * len(args), out_sp...  14.2 us
    all_to_all x1, waiting for transfers between devices, body(): lax.all_to_all(expert_out.reshape(n_ep, cap, width), 'ep', 0, 0, tiled=True)  10.4 us
    all_to_all x1, blocking collectives, body(): out_square = jnp.sum(lax.all_to_all(sent, 'tp', 0, 0, tiled=True), axis=0)  10.1 us
    ppermute x1, starting transfers between devices, body(): partner = lax.ppermute(tokens, 'tp', swap)  8.87 us
    ppermute x1, starting transfers between devices, body(): summed = home + lax.ppermute(away, 'tp', swap)  8.42 us
  transfers between devices with their start and end apart: 22, of which 13 were waited for; matrix products, arithmetic and copies ran while one was open for 0% of the time, Pallas kernels for 5%

profile of v6, /device:TPU:1, one launch (start us, length us, event | category | flops | bytes accessed | tf_op | source)
XLA Modules:
  0.0 174.9 jit_solution(13176962541279305693)
XLA Ops:
  0.0 8.9 %collective-permute-start.1 = (bf16[256,256]{1,0:T(8,128)(2,1)}, bf16[256,256]{1,0:T(8,128)(2,1)S(1)}, u32[]{:S(2)}, u32[]{:S(2)}) collective-permute-start(bf16[256,256]{1,0:T(8,128)(2,1)} %own_ref.4), channel_id=1, source_target_pairs={{0,1},{1,0},{2,3},{3,2},{4,5},{5,4},{6,7},{7,6},{8,9},{9,8},{10,11... | collective-permute-start | bytes 393224 | tf_op jit(solution)/shard_map/ppermute | solution.py:257
  10.7 2.3 %shard_map.111 = bf16[512,512]{1,0:T(8,128)(2,1)} custom-call(s32[3,256]{1,0:T(4,128)} %bitcast.17, bf16[256,256]{1,0:T(8,128)(2,1)} %own_ref.4, bf16[256,256]{1,0:T(8,128)(2,1)} %copy-done.14), custom_call_target="tpu_custom_call" | custom-call | flops 100000000 | bytes 2097152 | tf_op jit(solution)/shard_map/pallas_call | solution.py:200
  13.0 7.7 %all-to-all-start = ((bf16[32,16,512]{2,1,0:T(8,128)(2,1)}), bf16[32,16,512]{2,1,0:T(8,128)(2,1)}, u32[]{:S(2)}, u32[]{:S(2)}) async-start(bf16[32,16,512]{2,1,0:T(8,128)(2,1)} %bitcast.15), calls=%async_computation | async-start | bytes 1048576 | tf_op jit(solution)/shard_map/all_to_all | solution.py:266
  24.5 2.5 %collective-permute-start = (bf16[256,4096]{1,0:T(8,128)(2,1)}, bf16[256,4096]{1,0:T(8,128)(2,1)}, u32[]{:S(2)}, u32[]{:S(2)}) collective-permute-start(bf16[256,4096]{1,0:T(8,128)(2,1)} %shard_map.110), channel_id=1, source_target_pairs={{0,1},{1,0},{2,3},{3,2},{4,5},{5,4},{6,7},{7,6},{8,9},{9,8},{10,11... | collective-permute-start | bytes 6291464 | tf_op jit(solution)/shard_map/ppermute | solution.py:277
  27.1 1.9 %collective-permute-start.2 = (f32[256]{0:T(256)S(1)}, f32[256]{0:T(256)S(1)}, u32[]{:S(2)}, u32[]{:S(2)}) collective-permute-start(f32[256]{0:T(256)S(1)} %copy-done.17), channel_id=1, source_target_pairs={{0,1},{1,0},{2,3},{3,2},{4,5},{5,4},{6,7},{7,6},{8,9},{9,8},{10,11... | collective-permute-start | bytes 3080 | tf_op jit(solution)/shard_map/ppermute | solution.py:269
  29.0 2.2 %collective-permute-done.2 = f32[256]{0:T(256)S(1)} collective-permute-done((f32[256]{0:T(256)S(1)}, f32[256]{0:T(256)S(1)}, u32[]{:S(2)}, u32[]{:S(2)}) %collective-permute-start.2) | collective-permute-done | bytes 1056 | tf_op jit(solution)/shard_map/ppermute | solution.py:269
  31.2 6.1 %all-to-all-done = bf16[32,16,512]{2,1,0:T(8,128)(2,1)} async-done(((bf16[32,16,512]{2,1,0:T(8,128)(2,1)}), bf16[32,16,512]{2,1,0:T(8,128)(2,1)}, u32[]{:S(2)}, u32[]{:S(2)}) %all-to-all-start) | async-done | bytes 524320 | tf_op jit(solution)/shard_map/all_to_all | solution.py:266
  37.3 1.8 %shard_map.112 = (bf16[328,512]{1,0:T(8,128)(2,1)S(1)}, bf16[328,512]{1,0:T(8,128)(2,1)S(1)}) custom-call(bf16[512,512]{1,0:T(8,128)(2,1)} %bitcast.3.rows_ref, bf16[256,256]{1,0:T(8,128)(2,1)S(1)} %copy-done.13, bf16[256,256]{1,0:T(8,128)(2,1)S(1)} %copy-done.15, f32[1,512]{1,0:T(1,128)S(1)} %broadcast_select_fusion.gain_ref), custom_call_target="tpu_custom_call" | custom-call | flops 400000000 | bytes 2097152 | tf_op jit(solution)/shard_map/pallas_call | solution.py:200
  39.1 3.2 %collective-permute-start.3 = (bf16[328,512]{1,0:T(8,128)(2,1)S(1)}, bf16[328,512]{1,0:T(8,128)(2,1)S(1)}, u32[]{:S(2)}, u32[]{:S(2)}) collective-permute-start(bf16[328,512]{1,0:T(8,128)(2,1)S(1)} %get-tuple-element.19.refs_0_), channel_id=1, source_target_pairs={{0,2},{1,3},{2,4},{3,5},{4,6},{5,7},{6,8},{7,9},{8,10},{9,11},{10,... | collective-permute-start | bytes 1007624 | tf_op jit(solution)/shard_map/ppermute | solution.py:300
  42.3 3.8 %collective-permute-start.6 = (bf16[328,512]{1,0:T(8,128)(2,1)S(1)}, bf16[328,512]{1,0:T(8,128)(2,1)S(1)}, u32[]{:S(2)}, u32[]{:S(2)}) collective-permute-start(bf16[328,512]{1,0:T(8,128)(2,1)S(1)} %get-tuple-element.20.refs_1_), channel_id=1, source_target_pairs={{0,14},{1,15},{2,0},{3,1},{4,2},{5,3},{6,4},{7,5},{8,6},{9,7},{10,... | collective-permute-start | bytes 1007624 | tf_op jit(solution)/shard_map/ppermute | solution.py:304
  46.1 3.4 %collective-permute-start.4 = (bf16[328,512]{1,0:T(8,128)(2,1)S(1)}, bf16[328,512]{1,0:T(8,128)(2,1)S(1)}, u32[]{:S(2)}, u32[]{:S(2)}) collective-permute-start(bf16[328,512]{1,0:T(8,128)(2,1)S(1)} %get-tuple-element.19.refs_0_), channel_id=1, source_target_pairs={{0,14},{1,15},{2,0},{3,1},{4,2},{5,3},{6,4},{7,5},{8,6},{9,7},{10,... | collective-permute-start | bytes 1007624 | tf_op jit(solution)/shard_map/ppermute | solution.py:304
  49.5 1.9 %collective-permute-start.5 = (bf16[328,512]{1,0:T(8,128)(2,1)S(1)}, bf16[328,512]{1,0:T(8,128)(2,1)S(1)}, u32[]{:S(2)}, u32[]{:S(2)}) collective-permute-start(bf16[328,512]{1,0:T(8,128)(2,1)S(1)} %get-tuple-element.20.refs_1_), channel_id=1, source_target_pairs={{0,2},{1,3},{2,4},{3,5},{4,6},{5,7},{6,8},{7,9},{8,10},{9,11},{10,... | collective-permute-start | bytes 1007624 | tf_op jit(solution)/shard_map/ppermute | solution.py:300
  51.4 1.9 %collective-permute-start.7 = (bf16[328,512]{1,0:T(8,128)(2,1)S(1)}, bf16[328,512]{1,0:T(8,128)(2,1)S(1)}, u32[]{:S(2)}, u32[]{:S(2)}) collective-permute-start(bf16[328,512]{1,0:T(8,128)(2,1)S(1)} %collective-permute-done.3.refs_2_), channel_id=1, source_target_pairs={{0,2},{1,3},{2,4},{3,5},{4,6},{5,7},{6,8},{7,9},{8,10},{9,11},{10,... | collective-permute-start | bytes 1007624 | tf_op jit(solution)/shard_map/ppermute | solution.py:300
  53.4 4.6 %collective-permute-start.10 = (bf16[328,512]{1,0:T(8,128)(2,1)S(1)}, bf16[328,512]{1,0:T(8,128)(2,1)S(1)}, u32[]{:S(2)}, u32[]{:S(2)}) collective-permute-start(bf16[328,512]{1,0:T(8,128)(2,1)S(1)} %collective-permute-done.6.refs_5_), channel_id=1, source_target_pairs={{0,14},{1,15},{2,0},{3,1},{4,2},{5,3},{6,4},{7,5},{8,6},{9,7},{10,... | collective-permute-start | bytes 1007624 | tf_op jit(solution)/shard_map/ppermute | solution.py:304
  58.4 5.3 %collective-permute-start.8 = (bf16[328,512]{1,0:T(8,128)(2,1)S(1)}, bf16[328,512]{1,0:T(8,128)(2,1)S(1)}, u32[]{:S(2)}, u32[]{:S(2)}) collective-permute-start(bf16[328,512]{1,0:T(8,128)(2,1)S(1)} %collective-permute-done.4.refs_3_), channel_id=1, source_target_pairs={{0,14},{1,15},{2,0},{3,1},{4,2},{5,3},{6,4},{7,5},{8,6},{9,7},{10,... | collective-permute-start | bytes 1007624 | tf_op jit(solution)/shard_map/ppermute | solution.py:304
  63.7 1.9 %collective-permute-start.9 = (bf16[328,512]{1,0:T(8,128)(2,1)S(1)}, bf16[328,512]{1,0:T(8,128)(2,1)S(1)}, u32[]{:S(2)}, u32[]{:S(2)}) collective-permute-start(bf16[328,512]{1,0:T(8,128)(2,1)S(1)} %collective-permute-done.5.refs_4_), channel_id=1, source_target_pairs={{0,2},{1,3},{2,4},{3,5},{4,6},{5,7},{6,8},{7,9},{8,10},{9,11},{10,... | collective-permute-start | bytes 1007624 | tf_op jit(solution)/shard_map/ppermute | solution.py:300
  66.2 1.9 %collective-permute-start.11 = (bf16[328,512]{1,0:T(8,128)(2,1)S(1)}, bf16[328,512]{1,0:T(8,128)(2,1)S(1)}, u32[]{:S(2)}, u32[]{:S(2)}) collective-permute-start(bf16[328,512]{1,0:T(8,128)(2,1)S(1)} %collective-permute-done.7.refs_6_), channel_id=1, source_target_pairs={{0,2},{1,3},{2,4},{3,5},{4,6},{5,7},{6,8},{7,9},{8,10},{9,11},{10,... | collective-permute-start | bytes 1007624 | tf_op jit(solution)/shard_map/ppermute | solution.py:300
  68.2 4.6 %collective-permute-start.14 = (bf16[328,512]{1,0:T(8,128)(2,1)S(1)}, bf16[328,512]{1,0:T(8,128)(2,1)S(1)}, u32[]{:S(2)}, u32[]{:S(2)}) collective-permute-start(bf16[328,512]{1,0:T(8,128)(2,1)S(1)} %collective-permute-done.10.refs_9_), channel_id=1, source_target_pairs={{0,14},{1,15},{2,0},{3,1},{4,2},{5,3},{6,4},{7,5},{8,6},{9,7},{10,... | collective-permute-start | bytes 1007624 | tf_op jit(solution)/shard_map/ppermute | solution.py:304
  72.8 5.3 %collective-permute-start.12 = (bf16[328,512]{1,0:T(8,128)(2,1)S(1)}, bf16[328,512]{1,0:T(8,128)(2,1)S(1)}, u32[]{:S(2)}, u32[]{:S(2)}) collective-permute-start(bf16[328,512]{1,0:T(8,128)(2,1)S(1)} %collective-permute-done.8.refs_7_), channel_id=1, source_target_pairs={{0,14},{1,15},{2,0},{3,1},{4,2},{5,3},{6,4},{7,5},{8,6},{9,7},{10,... | collective-permute-start | bytes 1007624 | tf_op jit(solution)/shard_map/ppermute | solution.py:304
  78.2 1.9 %collective-permute-start.13 = (bf16[328,512]{1,0:T(8,128)(2,1)S(1)}, bf16[328,512]{1,0:T(8,128)(2,1)S(1)}, u32[]{:S(2)}, u32[]{:S(2)}) collective-permute-start(bf16[328,512]{1,0:T(8,128)(2,1)S(1)} %collective-permute-done.9.refs_8_), channel_id=1, source_target_pairs={{0,2},{1,3},{2,4},{3,5},{4,6},{5,7},{6,8},{7,9},{8,10},{9,11},{10,... | collective-permute-start | bytes 1007624 | tf_op jit(solution)/shard_map/ppermute | solution.py:300
  80.1 2.4 %collective-permute-start.15 = (bf16[328,512]{1,0:T(8,128)(2,1)S(1)}, bf16[328,512]{1,0:T(8,128)(2,1)S(1)}, u32[]{:S(2)}, u32[]{:S(2)}) collective-permute-start(bf16[328,512]{1,0:T(8,128)(2,1)S(1)} %collective-permute-done.11.refs_10_), channel_id=1, source_target_pairs={{0,2},{1,3},{2,4},{3,5},{4,6},{5,7},{6,8},{7,9},{8,10},{9,11},{10,... | collective-permute-start | bytes 1007624 | tf_op jit(solution)/shard_map/ppermute | solution.py:300
  82.6 4.1 %collective-permute-start.16 = (bf16[328,512]{1,0:T(8,128)(2,1)S(1)}, bf16[328,512]{1,0:T(8,128)(2,1)S(1)}, u32[]{:S(2)}, u32[]{:S(2)}) collective-permute-start(bf16[328,512]{1,0:T(8,128)(2,1)S(1)} %collective-permute-done.14.refs_13_), channel_id=1, source_target_pairs={{0,14},{1,15},{2,0},{3,1},{4,2},{5,3},{6,4},{7,5},{8,6},{9,7},{10,... | collective-permute-start | bytes 1007624 | tf_op jit(solution)/shard_map/ppermute | solution.py:304
  87.4 3.7 %shard_map.113 = (f32[640,256]{1,0:T(8,128)S(1)}, f32[16,512]{1,0:T(8,128)S(1)}, bf16[256,512]{1,0:T(8,128)(2,1)S(1)}, bf16[256,512]{1,0:T(8,128)(2,1)S(1)}) custom-call(bf16[2,64,4096]{2,1,0:T(8,128)(2,1)S(1)} %copy-done, bf16[2,64,4096]{2,1,0:T(8,128)(2,1)S(1)} %copy-done.2, bf16[64,4096]{1,0:T(8,128)(2,1)S(1)} %copy-done.4, ...), custom_call_target="tpu_custom_call" | custom-call | flops 1342177280 | bytes 2097152 | tf_op jit(solution)/shard_map/pallas_call | solution.py:200
  95.3 6.9 %all-to-all-start.1 = ((bf16[8,640,128]{2,1,0:T(8,128)(2,1)}), bf16[8,640,128]{2,1,0:T(8,128)(2,1)S(1)}, u32[]{:S(2)}, u32[]{:S(2)}) async-start(bf16[8,640,128]{2,1,0:T(8,128)(2,1)} %shard_map.114), calls=%async_computation.1 | async-start | bytes 2621440 | tf_op jit(solution)/shard_map/all_to_all | solution.py:330
  102.2 7.0 %collective-permute-start.17 = (bf16[2048,256]{1,0:T(8,128)(2,1)S(1)}, bf16[2048,256]{1,0:T(8,128)(2,1)S(1)}, u32[]{:S(2)}, u32[]{:S(2)}) collective-permute-start(bf16[2048,256]{1,0:T(8,128)(2,1)S(1)} %shard_map.115), channel_id=1, source_target_pairs={{0,1},{1,0},{2,3},{3,2},{4,5},{5,4},{6,7},{7,6},{8,9},{9,8},{10,11... | collective-permute-start | bytes 3145736 | tf_op jit(solution)/shard_map/ppermute | solution.py:285
  109.2 2.3 %collective-permute-done.17.got_ref = bf16[2048,256]{1,0:T(8,128)(2,1)S(1)} collective-permute-done((bf16[2048,256]{1,0:T(8,128)(2,1)S(1)}, bf16[2048,256]{1,0:T(8,128)(2,1)S(1)}, u32[]{:S(2)}, u32[]{:S(2)}) %collective-permute-start.17) | collective-permute-done | bytes 1048608 | tf_op jit(solution)/shard_map/ppermute | solution.py:285
  111.4 21.4 %all-to-all-done.1.hidden_ref = bf16[8,640,128]{2,1,0:T(8,128)(2,1)S(1)} async-done(((bf16[8,640,128]{2,1,0:T(8,128)(2,1)}), bf16[8,640,128]{2,1,0:T(8,128)(2,1)S(1)}, u32[]{:S(2)}, u32[]{:S(2)}) %all-to-all-start.1) | async-done | bytes 1310752 | tf_op jit(solution)/shard_map/all_to_all | solution.py:330
  134.3 6.4 %all-to-all-start.2 = ((bf16[32,16,512]{2,1,0:T(8,128)(2,1)}), bf16[32,16,512]{2,1,0:T(8,128)(2,1)S(1)}, u32[]{:S(2)}, u32[]{:S(2)}) async-start(bf16[32,16,512]{2,1,0:T(8,128)(2,1)} %bitcast.13), calls=%async_computation.2 | async-start | bytes 1048576 | tf_op jit(solution)/shard_map/all_to_all | solution.py:338
  140.8 2.0 %shard_map.109 = (bf16[256,512]{1,0:T(8,128)(2,1)}, bf16[256,512]{1,0:T(8,128)(2,1)}, bf16[256,512]{1,0:T(8,128)(2,1)}) custom-call(s32[3,256]{1,0:T(4,128)} %bitcast.18, f32[3,256]{1,0:T(4,128)} %bitcast.21), custom_call_target="tpu_custom_call" | custom-call | flops 400000000 | bytes 2097152 | tf_op jit(solution)/shard_map/pallas_call | solution.py:200
  143.3 10.4 %all-to-all-done.2 = bf16[32,16,512]{2,1,0:T(8,128)(2,1)S(1)} async-done(((bf16[32,16,512]{2,1,0:T(8,128)(2,1)}), bf16[32,16,512]{2,1,0:T(8,128)(2,1)S(1)}, u32[]{:S(2)}, u32[]{:S(2)}) %all-to-all-start.2) | async-done | bytes 524320 | tf_op jit(solution)/shard_map/all_to_all | solution.py:338
  154.2 8.4 %collective-permute-start.18 = (f32[256,256]{1,0:T(8,128)S(1)}, f32[256,256]{1,0:T(8,128)S(1)}, u32[]{:S(2)}, u32[]{:S(2)}) collective-permute-start(f32[256,256]{1,0:T(8,128)S(1)} %get-tuple-element.26), channel_id=1, source_target_pairs={{0,1},{1,0},{2,3},{3,2},{4,5},{5,4},{6,7},{7,6},{8,9},{9,8},{10,11... | collective-permute-start | bytes 786440 | tf_op jit(solution)/shard_map/ppermute | solution.py:356
  163.9 10.1 %all_to_all.21 = f32[16,1,256]{2,1,0:T(1,128)S(1)} all-to-all(f32[16,1,256]{2,1,0:T(1,128)S(1)} %broadcast_in_dim.2), channel_id=1, replica_groups=mesh['ep'=32,'tp'=16] {'tp'}, dimensions={0} | all-to-all | bytes 32768 | tf_op jit(solution)/shard_map/all_to_all | solution.py:359
  (66 shorter events, 16.3 us)
Async XLA Ops:
  0.0 20.7 %copy-start = (bf16[2,64,4096]{2,1,0:T(8,128)(2,1)S(1)}, bf16[2,64,4096]{2,1,0:T(8,128)(2,1)}, u32[]{:S(2)}) copy-start(bf16[2,64,4096]{2,1,0:T(8,128)(2,1)} %gate.1) | copy-start | bytes 3145732
  0.0 20.7 %copy-start.4 = (bf16[64,4096]{1,0:T(8,128)(2,1)S(1)}, bf16[64,4096]{1,0:T(8,128)(2,1)}, u32[]{:S(2)}) copy-start(bf16[64,4096]{1,0:T(8,128)(2,1)} %s_gate.1) | copy-start | bytes 1572868
  0.0 10.1 %collective-permute-start.1 = (bf16[256,256]{1,0:T(8,128)(2,1)}, bf16[256,256]{1,0:T(8,128)(2,1)S(1)}, u32[]{:S(2)}, u32[]{:S(2)}) collective-permute-start(bf16[256,256]{1,0:T(8,128)(2,1)} %own_ref.4), channel_id=1, source_target_pairs={{0,1},{1,0},{2,3},{3,2},{4,5},{5,4},{6,7},{7,6},{8,9},{9,8},{10,11... | collective-permute-start | bytes 393224 | tf_op jit(solution)/shard_map/ppermute | solution.py:257
  13.0 24.3 %all-to-all-start = ((bf16[32,16,512]{2,1,0:T(8,128)(2,1)}), bf16[32,16,512]{2,1,0:T(8,128)(2,1)}, u32[]{:S(2)}, u32[]{:S(2)}) async-start(bf16[32,16,512]{2,1,0:T(8,128)(2,1)} %bitcast.15), calls=%async_computation | async-start | bytes 1048576 | tf_op jit(solution)/shard_map/all_to_all | solution.py:266
  23.0 14.3 %copy-start.13 = (bf16[256,256]{1,0:T(8,128)(2,1)S(1)}, bf16[256,256]{1,0:T(8,128)(2,1)}, u32[]{:S(2)}) copy-start(bf16[256,256]{1,0:T(8,128)(2,1)} %own_ref.4) | copy-start | bytes 393220
  23.0 14.3 %copy-start.15 = (bf16[256,256]{1,0:T(8,128)(2,1)S(1)}, bf16[256,256]{1,0:T(8,128)(2,1)}, u32[]{:S(2)}) copy-start(bf16[256,256]{1,0:T(8,128)(2,1)} %copy-done.14) | copy-start | bytes 393220
  23.0 64.4 %copy-start.2 = (bf16[2,64,4096]{2,1,0:T(8,128)(2,1)S(1)}, bf16[2,64,4096]{2,1,0:T(8,128)(2,1)}, u32[]{:S(2)}) copy-start(bf16[2,64,4096]{2,1,0:T(8,128)(2,1)} %up.1) | copy-start | bytes 3145732
  23.0 64.4 %copy-start.6 = (bf16[64,4096]{1,0:T(8,128)(2,1)S(1)}, bf16[64,4096]{1,0:T(8,128)(2,1)}, u32[]{:S(2)}) copy-start(bf16[64,4096]{1,0:T(8,128)(2,1)} %s_up.1) | copy-start | bytes 1572868
  24.5 62.1 %collective-permute-start = (bf16[256,4096]{1,0:T(8,128)(2,1)}, bf16[256,4096]{1,0:T(8,128)(2,1)}, u32[]{:S(2)}, u32[]{:S(2)}) collective-permute-start(bf16[256,4096]{1,0:T(8,128)(2,1)} %shard_map.110), channel_id=1, source_target_pairs={{0,1},{1,0},{2,3},{3,2},{4,5},{5,4},{6,7},{7,6},{8,9},{9,8},{10,11... | collective-permute-start | bytes 6291464 | tf_op jit(solution)/shard_map/ppermute | solution.py:277
  27.1 4.1 %collective-permute-start.2 = (f32[256]{0:T(256)S(1)}, f32[256]{0:T(256)S(1)}, u32[]{:S(2)}, u32[]{:S(2)}) collective-permute-start(f32[256]{0:T(256)S(1)} %copy-done.17), channel_id=1, source_target_pairs={{0,1},{1,0},{2,3},{3,2},{4,5},{5,4},{6,7},{7,6},{8,9},{9,8},{10,11... | collective-permute-start | bytes 3080 | tf_op jit(solution)/shard_map/ppermute | solution.py:269
  39.1 12.3 %collective-permute-start.3 = (bf16[328,512]{1,0:T(8,128)(2,1)S(1)}, bf16[328,512]{1,0:T(8,128)(2,1)S(1)}, u32[]{:S(2)}, u32[]{:S(2)}) collective-permute-start(bf16[328,512]{1,0:T(8,128)(2,1)S(1)} %get-tuple-element.19.refs_0_), channel_id=1, source_target_pairs={{0,2},{1,3},{2,4},{3,5},{4,6},{5,7},{6,8},{7,9},{8,10},{9,11},{10,... | collective-permute-start | bytes 1007624 | tf_op jit(solution)/shard_map/ppermute | solution.py:300
  42.3 11.1 %collective-permute-start.6 = (bf16[328,512]{1,0:T(8,128)(2,1)S(1)}, bf16[328,512]{1,0:T(8,128)(2,1)S(1)}, u32[]{:S(2)}, u32[]{:S(2)}) collective-permute-start(bf16[328,512]{1,0:T(8,128)(2,1)S(1)} %get-tuple-element.20.refs_1_), channel_id=1, source_target_pairs={{0,14},{1,15},{2,0},{3,1},{4,2},{5,3},{6,4},{7,5},{8,6},{9,7},{10,... | collective-permute-start | bytes 1007624 | tf_op jit(solution)/shard_map/ppermute | solution.py:304
  46.1 12.3 %collective-permute-start.4 = (bf16[328,512]{1,0:T(8,128)(2,1)S(1)}, bf16[328,512]{1,0:T(8,128)(2,1)S(1)}, u32[]{:S(2)}, u32[]{:S(2)}) collective-permute-start(bf16[328,512]{1,0:T(8,128)(2,1)S(1)} %get-tuple-element.19.refs_0_), channel_id=1, source_target_pairs={{0,14},{1,15},{2,0},{3,1},{4,2},{5,3},{6,4},{7,5},{8,6},{9,7},{10,... | collective-permute-start | bytes 1007624 | tf_op jit(solution)/shard_map/ppermute | solution.py:304
  49.5 14.2 %collective-permute-start.5 = (bf16[328,512]{1,0:T(8,128)(2,1)S(1)}, bf16[328,512]{1,0:T(8,128)(2,1)S(1)}, u32[]{:S(2)}, u32[]{:S(2)}) collective-permute-start(bf16[328,512]{1,0:T(8,128)(2,1)S(1)} %get-tuple-element.20.refs_1_), channel_id=1, source_target_pairs={{0,2},{1,3},{2,4},{3,5},{4,6},{5,7},{6,8},{7,9},{8,10},{9,11},{10,... | collective-permute-start | bytes 1007624 | tf_op jit(solution)/shard_map/ppermute | solution.py:300
  51.4 14.8 %collective-permute-start.7 = (bf16[328,512]{1,0:T(8,128)(2,1)S(1)}, bf16[328,512]{1,0:T(8,128)(2,1)S(1)}, u32[]{:S(2)}, u32[]{:S(2)}) collective-permute-start(bf16[328,512]{1,0:T(8,128)(2,1)S(1)} %collective-permute-done.3.refs_2_), channel_id=1, source_target_pairs={{0,2},{1,3},{2,4},{3,5},{4,6},{5,7},{6,8},{7,9},{8,10},{9,11},{10,... | collective-permute-start | bytes 1007624 | tf_op jit(solution)/shard_map/ppermute | solution.py:300
  53.4 14.8 %collective-permute-start.10 = (bf16[328,512]{1,0:T(8,128)(2,1)S(1)}, bf16[328,512]{1,0:T(8,128)(2,1)S(1)}, u32[]{:S(2)}, u32[]{:S(2)}) collective-permute-start(bf16[328,512]{1,0:T(8,128)(2,1)S(1)} %collective-permute-done.6.refs_5_), channel_id=1, source_target_pairs={{0,14},{1,15},{2,0},{3,1},{4,2},{5,3},{6,4},{7,5},{8,6},{9,7},{10,... | collective-permute-start | bytes 1007624 | tf_op jit(solution)/shard_map/ppermute | solution.py:304
  58.4 14.4 %collective-permute-start.8 = (bf16[328,512]{1,0:T(8,128)(2,1)S(1)}, bf16[328,512]{1,0:T(8,128)(2,1)S(1)}, u32[]{:S(2)}, u32[]{:S(2)}) collective-permute-start(bf16[328,512]{1,0:T(8,128)(2,1)S(1)} %collective-permute-done.4.refs_3_), channel_id=1, source_target_pairs={{0,14},{1,15},{2,0},{3,1},{4,2},{5,3},{6,4},{7,5},{8,6},{9,7},{10,... | collective-permute-start | bytes 1007624 | tf_op jit(solution)/shard_map/ppermute | solution.py:304
  63.7 14.4 %collective-permute-start.9 = (bf16[328,512]{1,0:T(8,128)(2,1)S(1)}, bf16[328,512]{1,0:T(8,128)(2,1)S(1)}, u32[]{:S(2)}, u32[]{:S(2)}) collective-permute-start(bf16[328,512]{1,0:T(8,128)(2,1)S(1)} %collective-permute-done.5.refs_4_), channel_id=1, source_target_pairs={{0,2},{1,3},{2,4},{3,5},{4,6},{5,7},{6,8},{7,9},{8,10},{9,11},{10,... | collective-permute-start | bytes 1007624 | tf_op jit(solution)/shard_map/ppermute | solution.py:300
  66.2 13.8 %collective-permute-start.11 = (bf16[328,512]{1,0:T(8,128)(2,1)S(1)}, bf16[328,512]{1,0:T(8,128)(2,1)S(1)}, u32[]{:S(2)}, u32[]{:S(2)}) collective-permute-start(bf16[328,512]{1,0:T(8,128)(2,1)S(1)} %collective-permute-done.7.refs_6_), channel_id=1, source_target_pairs={{0,2},{1,3},{2,4},{3,5},{4,6},{5,7},{6,8},{7,9},{8,10},{9,11},{10,... | collective-permute-start | bytes 1007624 | tf_op jit(solution)/shard_map/ppermute | solution.py:300
  68.2 14.4 %collective-permute-start.14 = (bf16[328,512]{1,0:T(8,128)(2,1)S(1)}, bf16[328,512]{1,0:T(8,128)(2,1)S(1)}, u32[]{:S(2)}, u32[]{:S(2)}) collective-permute-start(bf16[328,512]{1,0:T(8,128)(2,1)S(1)} %collective-permute-done.10.refs_9_), channel_id=1, source_target_pairs={{0,14},{1,15},{2,0},{3,1},{4,2},{5,3},{6,4},{7,5},{8,6},{9,7},{10,... | collective-permute-start | bytes 1007624 | tf_op jit(solution)/shard_map/ppermute | solution.py:304
  72.8 13.8 %collective-permute-start.12 = (bf16[328,512]{1,0:T(8,128)(2,1)S(1)}, bf16[328,512]{1,0:T(8,128)(2,1)S(1)}, u32[]{:S(2)}, u32[]{:S(2)}) collective-permute-start(bf16[328,512]{1,0:T(8,128)(2,1)S(1)} %collective-permute-done.8.refs_7_), channel_id=1, source_target_pairs={{0,14},{1,15},{2,0},{3,1},{4,2},{5,3},{6,4},{7,5},{8,6},{9,7},{10,... | collective-permute-start | bytes 1007624 | tf_op jit(solution)/shard_map/ppermute | solution.py:304
  78.2 9.2 %collective-permute-start.13 = (bf16[328,512]{1,0:T(8,128)(2,1)S(1)}, bf16[328,512]{1,0:T(8,128)(2,1)S(1)}, u32[]{:S(2)}, u32[]{:S(2)}) collective-permute-start(bf16[328,512]{1,0:T(8,128)(2,1)S(1)} %collective-permute-done.9.refs_8_), channel_id=1, source_target_pairs={{0,2},{1,3},{2,4},{3,5},{4,6},{5,7},{6,8},{7,9},{8,10},{9,11},{10,... | collective-permute-start | bytes 1007624 | tf_op jit(solution)/shard_map/ppermute | solution.py:300
  80.1 12.7 %collective-permute-start.15 = (bf16[328,512]{1,0:T(8,128)(2,1)S(1)}, bf16[328,512]{1,0:T(8,128)(2,1)S(1)}, u32[]{:S(2)}, u32[]{:S(2)}) collective-permute-start(bf16[328,512]{1,0:T(8,128)(2,1)S(1)} %collective-permute-done.11.refs_10_), channel_id=1, source_target_pairs={{0,2},{1,3},{2,4},{3,5},{4,6},{5,7},{6,8},{7,9},{8,10},{9,11},{10,... | collective-permute-start | bytes 1007624 | tf_op jit(solution)/shard_map/ppermute | solution.py:300
  82.6 11.1 %collective-permute-start.16 = (bf16[328,512]{1,0:T(8,128)(2,1)S(1)}, bf16[328,512]{1,0:T(8,128)(2,1)S(1)}, u32[]{:S(2)}, u32[]{:S(2)}) collective-permute-start(bf16[328,512]{1,0:T(8,128)(2,1)S(1)} %collective-permute-done.14.refs_13_), channel_id=1, source_target_pairs={{0,14},{1,15},{2,0},{3,1},{4,2},{5,3},{6,4},{7,5},{8,6},{9,7},{10,... | collective-permute-start | bytes 1007624 | tf_op jit(solution)/shard_map/ppermute | solution.py:304
  95.3 37.6 %all-to-all-start.1 = ((bf16[8,640,128]{2,1,0:T(8,128)(2,1)}), bf16[8,640,128]{2,1,0:T(8,128)(2,1)S(1)}, u32[]{:S(2)}, u32[]{:S(2)}) async-start(bf16[8,640,128]{2,1,0:T(8,128)(2,1)} %shard_map.114), calls=%async_computation.1 | async-start | bytes 2621440 | tf_op jit(solution)/shard_map/all_to_all | solution.py:330
  102.2 9.2 %collective-permute-start.17 = (bf16[2048,256]{1,0:T(8,128)(2,1)S(1)}, bf16[2048,256]{1,0:T(8,128)(2,1)S(1)}, u32[]{:S(2)}, u32[]{:S(2)}) collective-permute-start(bf16[2048,256]{1,0:T(8,128)(2,1)S(1)} %shard_map.115), channel_id=1, source_target_pairs={{0,1},{1,0},{2,3},{3,2},{4,5},{5,4},{6,7},{7,6},{8,9},{9,8},{10,11... | collective-permute-start | bytes 3145736 | tf_op jit(solution)/shard_map/ppermute | solution.py:285
  134.3 19.3 %all-to-all-start.2 = ((bf16[32,16,512]{2,1,0:T(8,128)(2,1)}), bf16[32,16,512]{2,1,0:T(8,128)(2,1)S(1)}, u32[]{:S(2)}, u32[]{:S(2)}) async-start(bf16[32,16,512]{2,1,0:T(8,128)(2,1)} %bitcast.13), calls=%async_computation.2 | async-start | bytes 1048576 | tf_op jit(solution)/shard_map/all_to_all | solution.py:338
  142.9 10.8 %copy-start.10 = (bf16[256,512]{1,0:T(8,128)(2,1)S(1)}, bf16[256,512]{1,0:T(8,128)(2,1)}, u32[]{:S(2)}) copy-start(bf16[256,512]{1,0:T(8,128)(2,1)} %get-tuple-element.16.high) | copy-start | bytes 786436
  142.9 10.7 %copy-start.11 = (bf16[256,512]{1,0:T(8,128)(2,1)S(1)}, bf16[256,512]{1,0:T(8,128)(2,1)}, u32[]{:S(2)}) copy-start(bf16[256,512]{1,0:T(8,128)(2,1)} %get-tuple-element.17.middle) | copy-start | bytes 786436
  142.9 10.7 %copy-start.12 = (bf16[256,512]{1,0:T(8,128)(2,1)S(1)}, bf16[256,512]{1,0:T(8,128)(2,1)}, u32[]{:S(2)}) copy-start(bf16[256,512]{1,0:T(8,128)(2,1)} %get-tuple-element.18.low) | copy-start | bytes 786436
  143.3 30.9 %copy-start.16 = (f32[256]{0:T(256)S(1)}, f32[256]{0:T(256)}, u32[]{:S(2)}) copy-start(f32[256]{0:T(256)} %param.21) | copy-start | bytes 3076
  154.2 9.6 %collective-permute-start.18 = (f32[256,256]{1,0:T(8,128)S(1)}, f32[256,256]{1,0:T(8,128)S(1)}, u32[]{:S(2)}, u32[]{:S(2)}) collective-permute-start(f32[256,256]{1,0:T(8,128)S(1)} %get-tuple-element.26), channel_id=1, source_target_pairs={{0,1},{1,0},{2,3},{3,2},{4,5},{5,4},{6,7},{7,6},{8,9},{9,8},{10,11... | collective-permute-start | bytes 786440 | tf_op jit(solution)/shard_map/ppermute | solution.py:356
  (8 other events, 30.0 us)

commit v7 on v6

--- a/solution.py
+++ b/solution.py
@@ -76,13 +76,40 @@
         away_ref[at, :] = jnp.where(core == 0, right, left)
 
 
-def route_kernel(n_ep, cap, ids_ref, own_ref, other_ref, out_ref):
+def own_kernel(n_ep, cap, ids_ref, own_ref, pick_ref, part_ref):
+    one_hot = picks(ids_ref[...], here()[0], n_ep, cap)
+    pick_ref[...] = one_hot
+    part_ref[...] = jnp.dot(one_hot, own_ref[...], preferred_element_type=F32).astype(BF)
+
+
+def join_kernel(pick_ref, part_ref, other_ref, out_ref):
     core, _ = here()
-    one_hot = picks(ids_ref[...], core, n_ep, cap)
-    feat = own_ref.shape[1]
-    for ref, where in ((own_ref, core), (other_ref, 1 - core)):
-        at = pl.ds(pl.multiple_of(where * feat, feat), feat)
-        out_ref[:, at] = jnp.dot(one_hot, ref[...], preferred_element_type=F32).astype(BF)
+    feat = part_ref.shape[1]
+    out_ref[:, pl.ds(pl.multiple_of(core * feat, feat), feat)] = part_ref[...]
+    other = jnp.dot(pick_ref[...], other_ref[...], preferred_element_type=F32).astype(BF)
+    out_ref[:, pl.ds(pl.multiple_of((1 - core) * feat, feat), feat)] = other
+
+
+def mix_kernel(n_ep, cap, ids_ref, weight_ref, *out_refs):
+    mix = picks(ids_ref[...], here()[0], n_ep, cap, weight_ref[...]).T
+    for ref, value in zip(out_refs, thirds(mix)):
+        ref[...] = value
+
+
+def combine_kernel(high, middle, low, rows_ref, shared_ref, home_ref, away_ref):
+    core, _ = here()
+    rows = rows_ref[...]
+    part = jnp.dot(high[...], rows, preferred_element_type=F32)
+    part = part + jnp.dot(middle[...], rows, preferred_element_type=F32)
+    part = part + jnp.dot(low[...], rows, preferred_element_type=F32)
+    shared = shared_ref[...]
+    half, feat = shared.shape[0], home_ref.shape[1]
+    top = part[:half] + jnp.where(core == 0, shared, 0.0)
+    bottom = part[half:] + jnp.where(core == 0, 0.0, shared)
+    for at, value in ((slice(0, half), top), (slice(half, 2 * half), bottom)):
+        left, right = value[:, :feat], value[:, feat:]
+        home_ref[at, :] = jnp.where(core == 0, left, right)
+        away_ref[at, :] = jnp.where(core == 0, right, left)
 
 
 def arrive_kernel(rows_ref, own_ref, other_ref, gain_ref, first_ref, second_ref):
@@ -256,12 +283,19 @@
 
     partner = lax.ppermute(tokens, "tp", swap)
     ids = expert_ids.T
+    one_hot, own_part = call(
+        functools.partial(own_kernel, n_ep, cap),
+        (jax.ShapeDtypeStruct((slots, tok), BF), jax.ShapeDtypeStruct((slots, feat), BF)),
+        (ids, tokens),
+        10**8,
+        8,
+    )
     outgoing = call(
-        functools.partial(route_kernel, n_ep, cap),
+        join_kernel,
         jax.ShapeDtypeStruct((slots, width), BF),
-        (ids, tokens, partner),
+        (one_hot, own_part, partner),
         10**8,
-        60,
+        8,
     )
     arrived = lax.all_to_all(outgoing.reshape(n_ep, cap, width), "ep", 0, 0, tiled=True)
     arrived = arrived.reshape(slots, width)

time: 176 us -> 175 us (level)
    pallas_call x9 -> x10, Pallas kernels: 14.2 us -> 13.4 us  [call(): pl.pallas_call(kernel, out_shape=out, in_specs=[VMEM] * len(args), out_sp...]
  transfers between devices with their start and end apart: 22 -> 22, of which waited for: 13 -> 11; matrix products, arithmetic and copies ran while one was open for 0% -> 0% of each run, Pallas kernels for 5% -> 5%
where the time goes in v7:
time: 175 us; the launch traced here: 173 us
  starting transfers between devices  95.2 us (54%)
  waiting for transfers between devices  48.5 us (28%)
  Pallas kernels  13.4 us (8%)
  blocking collectives  10.1 us (6%)
  local copies, waits for them, and re-layouts  4.54 us (3%)
    ppermute x7, starting transfers between devices, body(): bwd[k] = lax.ppermute(bwd[k], 'tp', y_shift(-1))  31 us
    all_to_all x1, waiting for transfers between devices, body(): lax.all_to_all(hidden, 'tp', 0, 0, axis_index_groups=y_groups, tiled=True)  21.4 us
    ppermute x7, starting transfers between devices, body(): fwd[k] = lax.ppermute(fwd[k], 'tp', y_shift(1))  15.2 us
    pallas_call x10, Pallas kernels, call(): pl.pallas_call(kernel, out_shape=out, in_specs=[VMEM] * len(args), out_sp...  13.4 us
    all_to_all x1, waiting for transfers between devices, body(): lax.all_to_all(expert_out.reshape(n_ep, cap, width), 'ep', 0, 0, tiled=True)  10.4 us
    all_to_all x1, blocking collectives, body(): out_square = jnp.sum(lax.all_to_all(sent, 'tp', 0, 0, tiled=True), axis=0)  10.1 us
    ppermute x1, starting transfers between devices, body(): partner = lax.ppermute(tokens, 'tp', swap)  8.87 us
    ppermute x1, starting transfers between devices, body(): summed = home + lax.ppermute(away, 'tp', swap)  8.37 us
  transfers between devices with their start and end apart: 22, of which 11 were waited for; matrix products, arithmetic and copies ran while one was open for 0% of the time, Pallas kernels for 5%

profile of v7, /device:TPU:1, one launch (start us, length us, event | category | flops | bytes accessed | tf_op | source)
XLA Modules:
  0.0 173.4 jit_solution(10053326380950802189)
XLA Ops:
  0.0 8.9 %collective-permute-start.1 = (bf16[256,256]{1,0:T(8,128)(2,1)}, bf16[256,256]{1,0:T(8,128)(2,1)S(1)}, u32[]{:S(2)}, u32[]{:S(2)}) collective-permute-start(bf16[256,256]{1,0:T(8,128)(2,1)} %own_ref.4), channel_id=1, source_target_pairs={{0,1},{1,0},{2,3},{3,2},{4,5},{5,4},{6,7},{7,6},{8,9},{9,8},{10,11... | collective-permute-start | bytes 393224 | tf_op jit(solution)/shard_map/ppermute | solution.py:284
  11.9 7.7 %all-to-all-start = ((bf16[32,16,512]{2,1,0:T(8,128)(2,1)}), bf16[32,16,512]{2,1,0:T(8,128)(2,1)}, u32[]{:S(2)}, u32[]{:S(2)}) async-start(bf16[32,16,512]{2,1,0:T(8,128)(2,1)} %bitcast.2), calls=%async_computation | async-start | bytes 1048576 | tf_op jit(solution)/shard_map/all_to_all | solution.py:300
  23.2 2.2 %collective-permute-start = (bf16[256,4096]{1,0:T(8,128)(2,1)}, bf16[256,4096]{1,0:T(8,128)(2,1)}, u32[]{:S(2)}, u32[]{:S(2)}) collective-permute-start(bf16[256,4096]{1,0:T(8,128)(2,1)} %shard_map.110), channel_id=1, source_target_pairs={{0,1},{1,0},{2,3},{3,2},{4,5},{5,4},{6,7},{7,6},{8,9},{9,8},{10,11... | collective-permute-start | bytes 6291464 | tf_op jit(solution)/shard_map/ppermute | solution.py:311
  25.4 2.1 %collective-permute-start.2 = (f32[256]{0:T(256)S(1)}, f32[256]{0:T(256)S(1)}, u32[]{:S(2)}, u32[]{:S(2)}) collective-permute-start(f32[256]{0:T(256)S(1)} %copy-done.17), channel_id=1, source_target_pairs={{0,1},{1,0},{2,3},{3,2},{4,5},{5,4},{6,7},{7,6},{8,9},{9,8},{10,11... | collective-permute-start | bytes 3080 | tf_op jit(solution)/shard_map/ppermute | solution.py:303
  27.6 2.0 %collective-permute-done.2 = f32[256]{0:T(256)S(1)} collective-permute-done((f32[256]{0:T(256)S(1)}, f32[256]{0:T(256)S(1)}, u32[]{:S(2)}, u32[]{:S(2)}) %collective-permute-start.2) | collective-permute-done | bytes 1056 | tf_op jit(solution)/shard_map/ppermute | solution.py:303
  29.6 6.7 %all-to-all-done = bf16[32,16,512]{2,1,0:T(8,128)(2,1)} async-done(((bf16[32,16,512]{2,1,0:T(8,128)(2,1)}), bf16[32,16,512]{2,1,0:T(8,128)(2,1)}, u32[]{:S(2)}, u32[]{:S(2)}) %all-to-all-start) | async-done | bytes 524320 | tf_op jit(solution)/shard_map/all_to_all | solution.py:300
  36.3 1.8 %shard_map.113 = (bf16[328,512]{1,0:T(8,128)(2,1)S(1)}, bf16[328,512]{1,0:T(8,128)(2,1)S(1)}) custom-call(bf16[512,512]{1,0:T(8,128)(2,1)} %bitcast.3.rows_ref, bf16[256,256]{1,0:T(8,128)(2,1)S(1)} %copy-done.14, bf16[256,256]{1,0:T(8,128)(2,1)S(1)} %collective-permute-done.1.other_ref, f32[1,512]{1,0:T(1,128)S(1)} %broadcast_select_fusion.gain_ref), custom_call_target="tpu_custom_call" | custom-call | flops 400000000 | bytes 2097152 | tf_op jit(solution)/shard_map/pallas_call | solution.py:227
  38.1 3.2 %collective-permute-start.3 = (bf16[328,512]{1,0:T(8,128)(2,1)S(1)}, bf16[328,512]{1,0:T(8,128)(2,1)S(1)}, u32[]{:S(2)}, u32[]{:S(2)}) collective-permute-start(bf16[328,512]{1,0:T(8,128)(2,1)S(1)} %get-tuple-element.23.refs_0_), channel_id=1, source_target_pairs={{0,2},{1,3},{2,4},{3,5},{4,6},{5,7},{6,8},{7,9},{8,10},{9,11},{10,... | collective-permute-start | bytes 1007624 | tf_op jit(solution)/shard_map/ppermute | solution.py:334
  41.4 3.8 %collective-permute-start.6 = (bf16[328,512]{1,0:T(8,128)(2,1)S(1)}, bf16[328,512]{1,0:T(8,128)(2,1)S(1)}, u32[]{:S(2)}, u32[]{:S(2)}) collective-permute-start(bf16[328,512]{1,0:T(8,128)(2,1)S(1)} %get-tuple-element.24.refs_1_), channel_id=1, source_target_pairs={{0,14},{1,15},{2,0},{3,1},{4,2},{5,3},{6,4},{7,5},{8,6},{9,7},{10,... | collective-permute-start | bytes 1007624 | tf_op jit(solution)/shard_map/ppermute | solution.py:338
  45.2 3.4 %collective-permute-start.4 = (bf16[328,512]{1,0:T(8,128)(2,1)S(1)}, bf16[328,512]{1,0:T(8,128)(2,1)S(1)}, u32[]{:S(2)}, u32[]{:S(2)}) collective-permute-start(bf16[328,512]{1,0:T(8,128)(2,1)S(1)} %get-tuple-element.23.refs_0_), channel_id=1, source_target_pairs={{0,14},{1,15},{2,0},{3,1},{4,2},{5,3},{6,4},{7,5},{8,6},{9,7},{10,... | collective-permute-start | bytes 1007624 | tf_op jit(solution)/shard_map/ppermute | solution.py:338
  48.5 1.9 %collective-permute-start.5 = (bf16[328,512]{1,0:T(8,128)(2,1)S(1)}, bf16[328,512]{1,0:T(8,128)(2,1)S(1)}, u32[]{:S(2)}, u32[]{:S(2)}) collective-permute-start(bf16[328,512]{1,0:T(8,128)(2,1)S(1)} %get-tuple-element.24.refs_1_), channel_id=1, source_target_pairs={{0,2},{1,3},{2,4},{3,5},{4,6},{5,7},{6,8},{7,9},{8,10},{9,11},{10,... | collective-permute-start | bytes 1007624 | tf_op jit(solution)/shard_map/ppermute | solution.py:334
  50.5 1.9 %collective-permute-start.7 = (bf16[328,512]{1,0:T(8,128)(2,1)S(1)}, bf16[328,512]{1,0:T(8,128)(2,1)S(1)}, u32[]{:S(2)}, u32[]{:S(2)}) collective-permute-start(bf16[328,512]{1,0:T(8,128)(2,1)S(1)} %collective-permute-done.3.refs_2_), channel_id=1, source_target_pairs={{0,2},{1,3},{2,4},{3,5},{4,6},{5,7},{6,8},{7,9},{8,10},{9,11},{10,... | collective-permute-start | bytes 1007624 | tf_op jit(solution)/shard_map/ppermute | solution.py:334
  52.4 4.6 %collective-permute-start.10 = (bf16[328,512]{1,0:T(8,128)(2,1)S(1)}, bf16[328,512]{1,0:T(8,128)(2,1)S(1)}, u32[]{:S(2)}, u32[]{:S(2)}) collective-permute-start(bf16[328,512]{1,0:T(8,128)(2,1)S(1)} %collective-permute-done.6.refs_5_), channel_id=1, source_target_pairs={{0,14},{1,15},{2,0},{3,1},{4,2},{5,3},{6,4},{7,5},{8,6},{9,7},{10,... | collective-permute-start | bytes 1007624 | tf_op jit(solution)/shard_map/ppermute | solution.py:338
  57.6 5.3 %collective-permute-start.8 = (bf16[328,512]{1,0:T(8,128)(2,1)S(1)}, bf16[328,512]{1,0:T(8,128)(2,1)S(1)}, u32[]{:S(2)}, u32[]{:S(2)}) collective-permute-start(bf16[328,512]{1,0:T(8,128)(2,1)S(1)} %collective-permute-done.4.refs_3_), channel_id=1, source_target_pairs={{0,14},{1,15},{2,0},{3,1},{4,2},{5,3},{6,4},{7,5},{8,6},{9,7},{10,... | collective-permute-start | bytes 1007624 | tf_op jit(solution)/shard_map/ppermute | solution.py:338
  62.9 1.9 %collective-permute-start.9 = (bf16[328,512]{1,0:T(8,128)(2,1)S(1)}, bf16[328,512]{1,0:T(8,128)(2,1)S(1)}, u32[]{:S(2)}, u32[]{:S(2)}) collective-permute-start(bf16[328,512]{1,0:T(8,128)(2,1)S(1)} %collective-permute-done.5.refs_4_), channel_id=1, source_target_pairs={{0,2},{1,3},{2,4},{3,5},{4,6},{5,7},{6,8},{7,9},{8,10},{9,11},{10,... | collective-permute-start | bytes 1007624 | tf_op jit(solution)/shard_map/ppermute | solution.py:334
  65.4 1.9 %collective-permute-start.11 = (bf16[328,512]{1,0:T(8,128)(2,1)S(1)}, bf16[328,512]{1,0:T(8,128)(2,1)S(1)}, u32[]{:S(2)}, u32[]{:S(2)}) collective-permute-start(bf16[328,512]{1,0:T(8,128)(2,1)S(1)} %collective-permute-done.7.refs_6_), channel_id=1, source_target_pairs={{0,2},{1,3},{2,4},{3,5},{4,6},{5,7},{6,8},{7,9},{8,10},{9,11},{10,... | collective-permute-start | bytes 1007624 | tf_op jit(solution)/shard_map/ppermute | solution.py:334
  67.3 4.6 %collective-permute-start.14 = (bf16[328,512]{1,0:T(8,128)(2,1)S(1)}, bf16[328,512]{1,0:T(8,128)(2,1)S(1)}, u32[]{:S(2)}, u32[]{:S(2)}) collective-permute-start(bf16[328,512]{1,0:T(8,128)(2,1)S(1)} %collective-permute-done.10.refs_9_), channel_id=1, source_target_pairs={{0,14},{1,15},{2,0},{3,1},{4,2},{5,3},{6,4},{7,5},{8,6},{9,7},{10,... | collective-permute-start | bytes 1007624 | tf_op jit(solution)/shard_map/ppermute | solution.py:338
  72.0 5.3 %collective-permute-start.12 = (bf16[328,512]{1,0:T(8,128)(2,1)S(1)}, bf16[328,512]{1,0:T(8,128)(2,1)S(1)}, u32[]{:S(2)}, u32[]{:S(2)}) collective-permute-start(bf16[328,512]{1,0:T(8,128)(2,1)S(1)} %collective-permute-done.8.refs_7_), channel_id=1, source_target_pairs={{0,14},{1,15},{2,0},{3,1},{4,2},{5,3},{6,4},{7,5},{8,6},{9,7},{10,... | collective-permute-start | bytes 1007624 | tf_op jit(solution)/shard_map/ppermute | solution.py:338
  77.3 1.9 %collective-permute-start.13 = (bf16[328,512]{1,0:T(8,128)(2,1)S(1)}, bf16[328,512]{1,0:T(8,128)(2,1)S(1)}, u32[]{:S(2)}, u32[]{:S(2)}) collective-permute-start(bf16[328,512]{1,0:T(8,128)(2,1)S(1)} %collective-permute-done.9.refs_8_), channel_id=1, source_target_pairs={{0,2},{1,3},{2,4},{3,5},{4,6},{5,7},{6,8},{7,9},{8,10},{9,11},{10,... | collective-permute-start | bytes 1007624 | tf_op jit(solution)/shard_map/ppermute | solution.py:334
  79.2 2.4 %collective-permute-start.15 = (bf16[328,512]{1,0:T(8,128)(2,1)S(1)}, bf16[328,512]{1,0:T(8,128)(2,1)S(1)}, u32[]{:S(2)}, u32[]{:S(2)}) collective-permute-start(bf16[328,512]{1,0:T(8,128)(2,1)S(1)} %collective-permute-done.11.refs_10_), channel_id=1, source_target_pairs={{0,2},{1,3},{2,4},{3,5},{4,6},{5,7},{6,8},{7,9},{8,10},{9,11},{10,... | collective-permute-start | bytes 1007624 | tf_op jit(solution)/shard_map/ppermute | solution.py:334
  81.7 4.1 %collective-permute-start.16 = (bf16[328,512]{1,0:T(8,128)(2,1)S(1)}, bf16[328,512]{1,0:T(8,128)(2,1)S(1)}, u32[]{:S(2)}, u32[]{:S(2)}) collective-permute-start(bf16[328,512]{1,0:T(8,128)(2,1)S(1)} %collective-permute-done.14.refs_13_), channel_id=1, source_target_pairs={{0,14},{1,15},{2,0},{3,1},{4,2},{5,3},{6,4},{7,5},{8,6},{9,7},{10,... | collective-permute-start | bytes 1007624 | tf_op jit(solution)/shard_map/ppermute | solution.py:338
  86.5 3.7 %shard_map.114 = (f32[640,256]{1,0:T(8,128)S(1)}, f32[16,512]{1,0:T(8,128)S(1)}, bf16[256,512]{1,0:T(8,128)(2,1)S(1)}, bf16[256,512]{1,0:T(8,128)(2,1)S(1)}) custom-call(bf16[2,64,4096]{2,1,0:T(8,128)(2,1)S(1)} %copy-done, bf16[2,64,4096]{2,1,0:T(8,128)(2,1)S(1)} %copy-done.1, bf16[64,4096]{1,0:T(8,128)(2,1)S(1)} %copy-done.4, ...), custom_call_target="tpu_custom_call" | custom-call | flops 1342177280 | bytes 2097152 | tf_op jit(solution)/shard_map/pallas_call | solution.py:227
  90.1 1.8 %collective-permute-done.15.refs_0_ = bf16[328,512]{1,0:T(8,128)(2,1)S(1)} collective-permute-done((bf16[328,512]{1,0:T(8,128)(2,1)S(1)}, bf16[328,512]{1,0:T(8,128)(2,1)S(1)}, u32[]{:S(2)}, u32[]{:S(2)}) %collective-permute-start.15) | collective-permute-done | bytes 335904 | tf_op jit(solution)/shard_map/ppermute | solution.py:334
  94.3 6.9 %all-to-all-start.1 = ((bf16[8,640,128]{2,1,0:T(8,128)(2,1)}), bf16[8,640,128]{2,1,0:T(8,128)(2,1)S(1)}, u32[]{:S(2)}, u32[]{:S(2)}) async-start(bf16[8,640,128]{2,1,0:T(8,128)(2,1)} %shard_map.115), calls=%async_computation.1 | async-start | bytes 2621440 | tf_op jit(solution)/shard_map/all_to_all | solution.py:364
  101.3 6.9 %collective-permute-start.17 = (bf16[2048,256]{1,0:T(8,128)(2,1)S(1)}, bf16[2048,256]{1,0:T(8,128)(2,1)S(1)}, u32[]{:S(2)}, u32[]{:S(2)}) collective-permute-start(bf16[2048,256]{1,0:T(8,128)(2,1)S(1)} %shard_map.116), channel_id=1, source_target_pairs={{0,1},{1,0},{2,3},{3,2},{4,5},{5,4},{6,7},{7,6},{8,9},{9,8},{10,11... | collective-permute-start | bytes 3145736 | tf_op jit(solution)/shard_map/ppermute | solution.py:319
  108.2 2.3 %collective-permute-done.17.got_ref = bf16[2048,256]{1,0:T(8,128)(2,1)S(1)} collective-permute-done((bf16[2048,256]{1,0:T(8,128)(2,1)S(1)}, bf16[2048,256]{1,0:T(8,128)(2,1)S(1)}, u32[]{:S(2)}, u32[]{:S(2)}) %collective-permute-start.17) | collective-permute-done | bytes 1048608 | tf_op jit(solution)/shard_map/ppermute | solution.py:319
  110.5 21.4 %all-to-all-done.1.hidden_ref = bf16[8,640,128]{2,1,0:T(8,128)(2,1)S(1)} async-done(((bf16[8,640,128]{2,1,0:T(8,128)(2,1)}), bf16[8,640,128]{2,1,0:T(8,128)(2,1)S(1)}, u32[]{:S(2)}, u32[]{:S(2)}) %all-to-all-start.1) | async-done | bytes 1310752 | tf_op jit(solution)/shard_map/all_to_all | solution.py:364
  133.4 5.9 %all-to-all-start.2 = ((bf16[32,16,512]{2,1,0:T(8,128)(2,1)}), bf16[32,16,512]{2,1,0:T(8,128)(2,1)S(1)}, u32[]{:S(2)}, u32[]{:S(2)}) async-start(bf16[32,16,512]{2,1,0:T(8,128)(2,1)} %bitcast.13), calls=%async_computation.2 | async-start | bytes 1048576 | tf_op jit(solution)/shard_map/all_to_all | solution.py:372
  139.4 2.0 %shard_map.109 = (bf16[256,512]{1,0:T(8,128)(2,1)}, bf16[256,512]{1,0:T(8,128)(2,1)}, bf16[256,512]{1,0:T(8,128)(2,1)}) custom-call(s32[3,256]{1,0:T(4,128)} %bitcast.15, f32[3,256]{1,0:T(4,128)} %bitcast.20), custom_call_target="tpu_custom_call" | custom-call | flops 400000000 | bytes 2097152 | tf_op jit(solution)/shard_map/pallas_call | solution.py:227
  141.8 10.4 %all-to-all-done.2 = bf16[32,16,512]{2,1,0:T(8,128)(2,1)S(1)} async-done(((bf16[32,16,512]{2,1,0:T(8,128)(2,1)}), bf16[32,16,512]{2,1,0:T(8,128)(2,1)S(1)}, u32[]{:S(2)}, u32[]{:S(2)}) %all-to-all-start.2) | async-done | bytes 524320 | tf_op jit(solution)/shard_map/all_to_all | solution.py:372
  152.8 8.4 %collective-permute-start.18 = (f32[256,256]{1,0:T(8,128)S(1)}, f32[256,256]{1,0:T(8,128)S(1)}, u32[]{:S(2)}, u32[]{:S(2)}) collective-permute-start(f32[256,256]{1,0:T(8,128)S(1)} %get-tuple-element.30), channel_id=1, source_target_pairs={{0,1},{1,0},{2,3},{3,2},{4,5},{5,4},{6,7},{7,6},{8,9},{9,8},{10,11... | collective-permute-start | bytes 786440 | tf_op jit(solution)/shard_map/ppermute | solution.py:390
  162.4 10.1 %all_to_all.21 = f32[16,1,256]{2,1,0:T(1,128)S(1)} all-to-all(f32[16,1,256]{2,1,0:T(1,128)S(1)} %broadcast_in_dim.2), channel_id=1, replica_groups=mesh['ep'=32,'tp'=16] {'tp'}, dimensions={0} | all-to-all | bytes 32768 | tf_op jit(solution)/shard_map/all_to_all | solution.py:393
  (67 shorter events, 15.6 us)
Async XLA Ops:
  0.0 19.6 %copy-start = (bf16[2,64,4096]{2,1,0:T(8,128)(2,1)S(1)}, bf16[2,64,4096]{2,1,0:T(8,128)(2,1)}, u32[]{:S(2)}) copy-start(bf16[2,64,4096]{2,1,0:T(8,128)(2,1)} %gate.1) | copy-start | bytes 3145732
  0.0 19.6 %copy-start.1 = (bf16[2,64,4096]{2,1,0:T(8,128)(2,1)S(1)}, bf16[2,64,4096]{2,1,0:T(8,128)(2,1)}, u32[]{:S(2)}) copy-start(bf16[2,64,4096]{2,1,0:T(8,128)(2,1)} %up.1) | copy-start | bytes 3145732
  0.0 10.9 %collective-permute-start.1 = (bf16[256,256]{1,0:T(8,128)(2,1)}, bf16[256,256]{1,0:T(8,128)(2,1)S(1)}, u32[]{:S(2)}, u32[]{:S(2)}) collective-permute-start(bf16[256,256]{1,0:T(8,128)(2,1)} %own_ref.4), channel_id=1, source_target_pairs={{0,1},{1,0},{2,3},{3,2},{4,5},{5,4},{6,7},{7,6},{8,9},{9,8},{10,11... | collective-permute-start | bytes 393224 | tf_op jit(solution)/shard_map/ppermute | solution.py:284
  11.9 24.4 %all-to-all-start = ((bf16[32,16,512]{2,1,0:T(8,128)(2,1)}), bf16[32,16,512]{2,1,0:T(8,128)(2,1)}, u32[]{:S(2)}, u32[]{:S(2)}) async-start(bf16[32,16,512]{2,1,0:T(8,128)(2,1)} %bitcast.2), calls=%async_computation | async-start | bytes 1048576 | tf_op jit(solution)/shard_map/all_to_all | solution.py:300
  21.7 14.6 %copy-start.14 = (bf16[256,256]{1,0:T(8,128)(2,1)S(1)}, bf16[256,256]{1,0:T(8,128)(2,1)}, u32[]{:S(2)}) copy-start(bf16[256,256]{1,0:T(8,128)(2,1)} %own_ref.4) | copy-start | bytes 393220
  21.7 64.7 %copy-start.4 = (bf16[64,4096]{1,0:T(8,128)(2,1)S(1)}, bf16[64,4096]{1,0:T(8,128)(2,1)}, u32[]{:S(2)}) copy-start(bf16[64,4096]{1,0:T(8,128)(2,1)} %s_gate.1) | copy-start | bytes 1572868
  21.7 64.7 %copy-start.6 = (bf16[64,4096]{1,0:T(8,128)(2,1)S(1)}, bf16[64,4096]{1,0:T(8,128)(2,1)}, u32[]{:S(2)}) copy-start(bf16[64,4096]{1,0:T(8,128)(2,1)} %s_up.1) | copy-start | bytes 1572868
  23.2 62.5 %collective-permute-start = (bf16[256,4096]{1,0:T(8,128)(2,1)}, bf16[256,4096]{1,0:T(8,128)(2,1)}, u32[]{:S(2)}, u32[]{:S(2)}) collective-permute-start(bf16[256,4096]{1,0:T(8,128)(2,1)} %shard_map.110), channel_id=1, source_target_pairs={{0,1},{1,0},{2,3},{3,2},{4,5},{5,4},{6,7},{7,6},{8,9},{9,8},{10,11... | collective-permute-start | bytes 6291464 | tf_op jit(solution)/shard_map/ppermute | solution.py:311
  25.4 4.2 %collective-permute-start.2 = (f32[256]{0:T(256)S(1)}, f32[256]{0:T(256)S(1)}, u32[]{:S(2)}, u32[]{:S(2)}) collective-permute-start(f32[256]{0:T(256)S(1)} %copy-done.17), channel_id=1, source_target_pairs={{0,1},{1,0},{2,3},{3,2},{4,5},{5,4},{6,7},{7,6},{8,9},{9,8},{10,11... | collective-permute-start | bytes 3080 | tf_op jit(solution)/shard_map/ppermute | solution.py:303
  38.1 12.3 %collective-permute-start.3 = (bf16[328,512]{1,0:T(8,128)(2,1)S(1)}, bf16[328,512]{1,0:T(8,128)(2,1)S(1)}, u32[]{:S(2)}, u32[]{:S(2)}) collective-permute-start(bf16[328,512]{1,0:T(8,128)(2,1)S(1)} %get-tuple-element.23.refs_0_), channel_id=1, source_target_pairs={{0,2},{1,3},{2,4},{3,5},{4,6},{5,7},{6,8},{7,9},{8,10},{9,11},{10,... | collective-permute-start | bytes 1007624 | tf_op jit(solution)/shard_map/ppermute | solution.py:334
  41.4 11.1 %collective-permute-start.6 = (bf16[328,512]{1,0:T(8,128)(2,1)S(1)}, bf16[328,512]{1,0:T(8,128)(2,1)S(1)}, u32[]{:S(2)}, u32[]{:S(2)}) collective-permute-start(bf16[328,512]{1,0:T(8,128)(2,1)S(1)} %get-tuple-element.24.refs_1_), channel_id=1, source_target_pairs={{0,14},{1,15},{2,0},{3,1},{4,2},{5,3},{6,4},{7,5},{8,6},{9,7},{10,... | collective-permute-start | bytes 1007624 | tf_op jit(solution)/shard_map/ppermute | solution.py:338
  45.2 12.4 %collective-permute-start.4 = (bf16[328,512]{1,0:T(8,128)(2,1)S(1)}, bf16[328,512]{1,0:T(8,128)(2,1)S(1)}, u32[]{:S(2)}, u32[]{:S(2)}) collective-permute-start(bf16[328,512]{1,0:T(8,128)(2,1)S(1)} %get-tuple-element.23.refs_0_), channel_id=1, source_target_pairs={{0,14},{1,15},{2,0},{3,1},{4,2},{5,3},{6,4},{7,5},{8,6},{9,7},{10,... | collective-permute-start | bytes 1007624 | tf_op jit(solution)/shard_map/ppermute | solution.py:338
  48.5 14.3 %collective-permute-start.5 = (bf16[328,512]{1,0:T(8,128)(2,1)S(1)}, bf16[328,512]{1,0:T(8,128)(2,1)S(1)}, u32[]{:S(2)}, u32[]{:S(2)}) collective-permute-start(bf16[328,512]{1,0:T(8,128)(2,1)S(1)} %get-tuple-element.24.refs_1_), channel_id=1, source_target_pairs={{0,2},{1,3},{2,4},{3,5},{4,6},{5,7},{6,8},{7,9},{8,10},{9,11},{10,... | collective-permute-start | bytes 1007624 | tf_op jit(solution)/shard_map/ppermute | solution.py:334
  50.5 14.9 %collective-permute-start.7 = (bf16[328,512]{1,0:T(8,128)(2,1)S(1)}, bf16[328,512]{1,0:T(8,128)(2,1)S(1)}, u32[]{:S(2)}, u32[]{:S(2)}) collective-permute-start(bf16[328,512]{1,0:T(8,128)(2,1)S(1)} %collective-permute-done.3.refs_2_), channel_id=1, source_target_pairs={{0,2},{1,3},{2,4},{3,5},{4,6},{5,7},{6,8},{7,9},{8,10},{9,11},{10,... | collective-permute-start | bytes 1007624 | tf_op jit(solution)/shard_map/ppermute | solution.py:334
  52.4 14.9 %collective-permute-start.10 = (bf16[328,512]{1,0:T(8,128)(2,1)S(1)}, bf16[328,512]{1,0:T(8,128)(2,1)S(1)}, u32[]{:S(2)}, u32[]{:S(2)}) collective-permute-start(bf16[328,512]{1,0:T(8,128)(2,1)S(1)} %collective-permute-done.6.refs_5_), channel_id=1, source_target_pairs={{0,14},{1,15},{2,0},{3,1},{4,2},{5,3},{6,4},{7,5},{8,6},{9,7},{10,... | collective-permute-start | bytes 1007624 | tf_op jit(solution)/shard_map/ppermute | solution.py:338
  57.6 14.4 %collective-permute-start.8 = (bf16[328,512]{1,0:T(8,128)(2,1)S(1)}, bf16[328,512]{1,0:T(8,128)(2,1)S(1)}, u32[]{:S(2)}, u32[]{:S(2)}) collective-permute-start(bf16[328,512]{1,0:T(8,128)(2,1)S(1)} %collective-permute-done.4.refs_3_), channel_id=1, source_target_pairs={{0,14},{1,15},{2,0},{3,1},{4,2},{5,3},{6,4},{7,5},{8,6},{9,7},{10,... | collective-permute-start | bytes 1007624 | tf_op jit(solution)/shard_map/ppermute | solution.py:338
  62.9 14.4 %collective-permute-start.9 = (bf16[328,512]{1,0:T(8,128)(2,1)S(1)}, bf16[328,512]{1,0:T(8,128)(2,1)S(1)}, u32[]{:S(2)}, u32[]{:S(2)}) collective-permute-start(bf16[328,512]{1,0:T(8,128)(2,1)S(1)} %collective-permute-done.5.refs_4_), channel_id=1, source_target_pairs={{0,2},{1,3},{2,4},{3,5},{4,6},{5,7},{6,8},{7,9},{8,10},{9,11},{10,... | collective-permute-start | bytes 1007624 | tf_op jit(solution)/shard_map/ppermute | solution.py:334
  65.4 13.8 %collective-permute-start.11 = (bf16[328,512]{1,0:T(8,128)(2,1)S(1)}, bf16[328,512]{1,0:T(8,128)(2,1)S(1)}, u32[]{:S(2)}, u32[]{:S(2)}) collective-permute-start(bf16[328,512]{1,0:T(8,128)(2,1)S(1)} %collective-permute-done.7.refs_6_), channel_id=1, source_target_pairs={{0,2},{1,3},{2,4},{3,5},{4,6},{5,7},{6,8},{7,9},{8,10},{9,11},{10,... | collective-permute-start | bytes 1007624 | tf_op jit(solution)/shard_map/ppermute | solution.py:334
  67.3 14.3 %collective-permute-start.14 = (bf16[328,512]{1,0:T(8,128)(2,1)S(1)}, bf16[328,512]{1,0:T(8,128)(2,1)S(1)}, u32[]{:S(2)}, u32[]{:S(2)}) collective-permute-start(bf16[328,512]{1,0:T(8,128)(2,1)S(1)} %collective-permute-done.10.refs_9_), channel_id=1, source_target_pairs={{0,14},{1,15},{2,0},{3,1},{4,2},{5,3},{6,4},{7,5},{8,6},{9,7},{10,... | collective-permute-start | bytes 1007624 | tf_op jit(solution)/shard_map/ppermute | solution.py:338
  72.0 13.8 %collective-permute-start.12 = (bf16[328,512]{1,0:T(8,128)(2,1)S(1)}, bf16[328,512]{1,0:T(8,128)(2,1)S(1)}, u32[]{:S(2)}, u32[]{:S(2)}) collective-permute-start(bf16[328,512]{1,0:T(8,128)(2,1)S(1)} %collective-permute-done.8.refs_7_), channel_id=1, source_target_pairs={{0,14},{1,15},{2,0},{3,1},{4,2},{5,3},{6,4},{7,5},{8,6},{9,7},{10,... | collective-permute-start | bytes 1007624 | tf_op jit(solution)/shard_map/ppermute | solution.py:338
  77.3 9.2 %collective-permute-start.13 = (bf16[328,512]{1,0:T(8,128)(2,1)S(1)}, bf16[328,512]{1,0:T(8,128)(2,1)S(1)}, u32[]{:S(2)}, u32[]{:S(2)}) collective-permute-start(bf16[328,512]{1,0:T(8,128)(2,1)S(1)} %collective-permute-done.9.refs_8_), channel_id=1, source_target_pairs={{0,2},{1,3},{2,4},{3,5},{4,6},{5,7},{6,8},{7,9},{8,10},{9,11},{10,... | collective-permute-start | bytes 1007624 | tf_op jit(solution)/shard_map/ppermute | solution.py:334
  79.2 12.7 %collective-permute-start.15 = (bf16[328,512]{1,0:T(8,128)(2,1)S(1)}, bf16[328,512]{1,0:T(8,128)(2,1)S(1)}, u32[]{:S(2)}, u32[]{:S(2)}) collective-permute-start(bf16[328,512]{1,0:T(8,128)(2,1)S(1)} %collective-permute-done.11.refs_10_), channel_id=1, source_target_pairs={{0,2},{1,3},{2,4},{3,5},{4,6},{5,7},{6,8},{7,9},{8,10},{9,11},{10,... | collective-permute-start | bytes 1007624 | tf_op jit(solution)/shard_map/ppermute | solution.py:334
  81.7 11.1 %collective-permute-start.16 = (bf16[328,512]{1,0:T(8,128)(2,1)S(1)}, bf16[328,512]{1,0:T(8,128)(2,1)S(1)}, u32[]{:S(2)}, u32[]{:S(2)}) collective-permute-start(bf16[328,512]{1,0:T(8,128)(2,1)S(1)} %collective-permute-done.14.refs_13_), channel_id=1, source_target_pairs={{0,14},{1,15},{2,0},{3,1},{4,2},{5,3},{6,4},{7,5},{8,6},{9,7},{10,... | collective-permute-start | bytes 1007624 | tf_op jit(solution)/shard_map/ppermute | solution.py:338
  94.3 37.6 %all-to-all-start.1 = ((bf16[8,640,128]{2,1,0:T(8,128)(2,1)}), bf16[8,640,128]{2,1,0:T(8,128)(2,1)S(1)}, u32[]{:S(2)}, u32[]{:S(2)}) async-start(bf16[8,640,128]{2,1,0:T(8,128)(2,1)} %shard_map.115), calls=%async_computation.1 | async-start | bytes 2621440 | tf_op jit(solution)/shard_map/all_to_all | solution.py:364
  101.3 9.2 %collective-permute-start.17 = (bf16[2048,256]{1,0:T(8,128)(2,1)S(1)}, bf16[2048,256]{1,0:T(8,128)(2,1)S(1)}, u32[]{:S(2)}, u32[]{:S(2)}) collective-permute-start(bf16[2048,256]{1,0:T(8,128)(2,1)S(1)} %shard_map.116), channel_id=1, source_target_pairs={{0,1},{1,0},{2,3},{3,2},{4,5},{5,4},{6,7},{7,6},{8,9},{9,8},{10,11... | collective-permute-start | bytes 3145736 | tf_op jit(solution)/shard_map/ppermute | solution.py:319
  133.4 8.0 %copy-start.9 = (bf16[1024,256]{1,0:T(8,128)(2,1)S(1)}, bf16[1024,256]{1,0:T(8,128)(2,1)}, u32[]{:S(2)}) copy-start(bf16[1024,256]{1,0:T(8,128)(2,1)} %refs_1_.3) | copy-start | bytes 1572868
  133.4 18.8 %all-to-all-start.2 = ((bf16[32,16,512]{2,1,0:T(8,128)(2,1)}), bf16[32,16,512]{2,1,0:T(8,128)(2,1)S(1)}, u32[]{:S(2)}, u32[]{:S(2)}) async-start(bf16[32,16,512]{2,1,0:T(8,128)(2,1)} %bitcast.13), calls=%async_computation.2 | async-start | bytes 1048576 | tf_op jit(solution)/shard_map/all_to_all | solution.py:372
  141.4 10.8 %copy-start.10 = (bf16[256,512]{1,0:T(8,128)(2,1)S(1)}, bf16[256,512]{1,0:T(8,128)(2,1)}, u32[]{:S(2)}) copy-start(bf16[256,512]{1,0:T(8,128)(2,1)} %get-tuple-element.18.high) | copy-start | bytes 786436
  141.4 10.8 %copy-start.11 = (bf16[256,512]{1,0:T(8,128)(2,1)S(1)}, bf16[256,512]{1,0:T(8,128)(2,1)}, u32[]{:S(2)}) copy-start(bf16[256,512]{1,0:T(8,128)(2,1)} %get-tuple-element.19.middle) | copy-start | bytes 786436
  141.4 10.8 %copy-start.12 = (bf16[256,512]{1,0:T(8,128)(2,1)S(1)}, bf16[256,512]{1,0:T(8,128)(2,1)}, u32[]{:S(2)}) copy-start(bf16[256,512]{1,0:T(8,128)(2,1)} %get-tuple-element.20.low) | copy-start | bytes 786436
  141.8 30.8 %copy-start.16 = (f32[256]{0:T(256)S(1)}, f32[256]{0:T(256)}, u32[]{:S(2)}) copy-start(f32[256]{0:T(256)} %param.21) | copy-start | bytes 3076
  152.8 9.5 %collective-permute-start.18 = (f32[256,256]{1,0:T(8,128)S(1)}, f32[256,256]{1,0:T(8,128)S(1)}, u32[]{:S(2)}, u32[]{:S(2)}) collective-permute-start(f32[256,256]{1,0:T(8,128)S(1)} %get-tuple-element.30), channel_id=1, source_target_pairs={{0,1},{1,0},{2,3},{3,2},{4,5},{5,4},{6,7},{7,6},{8,9},{9,8},{10,11... | collective-permute-start | bytes 786440 | tf_op jit(solution)/shard_map/ppermute | solution.py:390
  (8 other events, 21.9 us)
